TPU v7x, 256 devices: a whole 4x4x8 slice. The times are simulated.
256 devices in a mesh: sp: 32 (over z, x), tp: 4 (over y), dp: 2 (over core).
Axes of the slice: x: 4, y: 4, z: 8, core: 2. Of those that a mesh axis runs over, the one named last changes fastest.
Arguments:
- latents: bfloat16 [2, 8192, 4096], P('dp', ('sp', 'tp')), may hold values from -8 to 8
- cond: bfloat16 [2, 4096], P('dp', 'sp'), may hold values from -6 to 6
- cond_ctx: bfloat16 [4096], P('sp'), may hold values from -6 to 6
- context: bfloat16 [2, 1024, 4096], P('dp', 'sp'), may hold values from -8 to 8
- w_shift: bfloat16 [4096, 4096], P('sp', 'tp'), may hold values from -0.09375 to 0.09375
- w_scale: bfloat16 [4096, 4096], P('sp', 'tp'), may hold values from -0.09375 to 0.09375
- w_gate: bfloat16 [4096, 4096], P('sp', 'tp'), may hold values from -0.1875 to 0.1875
- gain_pre: bfloat16 [4096], replicated, may hold values from 0.099609375 to 1.8984375
- gain_post: bfloat16 [4096], replicated, may hold values from 0.099609375 to 1.8984375
- w_query: bfloat16 [4096, 1024], P('dp', 'tp'), may hold values from -0.09375 to 0.09375
- w_key: bfloat16 [4096, 1024], P('dp', 'tp'), may hold values from -0.09375 to 0.09375
- w_value: bfloat16 [4096, 2048], P('dp', 'tp'), may hold values from -0.09375 to 0.09375
- w_outgate: bfloat16 [4096, 2048], P('dp', 'tp'), may hold values from -0.09375 to 0.09375
- w_down: bfloat16 [4096, 32], replicated, may hold values from -0.25 to 0.25
- decay_up: bfloat16 [2, 16, 1024], P(None, None, 'tp'), may hold values from -1.5 to 1.5
- decay_bias: float32 [2, 1024], P(None, 'tp'), may hold values from -0.5 to 11
- head_gain: bfloat16 [2048], P('tp'), may hold values from 0.099609375 to 1.8984375
- w_out: bfloat16 [2048, 4096], P('tp', 'dp'), may hold values from -0.125 to 0.125
Outputs:
- mixer_out: bfloat16 [2, 8192, 4096], P('dp', ('sp', 'tp'))
All inputs are finite; a program needn't handle non-finite values.
Results may differ from a plain program's by a relative error of at most 0.015.
Values may be sent and summed in bfloat16 or wider, within the bound.
A program may use at most 128 MiB of HBM per device.

v0:
```python
import jax
import jax.numpy as jnp
from jax import lax
from jax.sharding import Mesh
from jax.sharding import PartitionSpec as P

DK_HEAD = 256
DV_HEAD = 512
RANK = 16
BLOCK = 128
SP_TP = ("sp_0", "sp_1", "tp")
SP = ("sp_0", "sp_1")


EPS = 1e-06
TAU = 16.0


def over_axes(value, axes):
    for axis in axes:
        value = lax.psum(value, axis)
    return value


def rows_first(arrays, axis, dims):
    turned = [jnp.moveaxis(a, dim, 0) for a, dim in zip(arrays, dims)]
    widths = [t[0].size for t in turned]
    both = jnp.concatenate([t.reshape(-1, w) for t, w in zip(turned, widths)], axis=1)
    result = lax.all_gather(both, axis, axis=0, tiled=True)
    tiles = jnp.split(result, [sum(widths[:k]) for k in range(1, len(widths))], axis=1)
    return tuple(
        (
            jnp.moveaxis(b.reshape(-1, *t.shape[1:]), 0, dim)
            for b, t, dim in zip(tiles, turned, dims)
        )
    )


def in_one_piece(arrays, axis, dim, along):
    ends, at = ([], 0)
    for a in arrays[:-1]:
        at += a.shape[along]
        ends.append(at)
    both = jnp.concatenate(arrays, axis=along)
    return tuple(jnp.split(lax.all_gather(both, axis, axis=dim, tiled=True), ends, axis=along))


def nothing_yet(value, identity):
    return jax.tree.map(
        lambda a, e: jnp.broadcast_to(jnp.asarray(e, a.dtype), a.shape), value, identity
    )


def prefix_by_axis(value, axes, combine, identity, reverse):
    before = start = nothing_yet(value, identity)
    total = value
    for axis in reversed(axes):
        count, mine = (lax.axis_size(axis), lax.axis_index(axis))
        pieces = jax.tree.map(lambda part: lax.all_gather(part, axis), total)
        inside, total = (start, start)
        for k in reversed(range(count)) if reverse else range(count):
            passed = k > mine if reverse else k < mine
            total = combine(total, jax.tree.map(lambda part: part[k], pieces))
            inside = jax.tree.map(lambda new, old: jnp.where(passed, new, old), total, inside)
        before = combine(inside, before)
    return before


def in_blocks(value, dim, count):
    lengths = value.shape
    tiles = value.reshape(*lengths[:dim], count, lengths[dim] // count, *lengths[dim + 1 :])
    return jnp.moveaxis(tiles, dim, 0)


def sent_and_summed(value, axis, dim):
    tiles = in_blocks(value, dim, lax.axis_size(axis))
    arrived = lax.all_to_all(tiles, axis, split_axis=0, concat_axis=0, tiled=True)
    return arrived.astype(jnp.float32).sum(axis=0)


def matmul(left, right):
    return jnp.dot(left, right, preferred_element_type=jnp.float32)


def rms_scale(vectors, gain):
    return vectors * lax.rsqrt(jnp.mean(vectors * vectors, axis=-1, keepdims=True) + EPS) * gain


def log_decays(lowrank, decay_up, decay_bias):
    result = []
    for direction in range(2):
        preact = (
            matmul(lowrank[:, direction * RANK : (direction + 1) * RANK], decay_up[direction])
            + decay_bias[direction]
        )
        result.append(jax.nn.log_sigmoid(preact) / TAU)
    return result


def chain(earlier, later):
    return (earlier[0] + later[0], earlier[1] * jnp.exp(later[0])[:, :, None] + later[1])


def reverse_rows(array):
    return jnp.flip(array, axis=1)


def local_pass(queries, keys_in, values, decays):
    heads_here, length, key_width = queries.shape
    count = length // BLOCK
    middle = BLOCK // 2

    def blocks(array):
        return jnp.moveaxis(array.reshape(heads_here, count, BLOCK, array.shape[-1]), 1, 0)

    causal = jnp.tril(jnp.ones((BLOCK, BLOCK), bool))

    def advance(carried_state, inputs):
        query_block_tile, key_block_tile, value_block_tile, block_g = inputs
        running_decay_sum = jnp.cumsum(block_g, axis=1)
        center = running_decay_sum[:, middle : middle + 1]
        scores = jnp.einsum(
            "htk,hsk->hts",
            query_block_tile * jnp.exp(running_decay_sum - center),
            key_block_tile * jnp.exp(center - running_decay_sum),
        )
        scores = jnp.where(causal, scores, 0.0)
        final_state_value = running_decay_sum[:, -1:]
        output = jnp.einsum("hts,hsv->htv", scores, value_block_tile) + jnp.einsum(
            "nyf,nfe->nye", query_block_tile * jnp.exp(running_decay_sum), carried_state
        )
        carried_state = carried_state * jnp.exp(final_state_value[:, 0])[:, :, None] + jnp.einsum(
            "dzg,dzu->dgu",
            key_block_tile * jnp.exp(final_state_value - running_decay_sum),
            value_block_tile,
        )
        return (carried_state, output)

    initial = jnp.zeros((heads_here, key_width, values.shape[-1]), jnp.float32)
    carried_state, output = lax.scan(
        advance, initial, (blocks(queries), blocks(keys_in), blocks(values), blocks(decays))
    )
    output = jnp.moveaxis(output, 0, 1).reshape(heads_here, length, values.shape[-1])
    return (output, carried_state, jnp.sum(decays, axis=1))


def body(
    latents,
    cond,
    cond_ctx,
    context,
    w_shift,
    w_scale,
    w_gate,
    gain_pre,
    gain_post,
    w_query,
    w_key,
    w_value,
    w_outgate,
    w_down,
    decay_up,
    decay_bias,
    head_gain,
    w_out,
):
    width = gain_pre.shape[0]
    column_count = w_shift.shape[1]
    column_start = lax.axis_index("tp") * column_count
    activated = jax.nn.silu(cond.astype(jnp.float32)).astype(jnp.bfloat16)
    activated_ctx = jax.nn.silu(cond_ctx.astype(jnp.float32)).astype(jnp.bfloat16)[None, :]

    def placed(part):
        return lax.dynamic_update_slice_in_dim(
            jnp.zeros((part.shape[0], width), jnp.float32), part, column_start, 1
        )

    shift_vec, scale_vec, gate_vec, shift_ctx, scale_ctx = (
        over_axes(placed(matmul(activated, w_shift)), SP_TP),
        over_axes(placed(matmul(activated, w_scale)), SP_TP),
        over_axes(placed(matmul(activated, w_gate)), SP_TP),
        over_axes(placed(matmul(activated_ctx, w_shift)), SP_TP),
        over_axes(placed(matmul(activated_ctx, w_scale)), SP_TP),
    )
    w_query, w_key, w_value, w_outgate, w_out = rows_first(
        (w_query, w_key, w_value, w_outgate, w_out), "dp", (0, 0, 0, 0, 1)
    )

    def project(rows, mats):
        return tuple((matmul(rows, weight).astype(jnp.bfloat16) for weight in mats))

    gain_in = gain_pre.astype(jnp.float32)
    latent_rows = latents[0].astype(jnp.float32)
    modulated = (rms_scale(latent_rows, gain_in) * (1.0 + scale_vec[0]) + shift_vec[0]).astype(
        jnp.bfloat16
    )
    lowrank = matmul(modulated, w_down).astype(jnp.bfloat16)
    all_rows, all_lowrank = in_one_piece((modulated, lowrank), "tp", 0, 1)
    queries, latent_keys, values, out_gate = project(all_rows, (w_query, w_key, w_value, w_outgate))
    decay_fwd, decay_bwd = log_decays(all_lowrank, decay_up, decay_bias)
    ctx_float = context[0].astype(jnp.float32)
    modulated_ctx = (rms_scale(ctx_float, gain_in) * (1.0 + scale_ctx[0]) + shift_ctx[0]).astype(
        jnp.bfloat16
    )
    keys_part, values_part = project(modulated_ctx, (w_key, w_value))
    ctx_keys, ctx_values, ctx_lowrank = in_one_piece(
        (keys_part, values_part, matmul(modulated_ctx, w_down).astype(jnp.bfloat16)), SP, 0, 1
    )
    heads_here = queries.shape[1] // DK_HEAD

    def by_head(array, head_width):
        return jnp.moveaxis(
            array.astype(jnp.float32).reshape(array.shape[0], heads_here, head_width), 1, 0
        )

    ctx_fwd, ctx_bwd = log_decays(ctx_lowrank, decay_up, decay_bias)
    ctx_head_keys = by_head(ctx_keys, DK_HEAD)
    ctx_head_values = by_head(ctx_values, DV_HEAD)
    ctx_head_fwd = by_head(ctx_fwd, DK_HEAD)
    ctx_head_bwd = by_head(ctx_bwd, DK_HEAD)
    ctx_cumulative = jnp.cumsum(ctx_head_fwd, axis=1)
    start_fwd = jnp.einsum(
        "dzg,dzu->dgu",
        ctx_head_keys * jnp.exp(ctx_cumulative[:, -1:] - ctx_cumulative),
        ctx_head_values,
    )
    start_bwd = jnp.einsum(
        "dzg,dzu->dgu",
        ctx_head_keys * jnp.exp(jnp.cumsum(ctx_head_bwd, axis=1) - ctx_head_bwd),
        ctx_head_values,
    )
    head_query_rows = by_head(queries, DK_HEAD) * DK_HEAD ** (-0.5)
    head_k = by_head(latent_keys, DK_HEAD)
    head_v = by_head(values, DV_HEAD)
    forward_head_output = by_head(decay_fwd, DK_HEAD)
    backward_head_output = reverse_rows(by_head(decay_bwd, DK_HEAD))
    out_fwd, state_fwd, total_fwd = local_pass(head_query_rows, head_k, head_v, forward_head_output)
    empty_pair = (jnp.zeros_like(total_fwd), jnp.zeros_like(state_fwd))
    prior_total, prior_state = prefix_by_axis((total_fwd, state_fwd), SP, chain, empty_pair, False)
    forward_entry_state = start_fwd * jnp.exp(prior_total)[:, :, None] + prior_state
    out_fwd = out_fwd + jnp.einsum(
        "nyf,nfe->nye",
        head_query_rows * jnp.exp(jnp.cumsum(forward_head_output, axis=1)),
        forward_entry_state,
    )
    reversed_query_rows = reverse_rows(head_query_rows)
    out_bwd, state_bwd, total_bwd = local_pass(
        reversed_query_rows, reverse_rows(head_k), reverse_rows(head_v), backward_head_output
    )
    later_total, later_state = prefix_by_axis((total_bwd, state_bwd), SP, chain, empty_pair, True)
    backward_entry_state = start_bwd * jnp.exp(later_total)[:, :, None] + later_state
    out_bwd = out_bwd + jnp.einsum(
        "nyf,nfe->nye",
        reversed_query_rows * jnp.exp(jnp.cumsum(backward_head_output, axis=1)),
        backward_entry_state,
    )
    mixed_sum = out_fwd + reverse_rows(out_bwd)
    gains_head = by_head(head_gain[None, :], DV_HEAD)
    gated_rows = rms_scale(mixed_sum, gains_head) * jax.nn.silu(by_head(out_gate, DV_HEAD))
    heads_out = (
        jnp.moveaxis(gated_rows, 0, 1)
        .reshape(gated_rows.shape[1], heads_here * DV_HEAD)
        .astype(jnp.bfloat16)
    )
    rounded = lax.optimization_barrier(matmul(heads_out, w_out).astype(jnp.bfloat16))
    projected = sent_and_summed(rounded.astype(jnp.float32).astype(jnp.bfloat16), "tp", 0)
    result_rows = latent_rows + gate_vec[0] * rms_scale(projected, gain_post.astype(jnp.float32))
    return result_rows.astype(jnp.bfloat16)[None]


def solution(mesh):
    finer = Mesh(
        mesh.devices.reshape(8, 4, mesh.shape["tp"], mesh.shape["dp"]), ("sp_0", "sp_1", "tp", "dp")
    )
    in_specs = (
        P("dp", SP_TP, None),
        P("dp", SP),
        P(SP),
        P("dp", SP, None),
        P(SP, "tp"),
        P(SP, "tp"),
        P(SP, "tp"),
        P(),
        P(),
        P("dp", "tp"),
        P("dp", "tp"),
        P("dp", "tp"),
        P("dp", "tp"),
        P(),
        P(None, None, "tp"),
        P(None, "tp"),
        P("tp"),
        P("tp", "dp"),
    )
    out_specs = P("dp", SP_TP, None)
    return jax.shard_map(body, mesh=finer, in_specs=in_specs, out_specs=out_specs, check_vma=False)
```

profile of v0, /device:TPU:2, one launch (start us, length us, event | category | flops | bytes accessed | tf_op | source)
XLA Modules:
  0.0 587.9 jit_solution(8418258431428282053)
XLA Ops:
  13.3 74.2 %all-reduce.7.cloned.1.call-done = (f32[1,4096]{1,0:T(1,128)}, f32[1,4096]{1,0:T(1,128)}, f32[1,4096]{1,0:T(1,128)}, f32[1,4096]{1,0:T(1,128)}, f32[1,4096]{1,0:T(1,128)}) async-done(((f32[1,4096]{1,0:T(1,128)}, f32[1,4096]{1,0:T(1,128)}, f32[1,4096]{1,0:T(1,128)}, f32[1,4096]{1,0:T(1,128)}, f32[1,4096]{1,0:T(1,128)}), (f32[1,4096]{1,0:T(1,128)}, f32[1,4096]{1,0:T(1,128)}, f32[1,4096]{1,0:T(1,128)}, ...) | async-done | bytes 81936 | tf_op jit(solution)/shard_map/psum | solution.py:21
  88.8 46.9 %all-reduce.11.cloned.1.call-done = (f32[1,4096]{1,0:T(1,128)}, f32[1,4096]{1,0:T(1,128)}, f32[1,4096]{1,0:T(1,128)}, f32[1,4096]{1,0:T(1,128)}, f32[1,4096]{1,0:T(1,128)}) async-done(((f32[1,4096]{1,0:T(1,128)}, f32[1,4096]{1,0:T(1,128)}, f32[1,4096]{1,0:T(1,128)}, f32[1,4096]{1,0:T(1,128)}, f32[1,4096]{1,0:T(1,128)}), (f32[1,4096]{1,0:T(1,128)}, f32[1,4096]{1,0:T(1,128)}, f32[1,4096]{1,0:T(1,128)}, ...) | async-done | bytes 81936 | tf_op jit(solution)/shard_map/psum | solution.py:21
  135.9 49.7 %all-reduce.9.cloned.1.call-done = (f32[4096]{0:T(1024)}, f32[1,4096]{1,0:T(1,128)}, f32[4096]{0:T(1024)}, f32[1,4096]{1,0:T(1,128)}, f32[4096]{0:T(1024)}) async-done(((f32[4096]{0:T(1024)}, f32[1,4096]{1,0:T(1,128)}, f32[4096]{0:T(1024)}, f32[1,4096]{1,0:T(1,128)}, f32[4096]{0:T(1024)}), (f32[4096]{0:T(1024)}, f32[1,4096]{1,0:T(1,128)}, f32[4096]{0:T(1024)}, f32[1,4096]{1,0:T(1,128)}, ...) | async-done | bytes 81936 | tf_op jit(solution)/shard_map/psum | solution.py:21
  210.1 13.2 %all-gather.14.cloned.1.call-done = bf16[256,4128]{1,0:T(8,128)(2,1)} async-done(((bf16[64,4128]{1,0:T(8,128)(2,1)}), bf16[256,4128]{1,0:T(8,128)(2,1)}) %all-gather.14.cloned.1.call-update) | async-done | bytes 2113552 | tf_op jit(solution)/shard_map/all_gather | solution.py:45
  224.7 35.7 %all-gather.16.cloned.1.call-done = bf16[4096,2048]{0,1:T(8,128)(2,1)} async-done(((bf16[2048,2048]{0,1:T(8,128)(2,1)}), bf16[4096,2048]{0,1:T(8,128)(2,1)}) %all-gather.16.cloned.1.call-update) | async-done | bytes 16777232 | tf_op jit(solution)/shard_map/all_gather | solution.py:29
  263.5 4.1 fusion.131
  268.0 3.0 broadcast_multiply_fusion.2
  272.7 3.5 while.27
  287.2 3.5 fusion.168
  291.4 8.0 %all-gather.5 = f32[4,1,256]{2,1,0:T(1,128)S(1)} all-gather(f32[1,1,256]{2,1,0:T(1,128)S(1)} %bitcast.746), channel_id=4, replica_groups=mesh['sp_0'=8,'sp_1'=4,'tp'=4,'dp'=2] {'sp_1'}, dimensions={0}, use_global_device_ids=true | all-gather | bytes 5120 | tf_op jit(solution)/shard_map/all_gather | solution.py:59
  299.5 11.4 %all-gather.26.cloned.1.call-done = f32[4,256,512]{2,1,0:T(8,128)} async-done(((f32[1,256,512]{2,1,0:T(8,128)}), f32[4,256,512]{2,1,0:T(8,128)}) %all-gather.26.cloned.1.call-update) | async-done | bytes 2097168 | tf_op jit(solution)/shard_map/all_gather | solution.py:59
  313.5 8.5 %all-gather.4 = f32[4,1,256]{2,1,0:T(1,128)S(1)} all-gather(f32[1,1,256]{2,1,0:T(1,128)S(1)} %bitcast.748), channel_id=2, replica_groups=mesh['sp_0'=8,'sp_1'=4,'tp'=4,'dp'=2] {'sp_1'}, dimensions={0}, use_global_device_ids=true | all-gather | bytes 5120 | tf_op jit(solution)/shard_map/all_gather | solution.py:59
  322.0 24.1 %all-gather.24.cloned.1.call-done = f32[4,256,512]{2,1,0:T(8,128)} async-done(((f32[1,256,512]{2,1,0:T(8,128)}), f32[4,256,512]{2,1,0:T(8,128)}) %all-gather.24.cloned.1.call-update) | async-done | bytes 2097168 | tf_op jit(solution)/shard_map/all_gather | solution.py:59
  349.5 16.6 %all_gather.60 = f32[8,1,256]{2,1,0:T(1,128)S(1)} all-gather(f32[1,1,256]{2,1,0:T(1,128)S(1)} %get-tuple-element.224), channel_id=1, replica_groups=mesh['sp_0'=8,'sp_1'=4,'tp'=4,'dp'=2] {'sp_0'}, dimensions={0}, use_global_device_ids=true | all-gather | bytes 9216 | tf_op jit(solution)/shard_map/all_gather | solution.py:59
  367.2 14.4 %all_gather.54 = f32[8,1,256]{2,1,0:T(1,128)S(1)} all-gather(f32[1,1,256]{2,1,0:T(1,128)S(1)} %get-tuple-element.220), channel_id=1, replica_groups=mesh['sp_0'=8,'sp_1'=4,'tp'=4,'dp'=2] {'sp_0'}, dimensions={0}, use_global_device_ids=true | all-gather | bytes 9216 | tf_op jit(solution)/shard_map/all_gather | solution.py:59
  384.5 41.4 %all-gather.18.cloned.1.call-done = bf16[1024,800]{1,0:T(8,128)(2,1)} async-done(((bf16[32,800]{1,0:T(8,128)(2,1)}), bf16[1024,800]{1,0:T(8,128)(2,1)}) %all-gather.18.cloned.1.call-update) | async-done | bytes 1638416 | tf_op jit(solution)/shard_map/all_gather | solution.py:45
  436.0 45.0 %all-gather.22.cloned.1.call-done = f32[8,1,256,512]{3,2,1,0:T(8,128)} async-done(((f32[1,1,256,512]{3,2,1,0:T(8,128)}), f32[8,1,256,512]{3,2,1,0:T(8,128)}) %all-gather.22.cloned.1.call-update) | async-done | bytes 4194320 | tf_op jit(solution)/shard_map/all_gather | solution.py:59
  481.1 6.1 %fusion.125 = f32[256,512]{1,0:T(8,128)} fusion(f32[256,512]{1,0:T(8,128)} %bitcast.715, f32[1,256,1024]{1,2,0:T(8,128)} %bitcast_add_fusion, f32[1024,256]{1,0:T(8,128)S(1)} %copy-done.11, bf16[1024,800]{1,0:T(8,128)(2,1)} %all-gather.18.cloned.1.call-done, f32[8,1,256,512]{3,2,1,0:T(8,128)} %all-gather.22.cloned.1.call-done, ...), kind=kOutput, calls=%fused_computation.130 | convolution fusion | flops 341573632 | bytes 11548684 | tf_op jit(solution)/shard_map/nyf,nfe->nye/dot_general | solution.py:252
  487.2 3.4 reverse.21
  490.6 45.4 %all-gather.20.cloned.1.call-done = f32[8,1,256,512]{3,2,1,0:T(8,128)} async-done(((f32[1,1,256,512]{3,2,1,0:T(8,128)}), f32[8,1,256,512]{3,2,1,0:T(8,128)}) %all-gather.20.cloned.1.call-update) | async-done | bytes 4194320 | tf_op jit(solution)/shard_map/all_gather | solution.py:59
  536.0 4.9 multiply_reduce_fusion.1
  541.0 8.0 %convolution_convert_fusion = bf16[256,4096]{1,0:T(8,128)(2,1)} fusion(bf16[4096,2048]{0,1:T(8,128)(2,1)} %all-gather.16.cloned.1.call-done, bf16[256,4128]{1,0:T(8,128)(2,1)} %all-gather.14.cloned.1.call-done, f32[256,512]{1,0:T(8,128)S(1)} %get-tuple-element.263, f32[512]{0:T(512)S(1)} %copy-done.36, f32[256]{0:T(256)S(1)} %add_rsqrt_fusion), kind=kOutput, calls=%fused_computation.90 | convolution fusion | flops 2149842944 | bytes 13110272 | tf_op jit(solution)/shard_map/dot_general | solution.py:82
  548.9 4.4 all-to-all-start
  553.4 26.2 %all-to-all-done = bf16[4,64,4096]{2,1,0:T(8,128)(2,1)S(1)} async-done(((bf16[4,64,4096]{2,1,0:T(8,128)(2,1)}), bf16[4,64,4096]{2,1,0:T(8,128)(2,1)S(1)}, u32[]{:S(2)}, u32[]{:S(2)}) %all-to-all-start) | async-done | bytes 2097184 | tf_op jit(solution)/shard_map/all_to_all | solution.py:77
  (240 shorter events, 77.6 us)
Async XLA Ops:
  6.5 179.7 %copy-start.5 = (bf16[1,64,4096]{2,1,0:T(8,128)(2,1)S(1)}, bf16[1,64,4096]{2,1,0:T(8,128)(2,1)}, u32[]{:S(2)}) copy-start(bf16[1,64,4096]{2,1,0:T(8,128)(2,1)} %param.22) | copy-start | bytes 1572868
  6.5 129.3 %copy-start.26 = (bf16[4096]{0:T(1024)(128)(2,1)S(1)}, bf16[4096]{0:T(1024)(128)(2,1)}, u32[]{:S(2)}) copy-start(bf16[4096]{0:T(1024)(128)(2,1)} %param.29) | copy-start | bytes 24580
  6.5 180.7 %copy-start.13 = (bf16[4096,32]{0,1:T(8,128)(2,1)S(1)}, bf16[4096,32]{0,1:T(8,128)(2,1)}, u32[]{:S(2)}) copy-start(bf16[4096,32]{0,1:T(8,128)(2,1)} %param.35) | copy-start | bytes 786436
  6.5 80.9 %all-reduce.7.cloned.1.call-start = ((), (), s32[]{:S(2)}) async-start(), calls=%async_computation.8 | async-start | bytes 163840 | tf_op jit(solution)/shard_map/psum | solution.py:21
  13.2 122.5 %all-reduce.11.cloned.1.call-start = ((), (), s32[]{:S(2)}) async-start(), calls=%async_computation.10 | async-start | bytes 163840 | tf_op jit(solution)/shard_map/psum | solution.py:21
  87.5 98.0 %all-reduce.9.cloned.1.call-start = ((), (), s32[]{:S(2)}) async-start(), calls=%async_computation.9 | async-start | bytes 163840 | tf_op jit(solution)/shard_map/psum | solution.py:21
  135.8 87.5 %all-gather.14.cloned.1.call-start = ((), (), s32[]{:S(2)}) async-start(), calls=%async_computation.1 | async-start | bytes 2703360 | tf_op jit(solution)/shard_map/all_gather | solution.py:45
  135.9 55.1 %copy-start.18 = (f32[4096]{0:T(1024)}, f32[4096]{0:T(1024)S(1)}, u32[]{:S(2)}) copy-start(f32[4096]{0:T(1024)S(1)} %convert_element_type.101) | copy-start | bytes 49156
  188.5 71.9 %all-gather.16.cloned.1.call-start = ((), (), s32[]{:S(2)}) async-start(), calls=%async_computation.2 | async-start | bytes 25165824 | tf_op jit(solution)/shard_map/all_gather | solution.py:29
  208.9 101.9 %all-gather.26.cloned.1.call-start = ((), (), s32[]{:S(2)}) async-start(), calls=%async_computation.7 | async-start | bytes 2621440 | tf_op jit(solution)/shard_map/all_gather | solution.py:59
  277.0 69.0 %all-gather.24.cloned.1.call-start = ((), (), s32[]{:S(2)}) async-start(), calls=%async_computation.6 | async-start | bytes 2621440 | tf_op jit(solution)/shard_map/all_gather | solution.py:59
  281.3 144.6 %all-gather.18.cloned.1.call-start = ((), (), s32[]{:S(2)}) async-start(), calls=%async_computation.3 | async-start | bytes 1892352 | tf_op jit(solution)/shard_map/all_gather | solution.py:45
  291.4 189.6 %all-gather.22.cloned.1.call-start = ((), (), s32[]{:S(2)}) async-start(), calls=%async_computation.5 | async-start | bytes 4718592 | tf_op jit(solution)/shard_map/all_gather | solution.py:59
  299.4 49.2 %copy-start.30 = (f32[1,1,256]{2,1,0:T(1,128)}, f32[1,1,256]{2,1,0:T(1,128)S(1)}, u32[]{:S(2)}) copy-start(f32[1,1,256]{2,1,0:T(1,128)S(1)} %get-tuple-element.253) | copy-start | bytes 3076
  299.4 49.1 %copy-start.32 = (f32[1,1,256]{2,1,0:T(1,128)}, f32[1,1,256]{2,1,0:T(1,128)S(1)}, u32[]{:S(2)}) copy-start(f32[1,1,256]{2,1,0:T(1,128)S(1)} %get-tuple-element.254) | copy-start | bytes 3076
  313.4 222.6 %all-gather.20.cloned.1.call-start = ((), (), s32[]{:S(2)}) async-start(), calls=%async_computation.4 | async-start | bytes 4718592 | tf_op jit(solution)/shard_map/all_gather | solution.py:59
  348.6 77.3 %copy-start.45 = (f32[1,256]{1,0:T(1,128)S(1)}, f32[1,256]{1,0:T(1,128)}, u32[]{:S(2)}) copy-start(f32[1,256]{1,0:T(1,128)} %copy-done.44) | copy-start | bytes 3076
  348.6 77.3 %copy-start.47 = (bf16[2,16,256]{2,1,0:T(8,128)(2,1)S(1)}, bf16[2,16,256]{2,1,0:T(8,128)(2,1)}, u32[]{:S(2)}) copy-start(bf16[2,16,256]{2,1,0:T(8,128)(2,1)} %param.36) | copy-start | bytes 49156
  481.0 55.0 %copy-start.9 = (f32[1,256,1024]{1,2,0:T(8,128)S(1)}, f32[1,256,1024]{1,2,0:T(8,128)}, u32[]{:S(2)}) copy-start(f32[1,256,1024]{1,2,0:T(8,128)} %copy-done.8) | copy-start | bytes 3145732
  481.0 55.0 %copy-start.16 = (f32[256,256]{1,0:T(8,128)S(1)}, f32[256,256]{1,0:T(8,128)}, u32[]{:S(2)}) copy-start(f32[256,256]{1,0:T(8,128)} %copy-done.15) | copy-start | bytes 786436
  481.1 55.0 %copy-start.17 = (f32[1,256,256]{1,2,0:T(8,128)S(1)}, f32[1,256,256]{1,2,0:T(8,128)}, u32[]{:S(2)}) copy-start(f32[1,256,256]{1,2,0:T(8,128)} %fusion.331) | copy-start | bytes 786436
  481.1 55.0 %copy-start.39 = (f32[1,1,256]{2,1,0:T(1,128)S(1)}, f32[1,1,256]{2,1,0:T(1,128)}, u32[]{:S(2)}) copy-start(f32[1,1,256]{2,1,0:T(1,128)} %get-tuple-element.218) | copy-start | bytes 3076
  481.1 55.0 %copy-start.41 = (f32[1,1,256]{2,1,0:T(1,128)S(1)}, f32[1,1,256]{2,1,0:T(1,128)}, u32[]{:S(2)}) copy-start(f32[1,1,256]{2,1,0:T(1,128)} %exp.528) | copy-start | bytes 3076
  548.9 30.6 %all-to-all-start = ((bf16[4,64,4096]{2,1,0:T(8,128)(2,1)}), bf16[4,64,4096]{2,1,0:T(8,128)(2,1)S(1)}, u32[]{:S(2)}, u32[]{:S(2)}) async-start(bf16[4,64,4096]{2,1,0:T(8,128)(2,1)} %bitcast.711), calls=%async_computation | async-start | bytes 4194304 | tf_op jit(solution)/shard_map/all_to_all | solution.py:77
  (37 other events, 557.8 us)
Sparse Core Ops, SparseCore 0:
  13.4 74.0 all-reduce.6
  90.2 45.5 all-reduce.10
  138.4 47.0 all-reduce.8
  188.6 34.5 all-gather.13
  224.9 35.4 all-gather.15
  277.1 33.6 all-gather.25
  312.7 33.3 all-gather.23
  348.6 77.2 all-gather.17
  427.7 53.2 all-gather.21
  482.6 53.3 all-gather.19
where the time goes:
time: 589 us; the launch traced here: 588 us
  waiting for transfers between devices  413 us (70%)
  matrix products  52.2 us (9%)
  blocking collectives  47.5 us (8%)
  local copies, waits for them, and re-layouts  34.5 us (6%)
  other arithmetic  21.2 us (4%)
  between operations  14.4 us (2%)
    psum x3, waiting for transfers between devices, over_axes(): value = lax.psum(value, axis)  171 us
    all_gather x4, waiting for transfers between devices, prefix_by_axis(): pieces = jax.tree.map(lambda part: lax.all_gather(part, axis), total)  126 us
    all_gather x2, waiting for transfers between devices, in_one_piece(): lax.all_gather(both, axis, axis=dim, tiled=True)  54.5 us
    all_gather x4, blocking collectives, prefix_by_axis(): pieces = jax.tree.map(lambda part: lax.all_gather(part, axis), total)  47.5 us
    dot_general x17, matrix products, matmul(): return jnp.dot(left, right, preferred_element_type=jnp.float32)  36.6 us
    all_gather x1, waiting for transfers between devices, rows_first(): result = lax.all_gather(both, axis, axis=0, tiled=True)  35.7 us
    all_to_all x1, waiting for transfers between devices, sent_and_summed(): lax.all_to_all(tiles, axis, split_axis=0, concat_axis=0, tiled=True)  26.2 us
    unnamed x108, local copies, waits for them, and re-layouts  24.2 us
  transfers between devices with their start and end apart: 11, of which 11 were waited for; matrix products, arithmetic and copies ran while one was open for 11% of the time, Pallas kernels for 0%

commit v1 on v0

v1 whole, which is shorter than its diff:
```python
import jax
import jax.numpy as jnp
from jax import lax
from jax.experimental import pallas as pl
from jax.experimental.pallas import tpu as pltpu
from jax.sharding import Mesh
from jax.sharding import PartitionSpec as P

DK_HEAD = 256
DV_HEAD = 512
RANK = 16
BLOCK = 128
SP_TP = ("sp_0", "sp_1", "tp")
SP = ("sp_0", "sp_1")
NZ, NX, NY = 8, 4, 4
WIDTH = 4096
HALF = 2048
ANY = pl.BlockSpec(memory_space=pl.ANY)
VM = pl.BlockSpec(memory_space=pltpu.VMEM)
BF, F32 = jnp.bfloat16, jnp.float32


EPS = 1e-06
TAU = 16.0


def matmul(left, right):
    return jnp.dot(left, right, preferred_element_type=jnp.float32)


def rms_scale(vectors, gain):
    return vectors * lax.rsqrt(jnp.mean(vectors * vectors, axis=-1, keepdims=True) + EPS) * gain


def shape_of(*dims, dtype=BF):
    return jax.ShapeDtypeStruct(dims, dtype)


def send(src, dst, send_sem, recv_sem, **where):
    copy = pltpu.make_async_remote_copy(
        src_ref=src,
        dst_ref=dst,
        send_sem=send_sem,
        recv_sem=recv_sem,
        device_id=where,
        device_id_type=pl.DeviceIdType.MESH,
    )
    copy.start()
    return copy


def greet(partners):
    barrier = pltpu.get_barrier_semaphore()
    for where in partners:
        pl.semaphore_signal(
            barrier, inc=1, device_id=where, device_id_type=pl.DeviceIdType.MESH
        )
    return lambda: pl.semaphore_wait(barrier, len(partners))


def position():
    return tuple(lax.axis_index(a) for a in ("sp_0", "sp_1", "tp", "dp"))


def gather_kernel(
    lat, cond, cond_ctx, w_shift, w_scale, w_gate, wq, wk, wv, wg, wo,
    mods, lat_all, wq2, wk2, wv2, wg2, wo2,
    w_mod, lat_here, partial, arrived, tile,
    load_sem, s1, r1, s2, r2, sl, rl, sw, rw,
):
    z, x, y, c = position()
    at_sp = [
        (k, dict(sp_0=lax.rem(z + k // NX, NZ), sp_1=lax.rem(x + k % NX, NX)))
        for k in range(1, NZ * NX)
    ]
    at_yz = [
        (k, dict(sp_0=lax.rem(z + k // NY, NZ), tp=lax.rem(y + k % NY, NY)))
        for k in range(1, NZ * NY)
    ]
    other = dict(dp=1 - c)
    up, down = dict(tp=lax.rem(y + 1, NY)), dict(tp=lax.rem(y + 3, NY))
    entered = greet(
        [w for _, w in at_sp] + [w for k, w in at_yz if k % NY != 0] + [other]
    )
    loads = [
        pltpu.make_async_copy(src, dst, load_sem.at[k])
        for k, (src, dst) in enumerate(
            [(w_shift, w_mod.at[0]), (w_scale, w_mod.at[1]), (w_gate, w_mod.at[2]),
             (lat, lat_here)]
        )
    ]
    for load in loads:
        load.start()
    own = pltpu.make_async_copy(lat, lat_all.at[y], load_sem.at[4])
    own.start()
    rows = lax.broadcasted_iota(jnp.int32, (16, 128), 0)
    act = jax.nn.silu(cond[...].astype(F32))
    act_ctx = jax.nn.silu(cond_ctx[...].astype(F32))
    total = None
    for k in range(3):
        left = jnp.where(rows == k, act, jnp.where(rows == k + 3, act_ctx, 0.0)).astype(BF)
        loads[k].wait()
        part = matmul(left, w_mod[k])
        total = part if total is None else total + part
    for k in range(NZ):
        partial[k] = total[:8, k * 128 : (k + 1) * 128]
    entered()
    sends = [
        send(partial.at[w["sp_0"]], arrived.at[k], s1.at[k], r1.at[k], **w) for k, w in at_sp
    ]
    loads[3].wait()
    to_up = send(lat_here, lat_all.at[y], sl.at[0], rl.at[0], **up)
    to_down = send(lat_here, lat_all.at[y], sl.at[1], rl.at[1], **down)
    weights = [
        send(src, dst, sw.at[k], rw.at[k], **other)
        for k, (src, dst) in enumerate(
            [(wq, wq2), (wk, wk2), (wv, wv2), (wg, wg2), (wo, wo2)]
        )
    ]
    for copy in sends:
        copy.wait()
    summed = partial[z]
    for k in range(1, NZ * NX):
        summed = summed + arrived[k]
    tile[...] = summed
    here = y * NZ + z
    mods[here] = summed
    sends = [send(tile, mods.at[here], s2.at[k], r2.at[k], **w) for k, w in at_yz]
    for copy in sends:
        copy.wait()
    to_up.wait()
    before = lat_all.at[lax.rem(y + 3, NY), pl.ds(0, 32)]
    relay_up = send(before, before, sl.at[2], rl.at[2], **up)
    to_down.wait()
    after = lat_all.at[lax.rem(y + 1, NY), pl.ds(32, 32)]
    relay_down = send(after, after, sl.at[3], rl.at[3], **down)
    own.wait()
    relay_up.wait()
    relay_down.wait()
    for copy in weights:
        copy.wait()


def gather_inputs(lat, cond, cond_ctx, w_shift, w_scale, w_gate, *weights):
    dma = pltpu.SemaphoreType.DMA
    return pl.pallas_call(
        gather_kernel,
        out_shape=[shape_of(NY * NZ, 8, 128, dtype=F32), shape_of(NY, *lat.shape)]
        + [shape_of(*w.shape) for w in weights],
        in_specs=[ANY, VM, VM] + [ANY] * 8,
        out_specs=[VM, VM] + [ANY] * 5,
        scratch_shapes=[
            pltpu.VMEM((3, 128, 1024), BF),
            pltpu.VMEM(lat.shape, BF),
            pltpu.VMEM((NZ, 8, 128), F32),
            pltpu.VMEM((NZ * NX, 8, 128), F32),
            pltpu.VMEM((8, 128), F32),
            dma((5,)), dma((32,)), dma((32,)), dma((32,)), dma((32,)),
            dma((4,)), dma((4,)), dma((5,)), dma((5,)),
        ],
        compiler_params=pltpu.CompilerParams(collective_id=0, has_side_effects=True),
        name="gather_inputs",
    )(lat, cond, cond_ctx, w_shift, w_scale, w_gate, *weights)


def exchange_x_kernel(count, *refs):
    ins, outs, (s, r) = refs[:count], refs[count : 2 * count], refs[2 * count :]
    x = lax.axis_index("sp_1")
    peers = [(d, lax.rem(x + d, NX)) for d in range(1, NX)]
    entered = greet([dict(sp_1=p) for _, p in peers])
    for a, b in zip(ins, outs):
        b[x] = a[x]
    entered()
    copies = [
        send(a.at[p], b.at[x], s.at[k, d], r.at[k, d], sp_1=p)
        for k, (a, b) in enumerate(zip(ins, outs))
        for d, p in peers
    ]
    for copy in copies:
        copy.wait()


def exchange_x(collective_id, *arrays):
    n = len(arrays)
    return pl.pallas_call(
        lambda *refs: exchange_x_kernel(n, *refs),
        out_shape=[shape_of(*a.shape, dtype=a.dtype) for a in arrays],
        in_specs=[VM] * n,
        out_specs=[VM] * n,
        scratch_shapes=[pltpu.SemaphoreType.DMA((n, NX))] * 2,
        compiler_params=pltpu.CompilerParams(
            collective_id=collective_id, has_side_effects=True
        ),
        name=f"exchange_x_{collective_id}",
    )(*arrays)


def scan_z_kernel(group, decays, entry, got, got_decays, back, s, r, s_dec, r_dec, s_back, r_back):
    z = lax.axis_index("sp_0")
    peers = [(d, lax.rem(z + d, NZ)) for d in range(1, NZ)]
    entered = greet([dict(sp_0=p) for _, p in peers])
    got[z] = group[z]
    got_decays[z] = decays[...]
    entered()
    copies = []
    for d, p in peers:
        copies.append(send(group.at[p], got.at[z], s.at[d], r.at[d], sp_0=p))
        copies.append(send(decays, got_decays.at[z], s_dec.at[d], r_dec.at[d], sp_0=p))
    for copy in copies:
        copy.wait()
    for way in range(2):
        order = range(NZ) if way == 0 else range(NZ - 1, -1, -1)
        state = jnp.zeros((16, 256), F32)
        for k in order:
            state = state * jnp.exp(got_decays[k, 2 + way : 3 + way]) + got[k, 2 + way].astype(F32)
        for k in order:
            back[k, way] = state.astype(BF)
            state = state * jnp.exp(got_decays[k, way : way + 1]) + got[k, way].astype(F32)
    entry[z] = back[z]
    copies = [send(back.at[p], entry.at[z], s_back.at[d], r_back.at[d], sp_0=p) for d, p in peers]
    for copy in copies:
        copy.wait()


def scan_z(group, decays):
    dma = pltpu.SemaphoreType.DMA((NZ,))
    return pl.pallas_call(
        scan_z_kernel,
        out_shape=shape_of(NZ, 2, 16, 256),
        in_specs=[VM, VM],
        out_specs=VM,
        scratch_shapes=[
            pltpu.VMEM((NZ, 4, 16, 256), BF),
            pltpu.VMEM((NZ, 8, 256), F32),
            pltpu.VMEM((NZ, 2, 16, 256), BF),
        ]
        + [dma] * 6,
        compiler_params=pltpu.CompilerParams(collective_id=2, has_side_effects=True),
        name="scan_z",
    )(group, decays)


def reduce_y_kernel(pa, pb, out_a, out_b, near_a, near_b, far_a, far_b, sum_a, sum_b, relay_a, relay_b, s, r):
    y = lax.axis_index("tp")
    above, below, across = (lax.rem(y + k, NY) for k in (1, 3, 2))
    up, down = dict(tp=above), dict(tp=below)
    greet([up, down])()
    first_a = send(pa.at[across], relay_a, s.at[0], r.at[0], **down)
    first_b = send(pb.at[across], relay_b, s.at[1], r.at[1], **up)
    direct_b = send(pb.at[below], near_b, s.at[2], r.at[2], **down)
    direct_a = send(pa.at[above], near_a, s.at[3], r.at[3], **up)
    first_a.wait()
    sum_a[...] = (relay_a[...].astype(F32) + pa[below].astype(F32)).astype(BF)
    second_a = send(sum_a, far_a, s.at[4], r.at[4], **down)
    first_b.wait()
    sum_b[...] = (relay_b[...].astype(F32) + pb[above].astype(F32)).astype(BF)
    second_b = send(sum_b, far_b, s.at[5], r.at[5], **up)
    direct_a.wait()
    direct_b.wait()
    second_a.wait()
    out_a[...] = pa[y].astype(F32) + near_a[...].astype(F32) + far_a[...].astype(F32)
    second_b.wait()
    out_b[...] = pb[y].astype(F32) + near_b[...].astype(F32) + far_b[...].astype(F32)


def reduce_y(pa, pb):
    block = pltpu.VMEM(pa.shape[1:], BF)
    dma = pltpu.SemaphoreType.DMA((6,))
    return pl.pallas_call(
        reduce_y_kernel,
        out_shape=[shape_of(*pa.shape[1:], dtype=F32)] * 2,
        in_specs=[VM, VM],
        out_specs=[VM, VM],
        scratch_shapes=[block] * 8 + [dma] * 2,
        compiler_params=pltpu.CompilerParams(collective_id=4, has_side_effects=True),
        name="reduce_y",
    )(pa, pb)


def log_decays(lowrank, decay_up, decay_bias):
    return [
        jax.nn.log_sigmoid(
            matmul(lowrank[:, way * RANK : (way + 1) * RANK], decay_up[way]) + decay_bias[way]
        )
        / TAU
        for way in range(2)
    ]


def running_sums(decay_fwd, decay_bwd):
    n = decay_fwd.shape[0]
    lower = jnp.tril(jnp.ones((n, n), F32))
    fwd = jnp.dot(lower, decay_fwd, precision=lax.Precision.HIGHEST)
    bwd = jnp.dot(lower.T, decay_bwd, precision=lax.Precision.HIGHEST)
    return fwd, bwd


def across(left, right):
    return lax.dot_general(left, right, (((1,), (1,)), ((), ())), preferred_element_type=F32)


def outer(left, right):
    return lax.dot_general(left, right, (((0,), (0,)), ((), ())), preferred_element_type=F32)


def scores_of(queries, keys_in, fwd, bwd):
    tri = jnp.tril(jnp.ones((BLOCK, BLOCK), bool))
    bf = lambda a: a.astype(BF)
    rows = []
    for b in range(2):
        sl = slice(b * BLOCK, (b + 1) * BLOCK)
        q, k, f, g = queries[sl], keys_in[sl], fwd[sl], bwd[sl]
        cf, cg = f[BLOCK // 2 : BLOCK // 2 + 1], g[BLOCK // 2 - 1 : BLOCK // 2]
        sf = across(bf(q * jnp.exp(f - cf)), bf(k * jnp.exp(cf - f)))
        sb = across(bf(q * jnp.exp(g - cg)), bf(k * jnp.exp(cg - g)))
        near = jnp.where(tri, sf, 0.0) + jnp.where(tri.T, sb, 0.0)
        osl = slice((1 - b) * BLOCK, (2 - b) * BLOCK)
        if b == 0:
            edge = bwd[BLOCK : BLOCK + 1]
            far = across(bf(q * jnp.exp(g - edge)), bf(keys_in[osl] * jnp.exp(edge - bwd[osl])))
            rows.append(jnp.concatenate([near, far], axis=1))
        else:
            edge = fwd[BLOCK - 1 : BLOCK]
            far = across(bf(q * jnp.exp(f - edge)), bf(keys_in[osl] * jnp.exp(edge - fwd[osl])))
            rows.append(jnp.concatenate([far, near], axis=1))
    return jnp.concatenate(rows, axis=0)


def body(
    latents, cond, cond_ctx, context, w_shift, w_scale, w_gate, gain_pre, gain_post,
    w_query, w_key, w_value, w_outgate, w_down, decay_up, decay_bias, head_gain, w_out,
):
    z, x, y, c = position()
    latents, context = latents[0], context[0]
    mods, lat_all, wq2, wk2, wv2, wg2, wo2 = gather_inputs(
        latents, cond, cond_ctx[None], w_shift, w_scale, w_gate,
        w_query, w_key, w_value, w_outgate, w_out,
    )
    mods = jnp.moveaxis(mods, 0, 1).reshape(8, WIDTH)
    shift_vec, scale_vec, gate_vec, shift_ctx, scale_ctx = (mods[k : k + 1] for k in range(5))
    gain_in = gain_pre.astype(F32)

    def halves(array):
        return (
            lax.dynamic_slice_in_dim(array, c * HALF, HALF, 1),
            lax.dynamic_slice_in_dim(array, (1 - c) * HALF, HALF, 1),
        )

    def project(rows, here, there):
        mine, theirs = rows
        return (matmul(mine, here) + matmul(theirs, there)).astype(BF)

    rows = lat_all.reshape(NY * latents.shape[0], WIDTH).astype(F32)
    modulated = (rms_scale(rows, gain_in) * (1.0 + scale_vec) + shift_vec).astype(BF)
    lowrank = matmul(modulated, w_down).astype(BF)
    modulated = halves(modulated)
    queries = project(modulated, w_query, wq2)
    keys_in = project(modulated, w_key, wk2)
    values = project(modulated, w_value, wv2)
    out_gate = project(modulated, w_outgate, wg2)
    ctx_rows = context.astype(F32)
    modulated_ctx = (rms_scale(ctx_rows, gain_in) * (1.0 + scale_ctx) + shift_ctx).astype(BF)
    ctx_lowrank = matmul(modulated_ctx, w_down).astype(BF)
    modulated_ctx = halves(modulated_ctx)
    ctx_keys = project(modulated_ctx, w_key, wk2)
    ctx_values = project(modulated_ctx, w_value, wv2)

    fwd, bwd = running_sums(*log_decays(lowrank, decay_up, decay_bias))
    q = queries.astype(F32) * DK_HEAD ** (-0.5)
    k = keys_in.astype(F32)
    scores = scores_of(q, k, fwd, bwd)
    out = matmul(scores.astype(BF), values)
    state_f = outer(values, (k * jnp.exp(fwd[-1:] - fwd)).astype(BF)).astype(BF)
    state_b = outer(values, (k * jnp.exp(bwd[:1] - bwd)).astype(BF)).astype(BF)
    states = jnp.stack(
        [state_f.reshape(NX, 128, DK_HEAD), state_b.reshape(NX, 128, DK_HEAD)], axis=1
    )
    totals = jnp.concatenate([fwd[-1:], bwd[:1], jnp.zeros((6, DK_HEAD), F32)], axis=0)
    totals = jnp.broadcast_to(totals[None], (NX, 8, DK_HEAD))
    ctx_count = context.shape[0]
    ctx_pack = jnp.concatenate(
        [
            jnp.broadcast_to(ctx_keys[None], (NX, ctx_count, DK_HEAD)),
            jnp.moveaxis(ctx_values.reshape(ctx_count, NX, 128), 1, 0),
            jnp.broadcast_to(
                jnp.pad(ctx_lowrank, ((0, 0), (0, 128 - 2 * RANK)))[None], (NX, ctx_count, 128)
            ),
        ],
        axis=2,
    )
    states, totals, ctx_pack = exchange_x(1, states, totals, ctx_pack)

    ctx_pack = ctx_pack.reshape(NX * ctx_count, 512)
    ctx_k = ctx_pack[:, :DK_HEAD].astype(F32)
    ctx_v = ctx_pack[:, DK_HEAD : DK_HEAD + 128]
    ctx_lr = ctx_pack[:, DK_HEAD + 128 : DK_HEAD + 128 + 2 * RANK]
    cf, cb = running_sums(*log_decays(ctx_lr, decay_up, decay_bias))
    ctx_f = outer(ctx_v, (ctx_k * jnp.exp(cf[-1:] - cf)).astype(BF))
    ctx_b = outer(ctx_v, (ctx_k * jnp.exp(cb[:1] - cb)).astype(BF))

    def inside(way, order):
        state = jnp.zeros((128, DK_HEAD), F32)
        decay = jnp.zeros((1, DK_HEAD), F32)
        before, passed = [None] * NX, [None] * NX
        for j in order:
            before[j], passed[j] = state, decay
            step = totals[j, way : way + 1]
            state = state * jnp.exp(step) + states[j, way].astype(F32)
            decay = decay + step
        return state, decay, before, passed

    group_f, total_f, before_f, passed_f = inside(0, range(NX))
    group_b, total_b, before_b, passed_b = inside(1, range(NX - 1, -1, -1))
    group = jnp.stack([group_f, group_b, ctx_f, ctx_b]).astype(BF)
    group = jnp.moveaxis(group.reshape(4, NZ, 16, DK_HEAD), 1, 0)
    group_decays = jnp.concatenate(
        [total_f, total_b, cf[-1:], cb[:1], jnp.zeros((4, DK_HEAD), F32)], axis=0
    )
    entry = scan_z(group, group_decays)
    entry = jnp.moveaxis(entry, 1, 0).reshape(2, 128, DK_HEAD).astype(F32)
    entries = jnp.stack(
        [
            jnp.stack(
                [
                    entry[0] * jnp.exp(passed_f[j]) + before_f[j],
                    entry[1] * jnp.exp(passed_b[j]) + before_b[j],
                ]
            )
            for j in range(NX)
        ]
    ).astype(BF)
    (entries,) = exchange_x(3, entries)
    entries = jnp.moveaxis(entries, 1, 0).reshape(2, DV_HEAD, DK_HEAD)
    out = out + across((q * jnp.exp(fwd)).astype(BF), entries[0])
    out = out + across((q * jnp.exp(bwd)).astype(BF), entries[1])

    gated = rms_scale(out, head_gain.astype(F32)[None]) * jax.nn.silu(out_gate.astype(F32))
    heads_out = gated.astype(BF)
    shape = (NY, latents.shape[0], HALF)
    pa = matmul(heads_out, w_out).astype(BF).reshape(shape)
    pb = matmul(heads_out, wo2).astype(BF).reshape(shape)
    mine, theirs = reduce_y(pa, pb)
    first = c == 0
    projected = jnp.concatenate(
        [jnp.where(first, mine, theirs), jnp.where(first, theirs, mine)], axis=1
    )
    result = latents.astype(F32) + gate_vec * rms_scale(projected, gain_post.astype(F32))
    return result.astype(BF)[None]


def solution(mesh):
    finer = Mesh(
        mesh.devices.reshape(8, 4, mesh.shape["tp"], mesh.shape["dp"]), ("sp_0", "sp_1", "tp", "dp")
    )
    in_specs = (
        P("dp", SP_TP, None),
        P("dp", SP),
        P(SP),
        P("dp", SP, None),
        P(SP, "tp"),
        P(SP, "tp"),
        P(SP, "tp"),
        P(),
        P(),
        P("dp", "tp"),
        P("dp", "tp"),
        P("dp", "tp"),
        P("dp", "tp"),
        P(),
        P(None, None, "tp"),
        P(None, "tp"),
        P("tp"),
        P("tp", "dp"),
    )
    out_specs = P("dp", SP_TP, None)
    return jax.shard_map(body, mesh=finer, in_specs=in_specs, out_specs=out_specs, check_vma=False)
```

time: 589 us -> 138 us (0.23)
  waiting for transfers between devices: 413 us -> 0 us
  Pallas kernels: 0 us -> 93.6 us
  blocking collectives: 47.5 us -> 0 us
  matrix products: 52.2 us -> 19.6 us
  local copies, waits for them, and re-layouts: 34.5 us -> 6 us
  between operations: 14.4 us -> 0.78 us
    all_gather x7 -> x0, waiting for transfers between devices: 216 us -> none  [the longest x4 126 us: prefix_by_axis(): pieces = jax.tree.map(lambda part: lax.all_gather(part, axis), total)]
    psum x3 -> x0, waiting for transfers between devices: 171 us -> none  [over_axes(): value = lax.psum(value, axis)]
    pallas_call x0 -> x5, Pallas kernels: none -> 93.6 us  [the longest x1 35.4 us: gather_inputs(): pl.pallas_call(gather_kernel, out_shape=[shape_of(NY * NZ, 8, 128, dtype=...]
    all_gather x4 -> x0, blocking collectives: 47.5 us -> none  [prefix_by_axis(): pieces = jax.tree.map(lambda part: lax.all_gather(part, axis), total)]
    all_to_all x1 -> x0, waiting for transfers between devices: 26.2 us -> none  [sent_and_summed(): lax.all_to_all(tiles, axis, split_axis=0, concat_axis=0, tiled=True)]
    dot_general x17 -> x21, matrix products: 36.6 us -> 15.1 us  [matmul(): return jnp.dot(left, right, preferred_element_type=jnp.float32)]
    unnamed x108 -> x56, local copies, waits for them, and re-layouts: 24.2 us -> 3.36 us
    dot_general x14 -> x16, matrix products: 15.6 us -> 4.51 us  [the longest x8 1.8 us: across(): lax.dot_general(left, right, (((1,), (1,)), ((), ())), preferred_element_...]
  transfers between devices with their start and end apart: 11 -> 0, of which waited for: 11 -> 0; matrix products, arithmetic and copies ran while one was open for 11% -> 0% of each run, Pallas kernels for 0% -> 0%
where the time goes in v1:
time: 138 us; the launch traced here: 137 us
  Pallas kernels  93.6 us (68%)
  matrix products  19.6 us (14%)
  other arithmetic  16.9 us (12%)
  local copies, waits for them, and re-layouts  6 us (4%)
    pallas_call x1, Pallas kernels, gather_inputs(): pl.pallas_call(gather_kernel, out_shape=[shape_of(NY * NZ, 8, 128, dtype=...  35.4 us
    pallas_call x2, Pallas kernels, exchange_x(): pl.pallas_call(lambda *refs: exchange_x_kernel(n, *refs), out_shape=[shap...  20.3 us
    pallas_call x1, Pallas kernels, reduce_y(): pl.pallas_call(reduce_y_kernel, out_shape=[shape_of(*pa.shape[1:], dtype=...  19.4 us
    pallas_call x1, Pallas kernels, scan_z(): pl.pallas_call(scan_z_kernel, out_shape=shape_of(NZ, 2, 16, 256), in_spec...  18.5 us
    dot_general x21, matrix products, matmul(): return jnp.dot(left, right, preferred_element_type=jnp.float32)  15.1 us
    unnamed x56, local copies, waits for them, and re-layouts  3.36 us

profile of v1, /device:TPU:2, one launch (start us, length us, event | category | flops | bytes accessed | tf_op | source)
XLA Modules:
  0.0 136.9 jit_solution(8134650217782314902)
XLA Ops:
  0.0 35.4 %gather_inputs.1 = (f32[32,8,128]{2,1,0:T(8,128)}, bf16[4,64,4096]{2,1,0:T(8,128)(2,1)}, bf16[2048,256]{1,0:T(8,128)(2,1)}, bf16[2048,256]{1,0:T(8,128)(2,1)}, b...) custom-call(bf16[64,4096]{1,0:T(8,128)(2,1)} %bitcast.189, bf16[1,128]{1,0:T(2,128)(2,1)} %cond.1, ...), custom_call_target="tpu_custom_call" | custom-call | tf_op jit(solution)/shard_map/gather_inputs/pallas_call | solution.py:146
  35.5 1.4 %fusion.187 = (f32[1,32,128]{2,0,1:T(1,128)S(1)}, f32[1,32,128]{2,0,1:T(1,128)S(1)}, f32[1,32,128]{2,0,1:T(1,128)S(1)}, f32[1,32,128]{2,0,1:T(1,128)S(1)}, f32[1,32,128]{2,0,1:T(1,128)S(1)}) fusion(f32[8,32,128]{2,0,1:T(8,128)} %bitcast.219), kind=kLoop, calls=%fused_computation.291 | loop fusion | flops 8192 | bytes 163840 | tf_op jit(solution)/shard_map/slice | solution.py:340
  36.9 2.1 %multiply_reduce_fusion = f32[4,64]{1,0:T(4,128)S(1)} fusion(bf16[4,64,4096]{2,1,0:T(8,128)(2,1)} %get-tuple-element.18), kind=kLoop, calls=%fused_computation.5 | loop fusion | flops 3145472 | bytes 2098176 | tf_op jit(solution)/shard_map/reduce_sum | solution.py:32
  39.1 2.5 %fusion.3 = bf16[256,4096]{1,0:T(8,128)(2,1)S(1)} fusion(f32[4096]{0:T(1024)S(1)} %bitcast.215, f32[4096]{0:T(1024)S(1)} %bitcast.216, f32[4096]{0:T(1024)S(1)} %convert_element_type.362, f32[256]{0:T(256)S(1)} %rsqrt.36, bf16[4,64,4096]{2,1,0:T(8,128)(2,1)} %get-tuple-element.18), kind=kLoop, calls=%fused_computation.4 | loop fusion | flops 6291456 | bytes 4244480 | tf_op jit(solution)/shard_map/convert_element_type | solution.py:354
  41.6 1.1 fusion.36
  42.8 1.8 %fusion.13 = f32[256,256]{1,0:T(8,128)S(1)} fusion(f32[256,256]{1,0:T(8,128)} %fusion.36, bf16[2048,256]{1,0:T(8,128)(2,1)} %get-tuple-element.20, bf16[256,4096]{1,0:T(8,128)(2,1)S(1)} %fusion.3, s32[]{:T(128)S(6)} %select_n.65), kind=kOutput, calls=%fused_computation.27 | convolution fusion | flops 268632064 | bytes 2621444 | tf_op jit(solution)/shard_map/dot_general | solution.py:28
  45.5 1.0 copy-done.16
  50.2 0.8 pad_maximum_fusion.refs_0_
  54.6 11.6 %exchange_x_1.1 = (bf16[4,2,128,256]{3,2,1,0:T(8,128)(2,1)}, f32[4,8,256]{2,1,0:T(8,128)}, bf16[4,32,512]{2,1,0:T(8,128)(2,1)}) custom-call(bf16[4,2,128,256]{3,2,1,0:T(8,128)(2,1)} %pad_maximum_fusion.refs_0_, f32[4,8,256]{2,1,0:T(8,128)} %broadcast_in_dim.63.refs_1_, bf16[4,32,512]{2,1,0:T(8,128)(2,1)} %pad_maximum_fusion.2.refs_2_), custom_call_target="tpu_custom_call" | custom-call | tf_op jit(solution)/shard_map/exchange_x_1/pallas_call | solution.py:185
  67.1 0.8 fusion.180
  68.6 0.9 fusion.15
  69.9 1.0 fusion.14
  71.8 1.1 slice_convert_fusion.5
  74.3 18.5 %scan_z.1 = bf16[8,2,16,256]{3,2,1,0:T(8,128)(2,1)} custom-call(bf16[8,4,16,256]{3,2,1,0:T(8,128)(2,1)} %maximum_bitcast_fusion.group, f32[8,256]{1,0:T(8,128)} %concatenate.44.decays), custom_call_target="tpu_custom_call" | custom-call | tf_op jit(solution)/shard_map/scan_z/pallas_call | solution.py:227
  92.7 0.9 convert_bitcast_fusion
  94.0 0.9 pad_maximum_fusion.1.refs_0_
  94.9 8.6 %exchange_x_3.1 = bf16[4,2,128,256]{3,2,1,0:T(8,128)(2,1)} custom-call(bf16[4,2,128,256]{3,2,1,0:T(8,128)(2,1)} %pad_maximum_fusion.1.refs_0_), custom_call_target="tpu_custom_call" | custom-call | tf_op jit(solution)/shard_map/exchange_x_3/pallas_call | solution.py:185
  103.5 1.2 fusion.183
  109.8 0.8 multiply_convert_fusion
  111.4 1.7 %convolution_convert_fusion = bf16[256,2048]{1,0:T(8,128)(2,1)} fusion(bf16[256,512]{1,0:T(8,128)(2,1)S(1)} %multiply_convert_fusion, bf16[512,2048]{1,0:T(8,128)(2,1)S(1)} %copy-done.17), kind=kOutput, calls=%fused_computation.6 | convolution fusion | flops 537395200 | bytes 3407872 | tf_op jit(solution)/shard_map/dot_general | solution.py:28
  113.1 1.7 %convolution_convert_fusion.1 = bf16[256,2048]{1,0:T(8,128)(2,1)} fusion(bf16[256,512]{1,0:T(8,128)(2,1)S(1)} %multiply_convert_fusion, bf16[512,2048]{1,0:T(8,128)(2,1)S(1)} %copy-done.5), kind=kOutput, calls=%fused_computation.7 | convolution fusion | flops 537395200 | bytes 3407872 | tf_op jit(solution)/shard_map/dot_general | solution.py:28
  114.8 19.4 %reduce_y.1 = (f32[64,2048]{1,0:T(8,128)}, f32[64,2048]{1,0:T(8,128)}) custom-call(bf16[4,64,2048]{2,1,0:T(8,128)(2,1)} %bitcast.188, bf16[4,64,2048]{2,1,0:T(8,128)(2,1)} %bitcast.187), custom_call_target="tpu_custom_call" | custom-call | tf_op jit(solution)/shard_map/reduce_y/pallas_call | solution.py:269
  134.3 1.3 broadcast_select_fusion.1
  135.9 1.1 fusion.26
  (127 shorter events, 18.3 us)
Async XLA Ops:
  0.0 47.2 %copy-start = (bf16[4096,32]{0,1:T(8,128)(2,1)S(1)}, bf16[4096,32]{0,1:T(8,128)(2,1)}, u32[]{:S(2)}) copy-start(bf16[4096,32]{0,1:T(8,128)(2,1)} %param.31) | copy-start | bytes 786436
  35.5 3.6 %copy-start.23 = (bf16[4096]{0:T(1024)(128)(2,1)S(1)}, bf16[4096]{0:T(1024)(128)(2,1)}, u32[]{:S(2)}) copy-start(bf16[4096]{0:T(1024)(128)(2,1)} %param.25) | copy-start | bytes 24580
  39.1 2.5 %copy-start.1 = (bf16[2048,256]{1,0:T(8,128)(2,1)S(1)}, bf16[2048,256]{1,0:T(8,128)(2,1)}, u32[]{:S(2)}) copy-start(bf16[2048,256]{1,0:T(8,128)(2,1)} %wk.1) | copy-start | bytes 3145732
  42.8 2.0 %copy-start.4 = (bf16[2048,512]{1,0:T(8,128)(2,1)S(1)}, bf16[2048,512]{1,0:T(8,128)(2,1)}, u32[]{:S(2)}) copy-start(bf16[2048,512]{1,0:T(8,128)(2,1)} %wv.1) | copy-start | bytes 6291460
  44.8 5.1 %copy-start.2 = (f32[256,256]{1,0:T(8,128)}, f32[256,256]{1,0:T(8,128)S(1)}, u32[]{:S(2)}) copy-start(f32[256,256]{1,0:T(8,128)S(1)} %fusion.13) | copy-start | bytes 786436
  44.8 1.7 %copy-start.16 = (bf16[2048,512]{1,0:T(8,128)(2,1)S(1)}, bf16[2048,512]{1,0:T(8,128)(2,1)}, u32[]{:S(2)}) copy-start(bf16[2048,512]{1,0:T(8,128)(2,1)} %get-tuple-element.21) | copy-start | bytes 6291460
  47.2 2.7 %copy-start.12 = (bf16[256,512]{1,0:T(8,128)(2,1)}, bf16[256,512]{1,0:T(8,128)(2,1)S(1)}, u32[]{:S(2)}) copy-start(bf16[256,512]{1,0:T(8,128)(2,1)S(1)} %fusion.4) | copy-start | bytes 786436
  48.8 2.3 %copy-start.6 = (f32[256,256]{1,0:T(8,128)}, f32[256,256]{1,0:T(8,128)S(1)}, u32[]{:S(2)}) copy-start(f32[256,256]{1,0:T(8,128)S(1)} %fusion.47) | copy-start | bytes 786436
  49.0 2.8 %copy-start.20 = (bf16[1,32,4096]{2,1,0:T(8,128)(2,1)S(1)}, bf16[1,32,4096]{2,1,0:T(8,128)(2,1)}, u32[]{:S(2)}) copy-start(bf16[1,32,4096]{2,1,0:T(8,128)(2,1)} %param.21) | copy-start | bytes 786436
  49.6 2.9 %copy-start.8 = (f32[256,256]{1,0:T(8,128)}, f32[256,256]{1,0:T(8,128)S(1)}, u32[]{:S(2)}) copy-start(f32[256,256]{1,0:T(8,128)S(1)} %fusion.49) | copy-start | bytes 786436
  49.9 2.6 %copy-start.11 = (bf16[2048,256]{1,0:T(8,128)(2,1)S(1)}, bf16[2048,256]{1,0:T(8,128)(2,1)}, u32[]{:S(2)}) copy-start(bf16[2048,256]{1,0:T(8,128)(2,1)} %get-tuple-element.20) | copy-start | bytes 3145732
  66.3 6.8 %copy-start.21 = (bf16[4,32,512]{2,1,0:T(8,128)(2,1)S(1)}, bf16[4,32,512]{2,1,0:T(8,128)(2,1)}, u32[]{:S(2)}) copy-start(bf16[4,32,512]{2,1,0:T(8,128)(2,1)} %get-tuple-element.24) | copy-start | bytes 393220
  73.0 20.7 %copy-start.18 = (bf16[4,2,128,256]{3,2,1,0:T(8,128)(2,1)S(1)}, bf16[4,2,128,256]{3,2,1,0:T(8,128)(2,1)}, u32[]{:S(2)}) copy-start(bf16[4,2,128,256]{3,2,1,0:T(8,128)(2,1)} %get-tuple-element.23) | copy-start | bytes 1572868
  93.9 10.8 %copy-start.10 = (bf16[2048,256]{1,0:T(8,128)(2,1)S(1)}, bf16[2048,256]{1,0:T(8,128)(2,1)}, u32[]{:S(2)}) copy-start(bf16[2048,256]{1,0:T(8,128)(2,1)} %wq.1) | copy-start | bytes 3145732
  103.5 1.7 %copy-start.19 = (bf16[2048,256]{1,0:T(8,128)(2,1)S(1)}, bf16[2048,256]{1,0:T(8,128)(2,1)}, u32[]{:S(2)}) copy-start(bf16[2048,256]{1,0:T(8,128)(2,1)} %get-tuple-element.19) | copy-start | bytes 3145732
  104.7 1.1 copy-start.9
  105.6 1.4 %copy-start.13 = (bf16[256,512]{1,0:T(8,128)(2,1)S(1)}, bf16[256,512]{1,0:T(8,128)(2,1)}, u32[]{:S(2)}) copy-start(bf16[256,512]{1,0:T(8,128)(2,1)} %copy-done.12) | copy-start | bytes 786436
  107.1 1.6 %copy-start.14 = (bf16[2048,512]{1,0:T(8,128)(2,1)S(1)}, bf16[2048,512]{1,0:T(8,128)(2,1)}, u32[]{:S(2)}) copy-start(bf16[2048,512]{1,0:T(8,128)(2,1)} %wg.1) | copy-start | bytes 6291460
  108.1 1.3 copy-start.26
  108.1 1.7 %copy-start.27 = (bf16[2048,512]{1,0:T(8,128)(2,1)S(1)}, bf16[2048,512]{1,0:T(8,128)(2,1)}, u32[]{:S(2)}) copy-start(bf16[2048,512]{1,0:T(8,128)(2,1)} %get-tuple-element.25) | copy-start | bytes 6291460
  109.8 1.6 %copy-start.17 = (bf16[512,2048]{1,0:T(8,128)(2,1)S(1)}, bf16[512,2048]{1,0:T(8,128)(2,1)}, u32[]{:S(2)}) copy-start(bf16[512,2048]{1,0:T(8,128)(2,1)} %get-tuple-element.26) | copy-start | bytes 6291460
  110.7 2.5 %copy-start.5 = (bf16[512,2048]{1,0:T(8,128)(2,1)S(1)}, bf16[512,2048]{1,0:T(8,128)(2,1)}, u32[]{:S(2)}) copy-start(bf16[512,2048]{1,0:T(8,128)(2,1)} %wo.1) | copy-start | bytes 6291460
  134.3 1.6 %copy-start.24 = (bf16[4096]{0:T(1024)(128)(2,1)S(1)}, bf16[4096]{0:T(1024)(128)(2,1)}, u32[]{:S(2)}) copy-start(bf16[4096]{0:T(1024)(128)(2,1)} %param.26) | copy-start | bytes 24580
  134.3 1.6 %copy-start.15 = (bf16[1,64,4096]{2,1,0:T(8,128)(2,1)S(1)}, bf16[1,64,4096]{2,1,0:T(8,128)(2,1)}, u32[]{:S(2)}) copy-start(bf16[1,64,4096]{2,1,0:T(8,128)(2,1)} %param.18) | copy-start | bytes 1572868
  (4 other events, 3.5 us)

commit v2 on v1

v2 whole, which is shorter than its diff:
```python
import jax
import jax.numpy as jnp
from jax import lax
from jax.experimental import pallas as pl
from jax.experimental.pallas import tpu as pltpu
from jax.sharding import Mesh
from jax.sharding import PartitionSpec as P

DK_HEAD = 256
DV_HEAD = 512
RANK = 16
BLOCK = 128
SP_TP = ("sp_0", "sp_1", "tp")
SP = ("sp_0", "sp_1")
NZ, NX, NY = 8, 4, 4
WIDTH = 4096
HALF = 2048
ANY = pl.BlockSpec(memory_space=pl.ANY)
VM = pl.BlockSpec(memory_space=pltpu.VMEM)
BF, F32 = jnp.bfloat16, jnp.float32


EPS = 1e-06
TAU = 16.0


def matmul(left, right):
    return jnp.dot(left, right, preferred_element_type=jnp.float32)


def rms_scale(vectors, gain):
    return vectors * lax.rsqrt(jnp.mean(vectors * vectors, axis=-1, keepdims=True) + EPS) * gain


def shape_of(*dims, dtype=BF):
    return jax.ShapeDtypeStruct(dims, dtype)


def send(src, dst, send_sem, recv_sem, **where):
    copy = pltpu.make_async_remote_copy(
        src_ref=src,
        dst_ref=dst,
        send_sem=send_sem,
        recv_sem=recv_sem,
        device_id=where,
        device_id_type=pl.DeviceIdType.MESH,
    )
    copy.start()
    return copy


def greet(partners):
    barrier = pltpu.get_barrier_semaphore()
    for where in partners:
        pl.semaphore_signal(
            barrier, inc=1, device_id=where, device_id_type=pl.DeviceIdType.MESH
        )
    return lambda: pl.semaphore_wait(barrier, len(partners))


def position():
    return tuple(lax.axis_index(a) for a in ("sp_0", "sp_1", "tp", "dp"))


def gather_kernel(
    lat, context, cond, cond_ctx, gain_pre, w_shift, w_scale, w_gate, wq, wk, wv, wg, wo,
    mods, rows, wq2, wk2, wv2, wg2, wo2,
    w_mod, lat_all, partial, arrived, tile,
    load_sem, s1, r1, s2, r2, sl, rl, sw, rw,
):
    z, x, y, c = position()
    at_sp = [
        (k, dict(sp_0=lax.rem(z + k // NX, NZ), sp_1=lax.rem(x + k % NX, NX)))
        for k in range(1, NZ * NX)
    ]
    at_yz = [
        (k, dict(sp_0=lax.rem(z + k // NY, NZ), tp=lax.rem(y + k % NY, NY)))
        for k in range(1, NZ * NY)
    ]
    other = dict(dp=1 - c)
    above, below, facing = (lax.rem(y + k, NY) for k in (1, 3, 2))
    up, down = dict(tp=above), dict(tp=below)
    entered = greet(
        [w for _, w in at_sp] + [w for k, w in at_yz if k % NY != 0] + [other]
    )
    loads = [
        pltpu.make_async_copy(src, dst, load_sem.at[k])
        for k, (src, dst) in enumerate(
            [(w_shift, w_mod.at[0]), (w_scale, w_mod.at[1]), (w_gate, w_mod.at[2]),
             (lat, lat_all.at[y])]
        )
    ]
    for load in loads:
        load.start()
    line = lax.broadcasted_iota(jnp.int32, (16, 128), 0)
    act = jax.nn.silu(cond[...].astype(F32)).astype(BF).astype(F32)
    act_ctx = jax.nn.silu(cond_ctx[...].astype(F32)).astype(BF).astype(F32)
    total = None
    for k in range(3):
        left = jnp.where(line == k, act, jnp.where(line == k + 3, act_ctx, 0.0)).astype(BF)
        loads[k].wait()
        part = matmul(left, w_mod[k])
        total = part if total is None else total + part
    for k in range(NZ):
        partial[k] = total[:8, k * 128 : (k + 1) * 128]
    loads[3].wait()
    entered()
    sends = [
        send(partial.at[w["sp_0"]], arrived.at[k], s1.at[k], r1.at[k], **w) for k, w in at_sp
    ]
    own = lat_all.at[y]
    to_up = send(own, own, sl.at[0], rl.at[0], **up)
    to_down = send(own, own, sl.at[1], rl.at[1], **down)
    weights = [
        send(src, dst, sw.at[k], rw.at[k], **other)
        for k, (src, dst) in enumerate(
            [(wk, wk2), (wv, wv2), (wq, wq2), (wg, wg2), (wo, wo2)]
        )
    ]
    for copy in sends:
        copy.wait()
    summed = partial[z]
    for k in range(1, NZ * NX):
        summed = summed + arrived[k]
    tile[...] = summed
    here = mods.at[:, pl.ds(pl.multiple_of((y * NZ + z) * 128, 128), 128)]
    here[...] = summed
    sends = [send(tile, here, s2.at[k], r2.at[k], **w) for k, w in at_yz]
    to_up.wait()
    before = lat_all.at[below, pl.ds(0, 32)]
    relay_up = send(before, before, sl.at[2], rl.at[2], **up)
    to_down.wait()
    after = lat_all.at[above, pl.ds(32, 32)]
    relay_down = send(after, after, sl.at[3], rl.at[3], **down)
    for copy in sends:
        copy.wait()
    columns = [pl.ds(pl.multiple_of(k * HALF, HALF), HALF) for k in (c, 1 - c)]

    def modulate(source, target, scale_row, shift_row, length):
        def step(k, carry):
            at = pl.ds(pl.multiple_of(k * 16, 16), 16)
            to = pl.ds(pl.multiple_of(target + k * 16, 16), 16)
            halves = [source[at, columns[h]].astype(F32) for h in range(2)]
            square = sum(jnp.sum(v * v, axis=1, keepdims=True) for v in halves)
            norm = lax.rsqrt(square / WIDTH + EPS)
            for h in range(2):
                weight = gain_pre[:, columns[h]].astype(F32) * (
                    1.0 + mods[scale_row : scale_row + 1, columns[h]]
                )
                shift = mods[shift_row : shift_row + 1, columns[h]]
                rows[h, to] = (halves[h] * norm * weight + shift).astype(BF)
            return carry

        lax.fori_loop(0, length // 16, step, 0)

    modulate(context, NY * 64, 4, 3, 32)
    for block in (y, below, above):
        modulate(lat_all.at[block], block * 64, 1, 0, 64)
    relay_up.wait()
    relay_down.wait()
    modulate(lat_all.at[facing], facing * 64, 1, 0, 64)
    for copy in weights:
        copy.wait()


def gather_inputs(lat, context, cond, cond_ctx, gain, w_shift, w_scale, w_gate, *weights):
    dma = pltpu.SemaphoreType.DMA
    return pl.pallas_call(
        gather_kernel,
        out_shape=[shape_of(8, WIDTH, dtype=F32), shape_of(2, NY * 64 + 32, HALF)]
        + [shape_of(*w.shape) for w in weights],
        in_specs=[ANY, VM, VM, VM, VM] + [ANY] * 8,
        out_specs=[VM, VM] + [ANY] * 5,
        scratch_shapes=[
            pltpu.VMEM((3, 128, 1024), BF),
            pltpu.VMEM((NY, *lat.shape), BF),
            pltpu.VMEM((NZ, 8, 128), F32),
            pltpu.VMEM((NZ * NX, 8, 128), F32),
            pltpu.VMEM((8, 128), F32),
            dma((4,)), dma((32,)), dma((32,)), dma((32,)), dma((32,)),
            dma((4,)), dma((4,)), dma((5,)), dma((5,)),
        ],
        compiler_params=pltpu.CompilerParams(collective_id=0, has_side_effects=True),
        name="gather_inputs",
    )(lat, context, cond, cond_ctx, gain, w_shift, w_scale, w_gate, *weights)


def log_sigmoid(v):
    return jnp.minimum(v, 0.0) - jnp.log1p(jnp.exp(-jnp.abs(v)))


def log_decays(lowrank, decay_up, decay_bias):
    return [
        log_sigmoid(
            matmul(lowrank[:, way * RANK : (way + 1) * RANK], decay_up[way])
            + decay_bias[way : way + 1]
        )
        / TAU
        for way in range(2)
    ]


def triangle(n, lower):
    r = lax.broadcasted_iota(jnp.int32, (n, n), 0)
    c = lax.broadcasted_iota(jnp.int32, (n, n), 1)
    return r >= c if lower else r <= c


def running_sum(decay, lower):
    ones = jnp.where(triangle(decay.shape[0], lower), 1.0, 0.0).astype(BF)
    high = decay.astype(BF)
    rest = decay - high.astype(F32)
    middle = rest.astype(BF)
    low = (rest - middle.astype(F32)).astype(BF)
    return matmul(ones, high) + matmul(ones, middle) + matmul(ones, low)


def across(left, right):
    return lax.dot_general(left, right, (((1,), (1,)), ((), ())), preferred_element_type=F32)


def outer(left, right):
    return lax.dot_general(left, right, (((0,), (0,)), ((), ())), preferred_element_type=F32)


def scores_of(q, k, fwd, bwd, store):
    lower, upper = triangle(BLOCK, True), triangle(BLOCK, False)
    bf = lambda a: a.astype(BF)
    for b in range(2):
        sl = slice(b * BLOCK, (b + 1) * BLOCK)
        osl = slice((1 - b) * BLOCK, (2 - b) * BLOCK)
        f, g = fwd[sl], bwd[sl]
        cf, cg = f[BLOCK // 2 : BLOCK // 2 + 1], g[BLOCK // 2 - 1 : BLOCK // 2]
        sf = across(bf(q[sl] * jnp.exp(f - cf)), bf(k[sl] * jnp.exp(cf - f)))
        sb = across(bf(q[sl] * jnp.exp(g - cg)), bf(k[sl] * jnp.exp(cg - g)))
        store[sl, sl] = bf(jnp.where(lower, sf, 0.0) + jnp.where(upper, sb, 0.0))
        if b == 0:
            mine, other, edge = g, bwd[osl], bwd[BLOCK : BLOCK + 1]
        else:
            mine, other, edge = f, fwd[osl], fwd[BLOCK - 1 : BLOCK]
        store[sl, osl] = bf(across(bf(q[sl] * jnp.exp(mine - edge)), bf(k[osl] * jnp.exp(edge - other))))


def mixer_kernel(
    queries, keys_in, values, out_gate, lowrank, ctx_keys, ctx_values, ctx_lowrank,
    decay_up, decay_bias, head_gain, w_here, w_there, latents, mods, gain_post,
    result,
    w_out, pack, packs, states, got_states, decays, got_decays, scores, local, entering,
    group, groups, group_decays, all_decays, back, entry, before, leaving, entries, heads,
    part_a, part_b, near_a, near_b, far_a, far_b, sum_a, sum_b, relay_a, relay_b,
    s_load, s_x, r_x, s_z, r_z, s_e, r_e, s_y, r_y,
):
    z, x, y, c = position()
    x_peers = [(d, lax.rem(x + d, NX)) for d in (1, 3, 2)]
    z_peers = [(d, lax.rem(z + d, NZ)) for d in (4, 3, 5, 2, 6, 1, 7)]
    above, below, facing = (lax.rem(y + k, NY) for k in (1, 3, 2))
    up, down = dict(tp=above), dict(tp=below)
    entered = greet([dict(sp_1=p) for _, p in x_peers] + [dict(sp_0=p) for _, p in z_peers] + [up, down])
    loads = [
        pltpu.make_async_copy(src, w_out.at[k], s_load.at[k]) for k, src in enumerate((w_here, w_there))
    ]
    for load in loads:
        load.start()
    for j in range(NX):
        pack[j] = jnp.zeros((32, 512), BF)
        pack[j, :, :DK_HEAD] = ctx_keys[...]
        pack[j, :, DK_HEAD : DK_HEAD + 128] = ctx_values[:, j * 128 : (j + 1) * 128]
        pack[j, :, DK_HEAD + 128 : DK_HEAD + 128 + 2 * RANK] = ctx_lowrank[...]
    decay_f, decay_b = log_decays(lowrank[...], decay_up[...], decay_bias[...])
    fwd, bwd = running_sum(decay_f, True), running_sum(decay_b, False)
    decays[0:1] = fwd[-1:]
    decays[1:2] = bwd[:1]
    decays[2:8] = jnp.zeros((6, DK_HEAD), F32)
    k = keys_in[...].astype(F32)
    for way, scaled in enumerate((jnp.exp(fwd[-1:] - fwd), jnp.exp(bwd[:1] - bwd))):
        state = outer(values[...], (k * scaled).astype(BF)).astype(BF)
        for j in range(NX):
            states[j, way] = state[j * 128 : (j + 1) * 128]
    entered()
    x_copies = []
    for n, (a, b) in enumerate([(pack, packs), (states, got_states)]):
        for d, p in x_peers:
            x_copies.append(send(a.at[p], b.at[x], s_x.at[n, d], r_x.at[n, d], sp_1=p))
    for d, p in x_peers:
        x_copies.append(send(decays, got_decays.at[x], s_x.at[2, d], r_x.at[2, d], sp_1=p))
    packs[x] = pack[x]
    got_states[x] = states[x]
    got_decays[x] = decays[...]
    q = queries[...].astype(F32) * DK_HEAD ** (-0.5)
    scores_of(q, k, fwd, bwd, scores)
    local[...] = matmul(scores[...], values[...])
    entering[0] = (q * jnp.exp(fwd)).astype(BF)
    entering[1] = (q * jnp.exp(bwd)).astype(BF)
    for copy in x_copies[:3]:
        copy.wait()
    ctx = packs[...].reshape(NX * 32, 512)
    ctx_k = ctx[:, :DK_HEAD].astype(F32)
    ctx_v = ctx[:, DK_HEAD : DK_HEAD + 128]
    ctx_lr = ctx[:, DK_HEAD + 128 : DK_HEAD + 128 + 2 * RANK]
    cdf, cdb = log_decays(ctx_lr, decay_up[...], decay_bias[...])
    cf, cb = running_sum(cdf, True), running_sum(cdb, False)
    for way, scaled in enumerate((jnp.exp(cf[-1:] - cf), jnp.exp(cb[:1] - cb))):
        state = outer(ctx_v, (ctx_k * scaled).astype(BF)).astype(BF)
        for j in range(NZ):
            group[j, 2 + way] = state[j * 16 : (j + 1) * 16]
    group_decays[2:3] = cf[-1:]
    group_decays[3:4] = cb[:1]
    group_decays[4:8] = jnp.zeros((4, DK_HEAD), F32)
    for copy in x_copies[3:]:
        copy.wait()
    ways = (tuple(range(NX)), tuple(reversed(range(NX))))
    for way in range(2):
        state, total = None, None
        for j in ways[way]:
            step, piece = got_decays[j, way : way + 1], got_states[j, way].astype(F32)
            state = piece if state is None else state * jnp.exp(step) + piece
            total = step if total is None else total + step
        state = state.astype(BF)
        for j in range(NZ):
            group[j, way] = state[j * 16 : (j + 1) * 16]
        group_decays[way : way + 1] = total
    z_copies = []
    for d, p in z_peers:
        z_copies.append(send(group.at[p], groups.at[z], s_z.at[0, d], r_z.at[0, d], sp_0=p))
        z_copies.append(send(group_decays, all_decays.at[z], s_z.at[1, d], r_z.at[1, d], sp_0=p))
    groups[z] = group[z]
    all_decays[z] = group_decays[...]
    for way in range(2):
        state = jnp.zeros((128, DK_HEAD), F32)
        for j in ways[way]:
            before[j, way] = state
            state = state * jnp.exp(got_decays[j, way : way + 1]) + got_states[j, way].astype(F32)
    for copy in z_copies:
        copy.wait()
    orders = (tuple(range(NZ)), tuple(reversed(range(NZ))))
    for way in range(2):
        state = jnp.zeros((16, DK_HEAD), F32)
        for j in orders[way]:
            state = state * jnp.exp(all_decays[j, 2 + way : 3 + way]) + groups[j, 2 + way].astype(F32)
        for j in orders[way]:
            back[j, way] = state.astype(BF)
            state = state * jnp.exp(all_decays[j, way : way + 1]) + groups[j, way].astype(F32)
    z_copies = [send(back.at[p], entry.at[z], s_z.at[2, d], r_z.at[2, d], sp_0=p) for d, p in z_peers]
    entry[z] = back[z]
    for copy in z_copies:
        copy.wait()
    for way in range(2):
        start = jnp.concatenate([entry[j, way] for j in range(NZ)], axis=0).astype(F32)
        passed = jnp.zeros((1, DK_HEAD), F32)
        for j in ways[way]:
            leaving[j, way] = (start * jnp.exp(passed) + before[j, way]).astype(BF)
            passed = passed + got_decays[j, way : way + 1]
    e_copies = [send(leaving.at[p], entries.at[x], s_e.at[d], r_e.at[d], sp_1=p) for d, p in x_peers]
    entries[x] = leaving[x]
    gate = jax.nn.silu(out_gate[...].astype(F32)) * head_gain[...].astype(F32)
    for load in loads:
        load.wait()
    for copy in e_copies:
        copy.wait()
    out = [
        local[:, j * 128 : (j + 1) * 128]
        + across(entering[0], entries[j, 0])
        + across(entering[1], entries[j, 1])
        for j in range(NX)
    ]
    square = sum(jnp.sum(o * o, axis=1, keepdims=True) for o in out)
    scale = lax.rsqrt(square / DV_HEAD + EPS)
    for j in range(NX):
        heads[:, j * 128 : (j + 1) * 128] = (out[j] * scale * gate[:, j * 128 : (j + 1) * 128]).astype(BF)
    count = latents.shape[0]

    def project(owner):
        rows = heads[pl.ds(pl.multiple_of(owner * count, count), count)]
        part_a[owner] = matmul(rows, w_out[0]).astype(BF)
        part_b[owner] = matmul(rows, w_out[1]).astype(BF)

    project(facing)
    first_a = send(part_a.at[facing], relay_a, s_y.at[0], r_y.at[0], **down)
    first_b = send(part_b.at[facing], relay_b, s_y.at[1], r_y.at[1], **up)
    project(below)
    direct_b = send(part_b.at[below], near_b, s_y.at[2], r_y.at[2], **down)
    project(above)
    direct_a = send(part_a.at[above], near_a, s_y.at[3], r_y.at[3], **up)
    first_a.wait()
    sum_a[...] = (relay_a[...].astype(F32) + part_a[below].astype(F32)).astype(BF)
    second_a = send(sum_a, far_a, s_y.at[4], r_y.at[4], **down)
    first_b.wait()
    sum_b[...] = (relay_b[...].astype(F32) + part_b[above].astype(F32)).astype(BF)
    second_b = send(sum_b, far_b, s_y.at[5], r_y.at[5], **up)
    project(y)
    direct_a.wait()
    direct_b.wait()
    second_a.wait()
    second_b.wait()
    here, there = (
        pl.ds(pl.multiple_of(k * HALF, HALF), HALF) for k in (c, 1 - c)
    )

    def finish(k, carry):
        rows = pl.ds(pl.multiple_of(k * 16, 16), 16)
        a = part_a[y, rows].astype(F32) + near_a[rows].astype(F32) + far_a[rows].astype(F32)
        b = part_b[y, rows].astype(F32) + near_b[rows].astype(F32) + far_b[rows].astype(F32)
        square = jnp.sum(a * a, axis=1, keepdims=True) + jnp.sum(b * b, axis=1, keepdims=True)
        scale = lax.rsqrt(square / WIDTH + EPS)
        for columns, half in ((here, a), (there, b)):
            weight = mods[2:3, columns] * gain_post[:, columns].astype(F32)
            result[rows, columns] = (
                latents[rows, columns].astype(F32) + half * scale * weight
            ).astype(BF)
        return carry

    lax.fori_loop(0, count // 16, finish, 0)


def mixer(*args):
    dma = pltpu.SemaphoreType.DMA
    vm = pltpu.VMEM
    half = vm((64, HALF), BF)
    in_specs = [VM] * len(args)
    in_specs[11] = in_specs[12] = ANY
    return pl.pallas_call(
        mixer_kernel,
        out_shape=shape_of(64, WIDTH),
        in_specs=in_specs,
        out_specs=VM,
        scratch_shapes=[
            vm((2, DV_HEAD, HALF), BF),
            vm((NX, 32, 512), BF), vm((NX, 32, 512), BF),
            vm((NX, 2, 128, DK_HEAD), BF), vm((NX, 2, 128, DK_HEAD), BF),
            vm((8, DK_HEAD), F32), vm((NX, 8, DK_HEAD), F32),
            vm((256, 256), BF), vm((256, DV_HEAD), F32), vm((2, 256, DK_HEAD), BF),
            vm((NZ, 4, 16, DK_HEAD), BF), vm((NZ, 4, 16, DK_HEAD), BF),
            vm((8, DK_HEAD), F32), vm((NZ, 8, DK_HEAD), F32),
            vm((NZ, 2, 16, DK_HEAD), BF), vm((NZ, 2, 16, DK_HEAD), BF),
            vm((NX, 2, 128, DK_HEAD), F32),
            vm((NX, 2, 128, DK_HEAD), BF), vm((NX, 2, 128, DK_HEAD), BF),
            vm((256, DV_HEAD), BF),
            vm((NY, 64, HALF), BF), vm((NY, 64, HALF), BF),
            half, half, half, half, half, half, half, half,
            dma((2,)), dma((3, NX)), dma((3, NX)), dma((3, NZ)), dma((3, NZ)),
            dma((NX,)), dma((NX,)), dma((6,)), dma((6,)),
        ],
        compiler_params=pltpu.CompilerParams(
            collective_id=1, has_side_effects=True, vmem_limit_bytes=56 * 2**20
        ),
        name="mixer",
    )(*args)


def body(
    latents, cond, cond_ctx, context, w_shift, w_scale, w_gate, gain_pre, gain_post,
    w_query, w_key, w_value, w_outgate, w_down, decay_up, decay_bias, head_gain, w_out,
):
    latents, context = latents[0], context[0]
    mods, rows, wq2, wk2, wv2, wg2, wo2 = gather_inputs(
        latents, context, cond, cond_ctx[None], gain_pre[None], w_shift, w_scale, w_gate,
        w_query, w_key, w_value, w_outgate, w_out,
    )
    count = NY * latents.shape[0]

    def project(here, there, rows=rows):
        return (matmul(rows[0], here) + matmul(rows[1], there)).astype(BF)

    c = lax.axis_index("dp")
    keys_in = project(w_key, wk2)
    values = project(w_value, wv2)
    down = [lax.dynamic_slice_in_dim(w_down, k * HALF, HALF, 0) for k in (c, 1 - c)]
    lowrank = project(*down)
    main = rows[:, :count]
    queries = project(w_query, wq2, main)
    out_gate = project(w_outgate, wg2, main)
    result = mixer(
        queries, keys_in[:count], values[:count], out_gate, lowrank[:count],
        keys_in[count:], values[count:], lowrank[count:],
        decay_up, decay_bias, head_gain[None], w_out, wo2, latents, mods, gain_post[None],
    )
    return result[None]


def solution(mesh):
    finer = Mesh(
        mesh.devices.reshape(8, 4, mesh.shape["tp"], mesh.shape["dp"]), ("sp_0", "sp_1", "tp", "dp")
    )
    in_specs = (
        P("dp", SP_TP, None),
        P("dp", SP),
        P(SP),
        P("dp", SP, None),
        P(SP, "tp"),
        P(SP, "tp"),
        P(SP, "tp"),
        P(),
        P(),
        P("dp", "tp"),
        P("dp", "tp"),
        P("dp", "tp"),
        P("dp", "tp"),
        P(),
        P(None, None, "tp"),
        P(None, "tp"),
        P("tp"),
        P("tp", "dp"),
    )
    out_specs = P("dp", SP_TP, None)
    return jax.shard_map(body, mesh=finer, in_specs=in_specs, out_specs=out_specs, check_vma=False)
```

time: 138 us -> 110 us (0.80)
  other arithmetic: 16.9 us -> 0 us
  Pallas kernels: 93.6 us -> 84.9 us
  matrix products: 19.6 us -> 12.7 us
  local copies, waits for them, and re-layouts: 6 us -> 12.1 us
    pallas_call x5 -> x2, Pallas kernels: 93.6 us -> 84.9 us  [the longest x1 49.7 us: mixer(): pl.pallas_call(mixer_kernel, out_shape=shape_of(64, WIDTH), in_specs=in_s...]
    convert_element_type x8 -> x0, other arithmetic: 5.81 us -> none  [the longest x1 2.51 us: body(): (rms_scale(rows, gain_in) * (1.0 + scale_vec) + shift_vec).astype(BF)]
    dot_general x16 -> x0, matrix products: 4.51 us -> none  [the longest x8 1.8 us: across(): lax.dot_general(left, right, (((1,), (1,)), ((), ())), preferred_element_...]
    broadcast_in_dim x5 -> x3, local copies, waits for them, and re-layouts: 0.64 us -> 3.87 us  [the longest x1 1.31 us: body(): gain_pre[None]]
    reduce_sum x3 -> x0, other arithmetic: 2.44 us -> none  [rms_scale(): jnp.mean(vectors * vectors, axis=-1, keepdims=True) + EPS]
    dot_general x21 -> x10, matrix products: 15.1 us -> 12.7 us  [matmul(): return jnp.dot(left, right, preferred_element_type=jnp.float32)]
    exp x3 -> x0, other arithmetic: 2.32 us -> none  [the longest x2 1.59 us: body(): jnp.exp(passed_f[j])]
    unnamed x56 -> x23, local copies, waits for them, and re-layouts: 3.36 us -> 5.64 us
where the time goes in v2:
time: 110 us
  Pallas kernels  84.9 us (77%)
  matrix products  12.7 us (12%)
  local copies, waits for them, and re-layouts  12.1 us (11%)
    pallas_call x1, Pallas kernels, mixer(): pl.pallas_call(mixer_kernel, out_shape=shape_of(64, WIDTH), in_specs=in_s...  49.7 us
    pallas_call x1, Pallas kernels, gather_inputs(): pl.pallas_call(gather_kernel, out_shape=[shape_of(8, WIDTH, dtype=F32), s...  35.2 us
    dot_general x10, matrix products, matmul(): return jnp.dot(left, right, preferred_element_type=jnp.float32)  12.7 us
    unnamed x23, local copies, waits for them, and re-layouts  5.64 us

profile of v2, /device:TPU:2, one launch (start us, length us, event | category | flops | bytes accessed | tf_op | source)
XLA Modules:
  0.0 109.9 jit_solution(3651482399949755926)
XLA Ops:
  0.0 1.3 %broadcast_in_dim.17.head_gain = bf16[1,512]{1,0:T(2,128)(2,1)} reshape(bf16[512]{0:T(512)(128)(2,1)} %param.34) | data formatting | bytes 2048 | tf_op jit(solution)/shard_map/broadcast_in_dim | solution.py:475
  1.3 1.3 %broadcast_in_dim.16.gain_pre = bf16[1,4096]{1,0:T(2,128)(2,1)} reshape(bf16[4096]{0:T(1024)(128)(2,1)} %param.25) | data formatting | bytes 16384 | tf_op jit(solution)/shard_map/broadcast_in_dim | solution.py:456
  2.6 1.3 %broadcast_in_dim.18.gain_post = bf16[1,4096]{1,0:T(2,128)(2,1)} reshape(bf16[4096]{0:T(1024)(128)(2,1)} %param.26) | data formatting | bytes 16384 | tf_op jit(solution)/shard_map/broadcast_in_dim | solution.py:475
  3.9 35.2 %gather_inputs.1 = (f32[8,4096]{1,0:T(8,128)}, bf16[2,288,2048]{2,1,0:T(8,128)(2,1)}, bf16[2048,256]{1,0:T(8,128)(2,1)}, bf16[2048,256]{1,0:T(8,128)(2,1)}, bf16...) custom-call(bf16[64,4096]{1,0:T(8,128)(2,1)} %bitcast.42, bf16[32,4096]{1,0:T(8,128)(2,1)} %bitcast.45, ...), custom_call_target="tpu_custom_call" | custom-call | tf_op jit(solution)/shard_map/gather_inputs/pallas_call | solution.py:168
  39.1 1.7 %fusion.2 = f32[288,32]{0,1:T(8,128)S(1)} fusion(bf16[2,288,2048]{2,1,0:T(8,128)(2,1)} %get-tuple-element.12, bf16[4096,32]{0,1:T(8,128)(2,1)S(1)} %copy-done, s32[]{:T(128)S(6)} %select_n.7), kind=kOutput, calls=%fused_computation.4 | convolution fusion | flops 37748736 | bytes 1347588 | tf_op jit(solution)/shard_map/dot_general | solution.py:28
  40.9 2.2 %fusion.5 = f32[288,256]{1,0:T(8,128)S(1)} fusion(bf16[2048,256]{1,0:T(8,128)(2,1)} %get-tuple-element.14, bf16[2,288,2048]{2,1,0:T(8,128)(2,1)} %get-tuple-element.12), kind=kOutput, calls=%fused_computation.7 | convolution fusion | flops 301989888 | bytes 2523136 | tf_op jit(solution)/shard_map/dot_general | solution.py:28
  43.6 0.5 fusion.16
  44.1 0.5 fusion.20
  44.6 0.7 copy.23.ctx_lowrank
  45.3 0.6 slice.52.ctx_keys
  45.9 0.6 slice.49.keys_in
  46.5 0.7 copy.22.lowrank
  47.2 1.8 %fusion.27 = f32[256,256]{1,0:T(8,128)S(1)} fusion(bf16[2048,256]{1,0:T(8,128)(2,1)S(1)} %copy-done.4, bf16[2,288,2048]{2,1,0:T(8,128)(2,1)} %get-tuple-element.12), kind=kOutput, calls=%fused_computation.24 | convolution fusion | flops 268435456 | bytes 2359296 | tf_op jit(solution)/shard_map/dot_general | solution.py:28
  49.1 2.3 %fusion.19.queries = bf16[256,256]{1,0:T(8,128)(2,1)} fusion(f32[256,256]{1,0:T(8,128)S(1)} %fusion.27, bf16[2048,256]{1,0:T(8,128)(2,1)S(1)} %copy-done.9, bf16[2,288,2048]{2,1,0:T(8,128)(2,1)} %get-tuple-element.12), kind=kOutput, calls=%fused_computation.18 | convolution fusion | flops 268566528 | bytes 2490368 | tf_op jit(solution)/shard_map/dot_general | solution.py:28
  51.4 0.7 fusion.25
  52.1 0.9 copy-done.8
  53.0 1.4 %fusion.1.out_gate = bf16[256,512]{1,0:T(8,128)(2,1)} fusion(f32[256,512]{1,0:T(8,128)S(1)} %fusion.25, bf16[2048,512]{1,0:T(8,128)(2,1)S(1)} %copy-done.8, bf16[2,288,2048]{2,1,0:T(8,128)(2,1)S(1)} %copy-done.6), kind=kOutput, calls=%fused_computation.3 | convolution fusion | flops 537133056 | bytes 3932160 | tf_op jit(solution)/shard_map/dot_general | solution.py:28
  54.6 0.8 fusion.9
  55.4 0.8 copy-done.7
  56.2 0.8 fusion
  57.0 0.6 slice.53.ctx_values
  57.6 0.7 slice.50.values
  58.3 49.7 %mixer.1 = bf16[64,4096]{1,0:T(8,128)(2,1)} custom-call(bf16[256,256]{1,0:T(8,128)(2,1)} %fusion.19.queries, bf16[256,256]{1,0:T(8,128)(2,1)} %slice.49.keys_in, bf16[256,512]{1,0:T(8,128)(2,1)} %slice.50.values, bf16[256,512]{1,0:T(8,128)(2,1)} %fusion.1.out_gate, bf16[256,32]{1,0:T(8,128)(2,1)} %copy.22.lowrank, bf16[32,256]{1,0:T(8,128)(2,1)} %slice.52.ctx_keys, ...), custom_call_target="tpu_custom_call" | custom-call | tf_op jit(solution)/shard_map/mixer/pallas_call | solution.py:421
  108.0 1.9 %copy.25 = bf16[1,64,4096]{2,1,0:T(8,128)(2,1)} copy(bf16[1,64,4096]{2,1,0:T(8,128)(2,1)} %bitcast.44) | data formatting | bytes 1048576
  (20 shorter events, 0.7 us)
Async XLA Ops:
  0.0 39.1 %copy-start = (bf16[4096,32]{0,1:T(8,128)(2,1)S(1)}, bf16[4096,32]{0,1:T(8,128)(2,1)}, u32[]{:S(2)}) copy-start(bf16[4096,32]{0,1:T(8,128)(2,1)} %param.31) | copy-start | bytes 786436
  40.9 2.3 %copy-start.3 = (bf16[2048,256]{1,0:T(8,128)(2,1)S(1)}, bf16[2048,256]{1,0:T(8,128)(2,1)}, u32[]{:S(2)}) copy-start(bf16[2048,256]{1,0:T(8,128)(2,1)} %wk.1) | copy-start | bytes 3145732
  40.9 2.7 %copy-start.5 = (bf16[2,288,2048]{2,1,0:T(8,128)(2,1)S(1)}, bf16[2,288,2048]{2,1,0:T(8,128)(2,1)}, u32[]{:S(2)}) copy-start(bf16[2,288,2048]{2,1,0:T(8,128)(2,1)} %get-tuple-element.12) | copy-start | bytes 7077892
  43.6 3.7 %copy-start.4 = (bf16[2048,256]{1,0:T(8,128)(2,1)S(1)}, bf16[2048,256]{1,0:T(8,128)(2,1)}, u32[]{:S(2)}) copy-start(bf16[2048,256]{1,0:T(8,128)(2,1)} %wq.1) | copy-start | bytes 3145732
  44.1 5.0 %copy-start.9 = (bf16[2048,256]{1,0:T(8,128)(2,1)S(1)}, bf16[2048,256]{1,0:T(8,128)(2,1)}, u32[]{:S(2)}) copy-start(bf16[2048,256]{1,0:T(8,128)(2,1)} %get-tuple-element.13) | copy-start | bytes 3145732
  47.2 4.2 %copy-start.1 = (bf16[2048,512]{1,0:T(8,128)(2,1)S(1)}, bf16[2048,512]{1,0:T(8,128)(2,1)}, u32[]{:S(2)}) copy-start(bf16[2048,512]{1,0:T(8,128)(2,1)} %wg.1) | copy-start | bytes 6291460
  47.2 4.2 %copy-start.6 = (bf16[2,288,2048]{2,1,0:T(8,128)(2,1)S(1)}, bf16[2,288,2048]{2,1,0:T(8,128)(2,1)}, u32[]{:S(2)}) copy-start(bf16[2,288,2048]{2,1,0:T(8,128)(2,1)} %get-tuple-element.12) | copy-start | bytes 7077892
  51.4 1.6 %copy-start.8 = (bf16[2048,512]{1,0:T(8,128)(2,1)S(1)}, bf16[2048,512]{1,0:T(8,128)(2,1)}, u32[]{:S(2)}) copy-start(bf16[2048,512]{1,0:T(8,128)(2,1)} %get-tuple-element.16) | copy-start | bytes 6291460
  53.0 1.6 %copy-start.2 = (bf16[2048,512]{1,0:T(8,128)(2,1)S(1)}, bf16[2048,512]{1,0:T(8,128)(2,1)}, u32[]{:S(2)}) copy-start(bf16[2048,512]{1,0:T(8,128)(2,1)} %wv.1) | copy-start | bytes 6291460
  54.6 1.6 %copy-start.7 = (bf16[2048,512]{1,0:T(8,128)(2,1)S(1)}, bf16[2048,512]{1,0:T(8,128)(2,1)}, u32[]{:S(2)}) copy-start(bf16[2048,512]{1,0:T(8,128)(2,1)} %get-tuple-element.15) | copy-start | bytes 6291460

commit v3 on v2

v3 whole, which is shorter than its diff:
```python
import jax
import jax.numpy as jnp
from jax import lax
from jax.experimental import pallas as pl
from jax.experimental.pallas import tpu as pltpu
from jax.sharding import Mesh
from jax.sharding import PartitionSpec as P

DK_HEAD = 256
DV_HEAD = 512
RANK = 16
BLOCK = 128
SP_TP = ("sp_0", "sp_1", "tp")
SP = ("sp_0", "sp_1")
NZ, NX, NY = 8, 4, 4
WIDTH = 4096
HALF = 2048
ANY = pl.BlockSpec(memory_space=pl.ANY)
VM = pl.BlockSpec(memory_space=pltpu.VMEM)
BF, F32 = jnp.bfloat16, jnp.float32


EPS = 1e-06
TAU = 16.0


def matmul(left, right):
    return jnp.dot(left, right, preferred_element_type=jnp.float32)


def rms_scale(vectors, gain):
    return vectors * lax.rsqrt(jnp.mean(vectors * vectors, axis=-1, keepdims=True) + EPS) * gain


def shape_of(*dims, dtype=BF):
    return jax.ShapeDtypeStruct(dims, dtype)


def send(src, dst, send_sem, recv_sem, **where):
    copy = pltpu.make_async_remote_copy(
        src_ref=src,
        dst_ref=dst,
        send_sem=send_sem,
        recv_sem=recv_sem,
        device_id=where,
        device_id_type=pl.DeviceIdType.MESH,
    )
    copy.start()
    return copy


def greet(partners):
    barrier = pltpu.get_barrier_semaphore()
    for where in partners:
        pl.semaphore_signal(
            barrier, inc=1, device_id=where, device_id_type=pl.DeviceIdType.MESH
        )
    return lambda: pl.semaphore_wait(barrier, len(partners))


def position():
    return tuple(lax.axis_index(a) for a in ("sp_0", "sp_1", "tp", "dp"))


def log_sigmoid(v):
    return jnp.minimum(v, 0.0) - jnp.log1p(jnp.exp(-jnp.abs(v)))


def log_decays(lowrank, decay_up, decay_bias):
    return [
        log_sigmoid(
            matmul(lowrank[:, way * RANK : (way + 1) * RANK], decay_up[way])
            + decay_bias[way : way + 1]
        )
        / TAU
        for way in range(2)
    ]


def triangle(n, lower):
    r = lax.broadcasted_iota(jnp.int32, (n, n), 0)
    c = lax.broadcasted_iota(jnp.int32, (n, n), 1)
    return r >= c if lower else r <= c


def running_sum(decay, lower):
    ones = jnp.where(triangle(decay.shape[0], lower), 1.0, 0.0).astype(BF)
    high = decay.astype(BF)
    rest = decay - high.astype(F32)
    middle = rest.astype(BF)
    low = (rest - middle.astype(F32)).astype(BF)
    return matmul(ones, high) + matmul(ones, middle) + matmul(ones, low)


def across(left, right):
    return lax.dot_general(left, right, (((1,), (1,)), ((), ())), preferred_element_type=F32)


def outer(left, right):
    return lax.dot_general(left, right, (((0,), (0,)), ((), ())), preferred_element_type=F32)


def scores_of(q, k, fwd, bwd, store):
    lower, upper = triangle(BLOCK, True), triangle(BLOCK, False)
    bf = lambda a: a.astype(BF)
    for b in range(2):
        sl = slice(b * BLOCK, (b + 1) * BLOCK)
        osl = slice((1 - b) * BLOCK, (2 - b) * BLOCK)
        f, g = fwd[sl], bwd[sl]
        cf, cg = f[BLOCK // 2 : BLOCK // 2 + 1], g[BLOCK // 2 - 1 : BLOCK // 2]
        sf = across(bf(q[sl] * jnp.exp(f - cf)), bf(k[sl] * jnp.exp(cf - f)))
        sb = across(bf(q[sl] * jnp.exp(g - cg)), bf(k[sl] * jnp.exp(cg - g)))
        store[sl, sl] = bf(jnp.where(lower, sf, 0.0) + jnp.where(upper, sb, 0.0))
        if b == 0:
            mine, other, edge = g, bwd[osl], bwd[BLOCK : BLOCK + 1]
        else:
            mine, other, edge = f, fwd[osl], fwd[BLOCK - 1 : BLOCK]
        store[sl, osl] = bf(across(bf(q[sl] * jnp.exp(mine - edge)), bf(k[osl] * jnp.exp(edge - other))))


def mixer_kernel(
    lat, context, cond, cond_ctx, gain_pre, gain_post, head_gain, w_shift, w_scale, w_gate,
    wq, wk, wv, wg, wo, w_down, decay_up, decay_bias,
    result,
    w_mod, partial, arrived, tile, tiles, column_sum, mods, vectors, lat_all, rows, w_all, proj, low, w_out,
    pack, packs, states, got_states, relay_f, relay_b, relay_g, relay_h, decays, got_decays, scores, local, entering,
    group, groups, ctx_group, ctx_groups, group_decays, all_decays, ctx_decays, all_ctx_decays,
    back, entry, before, leaving, entries, heads,
    part_a, part_b, near_a, near_b, far_a, far_b, sum_a, sum_b, relay_a, relay_c,
    s_load, s_m1, r_m1, s_m2, r_m2, s_m3, r_m3, s_l, r_l, s_w, r_w,
    s_x, r_x, s_z, r_z, s_e, r_e, s_y, r_y,
):
    z, x, y, c = position()
    x_peers = [(d, lax.rem(x + d, NX)) for d in (1, 3, 2)]
    z_peers = [(d, lax.rem(z + d, NZ)) for d in (4, 3, 5, 2, 6, 1, 7)]
    xy_peers = [
        (k, dict(sp_1=lax.rem(x + k // NY, NX), tp=lax.rem(y + k % NY, NY)))
        for k in range(1, NX * NY)
    ]
    above, below, facing = (lax.rem(y + k, NY) for k in (1, 3, 2))
    up, down = dict(tp=above), dict(tp=below)
    east, west = lax.rem(x + 1, NX), lax.rem(x + 3, NX)
    opposite = lax.rem(x + 2, NX)
    other = dict(dp=1 - c)
    columns = [pl.ds(pl.multiple_of(k * HALF, HALF), HALF) for k in (c, 1 - c)]
    entered = greet([dict(sp_0=p) for _, p in z_peers] + [w for _, w in xy_peers] + [other])
    spans = (slice(0, 256), slice(256, 512), slice(512, 1024), slice(1024, 1536))
    sources = list(zip((wq, wk, wv, wg), spans))
    loads = [(w_shift, w_mod.at[0]), (w_scale, w_mod.at[1]), (w_gate, w_mod.at[2]), (lat, lat_all.at[y])]
    loads += [(w, w_all.at[0, :, span]) for w, span in sources] + [(wo, w_out.at[0])]
    loads = [pltpu.make_async_copy(src, dst, s_load.at[k]) for k, (src, dst) in enumerate(loads)]
    for load in loads:
        load.start()
    line = lax.broadcasted_iota(jnp.int32, (16, 128), 0)
    act = jax.nn.silu(cond[...].astype(F32)).astype(BF).astype(F32)
    act_ctx = jax.nn.silu(cond_ctx[...].astype(F32)).astype(BF).astype(F32)
    total = None
    for k in range(3):
        left = jnp.where(line == k, act, jnp.where(line == k + 3, act_ctx, 0.0)).astype(BF)
        loads[k].wait()
        part = matmul(left, w_mod[k])
        total = part if total is None else total + part
    for k in range(NZ):
        partial[k] = total[:8, k * 128 : (k + 1) * 128]
    loads[3].wait()
    entered()
    m_copies = [
        send(partial.at[p], arrived.at[d], s_m1.at[d], r_m1.at[d], sp_0=p) for d, p in z_peers
    ]
    top, bottom = pl.ds(0, 32), pl.ds(32, 32)
    up_1 = send(lat_all.at[y, top], lat_all.at[y, top], s_l.at[0], r_l.at[0], **up)
    down_1 = send(lat_all.at[y, bottom], lat_all.at[y, bottom], s_l.at[1], r_l.at[1], **down)
    weights = [
        send(w, w_all.at[1, :, span], s_w.at[k], r_w.at[k], **other)
        for k, (w, span) in enumerate(sources)
    ]
    weights.append(send(wo, w_out.at[1], s_w.at[4], r_w.at[4], **other))
    for copy in m_copies:
        copy.wait()
    summed = partial[z]
    for d in range(1, NZ):
        summed = summed + arrived[d]
    tile[...] = summed
    m_copies = [
        send(tile, tiles.at[y, x], s_m2.at[k], r_m2.at[k], **w) for k, w in xy_peers
    ]
    tiles[y, x] = summed
    up_2 = send(lat_all.at[y, bottom], lat_all.at[y, bottom], s_l.at[2], r_l.at[2], **up)
    down_2 = send(lat_all.at[y, top], lat_all.at[y, top], s_l.at[3], r_l.at[3], **down)
    for copy in m_copies:
        copy.wait()
    for k in range(NY):
        block = tiles[k, 0] + tiles[k, 1] + tiles[k, 2] + tiles[k, 3]
        column_sum[k] = block
        mods[z, k] = block
    m_copies = [
        send(column_sum, mods.at[z], s_m3.at[d], r_m3.at[d], sp_0=p) for d, p in z_peers
    ]
    up_1.wait()
    passed = lat_all.at[below, top]
    relay_up = send(passed, passed, s_l.at[4], r_l.at[4], **up)
    down_1.wait()
    passed = lat_all.at[above, bottom]
    relay_down = send(passed, passed, s_l.at[5], r_l.at[5], **down)
    for copy in m_copies:
        copy.wait()
    for k in range(NY):
        for j in range(NZ):
            at = (k * NZ + j) * 128
            vectors[:, at : at + 128] = mods[j, k]

    def modulate(source, target, scale_row, shift_row, length):
        def step(k, carry):
            at = pl.ds(pl.multiple_of(k * 16, 16), 16)
            to = pl.ds(pl.multiple_of(target + k * 16, 16), 16)
            halves = [source[at, columns[h]].astype(F32) for h in range(2)]
            square = sum(jnp.sum(v * v, axis=1, keepdims=True) for v in halves)
            norm = lax.rsqrt(square / WIDTH + EPS)
            for h in range(2):
                weight = gain_pre[:, columns[h]].astype(F32) * (
                    1.0 + vectors[scale_row : scale_row + 1, columns[h]]
                )
                shift = vectors[shift_row : shift_row + 1, columns[h]]
                rows[h, to] = (halves[h] * norm * weight + shift).astype(BF)
            return carry

        lax.fori_loop(0, length // 16, step, 0)

    def project_rows(at, length, places):
        def step(k, carry):
            span = pl.ds(pl.multiple_of(k * 256, 256), 256)
            out = matmul(rows[0, at : at + length], w_all[0, :, span])
            out = (out + matmul(rows[1, at : at + length], w_all[1, :, span])).astype(BF)
            for offset, place, count in places:
                to = pl.ds(pl.multiple_of(place, 32), count)
                proj[to, span] = out[offset : offset + count]
            return carry

        lax.fori_loop(0, 6, step, 0)
        out = across(rows[0, at : at + length], w_down[:, columns[0]])
        out = (out + across(rows[1, at : at + length], w_down[:, columns[1]])).astype(BF)
        for offset, place, count in places:
            low[pl.ds(pl.multiple_of(place, 32), count)] = out[offset : offset + count]

    modulate(context, 0, 4, 3, 32)
    modulate(lat_all.at[y], 32, 1, 0, 64)
    up_2.wait()
    modulate(lat_all.at[below], 96, 1, 0, 64)
    down_2.wait()
    modulate(lat_all.at[above], 160, 1, 0, 64)
    for load in loads[4:8]:
        load.wait()
    for copy in weights[:4]:
        copy.wait()
    project_rows(0, 224, ((0, 256, 32), (32, y * 64, 64), (96, below * 64, 64), (160, above * 64, 64)))
    for j in range(NX):
        pack[j] = jnp.zeros((32, 512), BF)
        pack[j, :, :DK_HEAD] = proj[256:288, 256:512]
        pack[j, :, DK_HEAD : DK_HEAD + 128] = proj[256:288, 512 + j * 128 : 640 + j * 128]
        pack[j, :, DK_HEAD + 128 : DK_HEAD + 128 + 2 * RANK] = low[256:288]
    c_copies = [send(pack.at[p], packs.at[x], s_x.at[0, d], r_x.at[0, d], sp_1=p) for d, p in x_peers]
    packs[x] = pack[x]
    relay_up.wait()
    relay_down.wait()
    modulate(lat_all.at[facing], 224, 1, 0, 64)
    project_rows(224, 64, ((0, facing * 64, 64),))
    decay_f, decay_b = log_decays(low[:256], decay_up[...], decay_bias[...])
    fwd, bwd = running_sum(decay_f, True), running_sum(decay_b, False)
    decays[0:1] = fwd[-1:]
    decays[1:2] = bwd[:1]
    decays[2:8] = jnp.zeros((6, DK_HEAD), F32)
    x_copies = [
        send(decays, got_decays.at[x], s_x.at[1, d], r_x.at[1, d], sp_1=p) for d, p in x_peers
    ]
    got_decays[x] = decays[...]
    k = proj[:256, 256:512].astype(F32)
    v = proj[:256, 512:1024]

    def local_state(way, scaled):
        state = outer(v, (k * scaled).astype(BF)).astype(BF)
        for j in range(NX):
            states[j, way] = state[j * 128 : (j + 1) * 128]

    def to_neighbour(p, d, way):
        return send(states.at[p, way], got_states.at[x, way], s_x.at[2 + way, d], r_x.at[2 + way, d], sp_1=p)

    local_state(0, jnp.exp(fwd[-1:] - fwd))
    pass_f = send(states.at[opposite, 0], relay_f, s_x.at[2, 2], r_x.at[2, 2], sp_1=east)
    x_copies += [to_neighbour(west, 3, 0), to_neighbour(east, 1, 0)]
    local_state(1, jnp.exp(bwd[:1] - bwd))
    pass_b = send(states.at[opposite, 1], relay_b, s_x.at[3, 2], r_x.at[3, 2], sp_1=west)
    x_copies += [to_neighbour(east, 1, 1), to_neighbour(west, 3, 1)]
    got_states[x] = states[x]
    q = proj[:256, :256].astype(F32) * DK_HEAD ** (-0.5)
    scores_of(q, k, fwd, bwd, scores)
    pass_f.wait()
    x_copies.append(send(relay_f, got_states.at[west, 0], s_x.at[4, 1], r_x.at[4, 1], sp_1=east))
    pass_b.wait()
    x_copies.append(send(relay_b, got_states.at[east, 1], s_x.at[4, 3], r_x.at[4, 3], sp_1=west))
    for copy in c_copies:
        copy.wait()
    ctx = packs[...].reshape(NX * 32, 512)
    ctx_k = ctx[:, :DK_HEAD].astype(F32)
    ctx_v = ctx[:, DK_HEAD : DK_HEAD + 128]
    ctx_lr = ctx[:, DK_HEAD + 128 : DK_HEAD + 128 + 2 * RANK]
    cdf, cdb = log_decays(ctx_lr, decay_up[...], decay_bias[...])
    cf, cb = running_sum(cdf, True), running_sum(cdb, False)
    for way, scaled in enumerate((jnp.exp(cf[-1:] - cf), jnp.exp(cb[:1] - cb))):
        state = outer(ctx_v, (ctx_k * scaled).astype(BF)).astype(BF)
        for j in range(NZ):
            ctx_group[j, way] = state[j * 16 : (j + 1) * 16]
    ctx_decays[0:1] = cf[-1:]
    ctx_decays[1:2] = cb[:1]
    ctx_decays[2:8] = jnp.zeros((6, DK_HEAD), F32)
    c_copies = []
    for d, p in z_peers:
        c_copies.append(send(ctx_group.at[p], ctx_groups.at[z], s_z.at[0, d], r_z.at[0, d], sp_0=p))
        c_copies.append(send(ctx_decays, all_ctx_decays.at[z], s_z.at[1, d], r_z.at[1, d], sp_0=p))
    ctx_groups[z] = ctx_group[z]
    all_ctx_decays[z] = ctx_decays[...]
    local[...] = matmul(scores[...], v)
    entering[0] = (q * jnp.exp(fwd)).astype(BF)
    entering[1] = (q * jnp.exp(bwd)).astype(BF)
    for copy in x_copies:
        copy.wait()
    ways = (tuple(range(NX)), tuple(reversed(range(NX))))
    for way in range(2):
        state, total = None, None
        for j in ways[way]:
            step, piece = got_decays[j, way : way + 1], got_states[j, way].astype(F32)
            state = piece if state is None else state * jnp.exp(step) + piece
            total = step if total is None else total + step
        state = state.astype(BF)
        for j in range(NZ):
            group[j, way] = state[j * 16 : (j + 1) * 16]
        group_decays[way : way + 1] = total
    group_decays[2:8] = jnp.zeros((6, DK_HEAD), F32)
    z_copies = []
    for d, p in z_peers:
        z_copies.append(send(group.at[p], groups.at[z], s_z.at[2, d], r_z.at[2, d], sp_0=p))
        z_copies.append(send(group_decays, all_decays.at[z], s_z.at[3, d], r_z.at[3, d], sp_0=p))
    groups[z] = group[z]
    all_decays[z] = group_decays[...]
    for way in range(2):
        state = jnp.zeros((128, DK_HEAD), F32)
        for j in ways[way]:
            before[j, way] = state
            state = state * jnp.exp(got_decays[j, way : way + 1]) + got_states[j, way].astype(F32)
    orders = (tuple(range(NZ)), tuple(reversed(range(NZ))))
    for copy in c_copies:
        copy.wait()
    starts = []
    for way in range(2):
        state = jnp.zeros((16, DK_HEAD), F32)
        for j in orders[way]:
            state = state * jnp.exp(all_ctx_decays[j, way : way + 1]) + ctx_groups[j, way].astype(F32)
        starts.append(state)
    for copy in z_copies:
        copy.wait()
    for way in range(2):
        state = starts[way]
        for j in orders[way]:
            back[j, way] = state.astype(BF)
            state = state * jnp.exp(all_decays[j, way : way + 1]) + groups[j, way].astype(F32)
    z_copies = [send(back.at[p], entry.at[z], s_z.at[4, d], r_z.at[4, d], sp_0=p) for d, p in z_peers]
    entry[z] = back[z]
    gate = jax.nn.silu(proj[:256, 1024:1536].astype(F32)) * head_gain[...].astype(F32)
    for copy in z_copies:
        copy.wait()
    for way in range(2):
        start = jnp.concatenate([entry[j, way] for j in range(NZ)], axis=0).astype(F32)
        passed = jnp.zeros((1, DK_HEAD), F32)
        for j in ways[way]:
            leaving[j, way] = (start * jnp.exp(passed) + before[j, way]).astype(BF)
            passed = passed + got_decays[j, way : way + 1]

    def return_to(p, d, way):
        return send(leaving.at[p, way], entries.at[x, way], s_e.at[way, d], r_e.at[way, d], sp_1=p)

    pass_f = send(leaving.at[opposite, 0], relay_g, s_e.at[0, 2], r_e.at[0, 2], sp_1=east)
    pass_b = send(leaving.at[opposite, 1], relay_h, s_e.at[1, 2], r_e.at[1, 2], sp_1=west)
    e_copies = [return_to(p, d, way) for way in range(2) for p, d in ((east, 1), (west, 3))]
    entries[x] = leaving[x]
    pass_f.wait()
    e_copies.append(send(relay_g, entries.at[west, 0], s_e.at[2, 1], r_e.at[2, 1], sp_1=east))
    pass_b.wait()
    e_copies.append(send(relay_h, entries.at[east, 1], s_e.at[2, 3], r_e.at[2, 3], sp_1=west))
    loads[8].wait()
    weights[4].wait()
    for copy in e_copies:
        copy.wait()
    out = [
        local[:, j * 128 : (j + 1) * 128]
        + across(entering[0], entries[j, 0])
        + across(entering[1], entries[j, 1])
        for j in range(NX)
    ]
    square = sum(jnp.sum(o * o, axis=1, keepdims=True) for o in out)
    scale = lax.rsqrt(square / DV_HEAD + EPS)
    for j in range(NX):
        heads[:, j * 128 : (j + 1) * 128] = (out[j] * scale * gate[:, j * 128 : (j + 1) * 128]).astype(BF)
    count = 64

    def project(owner):
        at = heads[pl.ds(pl.multiple_of(owner * count, count), count)]
        part_a[owner] = matmul(at, w_out[0]).astype(BF)
        part_b[owner] = matmul(at, w_out[1]).astype(BF)

    project(facing)
    first_a = send(part_a.at[facing], relay_a, s_y.at[0], r_y.at[0], **down)
    first_b = send(part_b.at[facing], relay_c, s_y.at[1], r_y.at[1], **up)
    project(below)
    direct_b = send(part_b.at[below], near_b, s_y.at[2], r_y.at[2], **down)
    project(above)
    direct_a = send(part_a.at[above], near_a, s_y.at[3], r_y.at[3], **up)
    first_a.wait()
    sum_a[...] = (relay_a[...].astype(F32) + part_a[below].astype(F32)).astype(BF)
    second_a = send(sum_a, far_a, s_y.at[4], r_y.at[4], **down)
    first_b.wait()
    sum_b[...] = (relay_c[...].astype(F32) + part_b[above].astype(F32)).astype(BF)
    second_b = send(sum_b, far_b, s_y.at[5], r_y.at[5], **up)
    project(y)
    direct_a.wait()
    direct_b.wait()
    second_a.wait()
    second_b.wait()

    def finish(k, carry):
        at = pl.ds(pl.multiple_of(k * 16, 16), 16)
        a = part_a[y, at].astype(F32) + near_a[at].astype(F32) + far_a[at].astype(F32)
        b = part_b[y, at].astype(F32) + near_b[at].astype(F32) + far_b[at].astype(F32)
        square = jnp.sum(a * a, axis=1, keepdims=True) + jnp.sum(b * b, axis=1, keepdims=True)
        scale = lax.rsqrt(square / WIDTH + EPS)
        for span, half in zip(columns, (a, b)):
            weight = vectors[2:3, span] * gain_post[:, span].astype(F32)
            result[at, span] = (
                lat_all[y, at, span].astype(F32) + half * scale * weight
            ).astype(BF)
        return carry

    lax.fori_loop(0, count // 16, finish, 0)


def mixer(*args):
    dma = pltpu.SemaphoreType.DMA
    vm = pltpu.VMEM
    half = vm((64, HALF), BF)
    in_specs = [VM] * len(args)
    for k in (0, 7, 8, 9, 10, 11, 12, 13, 14):
        in_specs[k] = ANY
    piece = vm((128, DK_HEAD), BF)
    return pl.pallas_call(
        mixer_kernel,
        out_shape=shape_of(64, WIDTH),
        in_specs=in_specs,
        out_specs=VM,
        scratch_shapes=[
            vm((3, 128, 1024), BF), vm((NZ, 8, 128), F32), vm((NZ, 8, 128), F32),
            vm((8, 128), F32), vm((NY, NX, 8, 128), F32), vm((NY, 8, 128), F32),
            vm((NZ, NY, 8, 128), F32), vm((8, WIDTH), F32),
            vm((NY, 64, WIDTH), BF), vm((2, 288, HALF), BF), vm((2, HALF, 1536), BF),
            vm((288, 1536), BF), vm((288, 2 * RANK), BF), vm((2, DV_HEAD, HALF), BF),
            vm((NX, 32, 512), BF), vm((NX, 32, 512), BF),
            vm((NX, 2, 128, DK_HEAD), BF), vm((NX, 2, 128, DK_HEAD), BF), piece, piece, piece, piece,
            vm((8, DK_HEAD), F32), vm((NX, 8, DK_HEAD), F32),
            vm((256, 256), BF), vm((256, DV_HEAD), F32), vm((2, 256, DK_HEAD), BF),
            vm((NZ, 2, 16, DK_HEAD), BF), vm((NZ, 2, 16, DK_HEAD), BF),
            vm((NZ, 2, 16, DK_HEAD), BF), vm((NZ, 2, 16, DK_HEAD), BF),
            vm((8, DK_HEAD), F32), vm((NZ, 8, DK_HEAD), F32),
            vm((8, DK_HEAD), F32), vm((NZ, 8, DK_HEAD), F32),
            vm((NZ, 2, 16, DK_HEAD), BF), vm((NZ, 2, 16, DK_HEAD), BF),
            vm((NX, 2, 128, DK_HEAD), F32),
            vm((NX, 2, 128, DK_HEAD), BF), vm((NX, 2, 128, DK_HEAD), BF),
            vm((256, DV_HEAD), BF),
            vm((NY, 64, HALF), BF), vm((NY, 64, HALF), BF),
            half, half, half, half, half, half, half, half,
            dma((9,)), dma((NZ,)), dma((NZ,)), dma((16,)), dma((16,)), dma((NZ,)), dma((NZ,)),
            dma((6,)), dma((6,)), dma((5,)), dma((5,)),
            dma((5, NX)), dma((5, NX)), dma((5, NZ)), dma((5, NZ)),
            dma((3, NX)), dma((3, NX)), dma((6,)), dma((6,)),
        ],
        compiler_params=pltpu.CompilerParams(
            collective_id=0, has_side_effects=True, vmem_limit_bytes=60 * 2**20
        ),
        name="mixer",
    )(*args)


def body(
    latents, cond, cond_ctx, context, w_shift, w_scale, w_gate, gain_pre, gain_post,
    w_query, w_key, w_value, w_outgate, w_down, decay_up, decay_bias, head_gain, w_out,
):
    result = mixer(
        latents[0], context[0], cond, cond_ctx[None], gain_pre[None], gain_post[None], head_gain[None],
        w_shift, w_scale, w_gate, w_query, w_key, w_value, w_outgate, w_out,
        w_down.T, decay_up, decay_bias,
    )
    return result[None]


def solution(mesh):
    finer = Mesh(
        mesh.devices.reshape(8, 4, mesh.shape["tp"], mesh.shape["dp"]), ("sp_0", "sp_1", "tp", "dp")
    )
    in_specs = (
        P("dp", SP_TP, None),
        P("dp", SP),
        P(SP),
        P("dp", SP, None),
        P(SP, "tp"),
        P(SP, "tp"),
        P(SP, "tp"),
        P(),
        P(),
        P("dp", "tp"),
        P("dp", "tp"),
        P("dp", "tp"),
        P("dp", "tp"),
        P(),
        P(None, None, "tp"),
        P(None, "tp"),
        P("tp"),
        P("tp", "dp"),
    )
    out_specs = P("dp", SP_TP, None)
    return jax.shard_map(body, mesh=finer, in_specs=in_specs, out_specs=out_specs, check_vma=False)
```

time: 110 us -> 87.9 us (0.80)
  matrix products: 12.7 us -> 0 us
  local copies, waits for them, and re-layouts: 12.1 us -> 5.75 us
  Pallas kernels: 84.9 us -> 81.9 us
    pallas_call x1 -> x0, Pallas kernels: 35.2 us -> none  [gather_inputs(): pl.pallas_call(gather_kernel, out_shape=[shape_of(8, WIDTH, dtype=F32), s...]
    pallas_call x1, Pallas kernels: 49.7 us -> 81.9 us  [mixer(): pl.pallas_call(mixer_kernel, out_shape=shape_of(64, WIDTH), in_specs=in_s...]
    dot_general x10 -> x0, matrix products: 12.7 us -> none  [matmul(): return jnp.dot(left, right, preferred_element_type=jnp.float32)]
    unnamed x23 -> x1, local copies, waits for them, and re-layouts: 5.64 us -> 1.87 us
    slice x6 -> x0, local copies, waits for them, and re-layouts: 2.59 us -> none  [the longest x1 0.72 us: body(): values[:count]]
where the time goes in v3:
time: 87.9 us; the launch traced here: 87.7 us
  Pallas kernels  81.9 us (93%)
  local copies, waits for them, and re-layouts  5.75 us (7%)
    pallas_call x1, Pallas kernels, mixer(): pl.pallas_call(mixer_kernel, out_shape=shape_of(64, WIDTH), in_specs=in_s...  81.9 us
    unnamed x1, local copies, waits for them, and re-layouts  1.87 us

profile of v3, /device:TPU:2, one launch (start us, length us, event | category | flops | bytes accessed | tf_op | source)
XLA Modules:
  0.0 87.7 jit_solution(13710750160012370008)
XLA Ops:
  0.0 1.3 %broadcast_in_dim.18.head_gain = bf16[1,512]{1,0:T(2,128)(2,1)} reshape(bf16[512]{0:T(512)(128)(2,1)} %param.34) | data formatting | bytes 2048 | tf_op jit(solution)/shard_map/broadcast_in_dim | solution.py:494
  1.3 1.3 %broadcast_in_dim.16.gain_pre = bf16[1,4096]{1,0:T(2,128)(2,1)} reshape(bf16[4096]{0:T(1024)(128)(2,1)} %param.25) | data formatting | bytes 16384 | tf_op jit(solution)/shard_map/broadcast_in_dim | solution.py:494
  2.6 1.3 %broadcast_in_dim.17.gain_post = bf16[1,4096]{1,0:T(2,128)(2,1)} reshape(bf16[4096]{0:T(1024)(128)(2,1)} %param.26) | data formatting | bytes 16384 | tf_op jit(solution)/shard_map/broadcast_in_dim | solution.py:494
  3.9 81.9 %mixer.1 = bf16[64,4096]{1,0:T(8,128)(2,1)} custom-call(bf16[64,4096]{1,0:T(8,128)(2,1)} %bitcast.6, bf16[32,4096]{1,0:T(8,128)(2,1)} %bitcast.7, bf16[1,128]{1,0:T(2,128)(2,1)} %cond.1, bf16[1,128]{1,0:T(2,128)(2,1)} %bitcast.9, bf16[1,4096]{1,0:T(2,128)(2,1)} %broadcast_in_dim.16.gain_pre, bf16[1,4096]{1,0:T(2,128)(2,1)} %broadcast_in_dim.17.gain_post, ...), custom_call_target="tpu_custom_call" | custom-call | tf_op jit(solution)/shard_map/mixer/pallas_call | solution.py:452
  85.8 1.9 %copy.20 = bf16[1,64,4096]{2,1,0:T(8,128)(2,1)} copy(bf16[1,64,4096]{2,1,0:T(8,128)(2,1)} %bitcast.5) | data formatting | bytes 1048576

commit v4 on v3

v4 whole, which is shorter than its diff:
```python
import jax
import jax.numpy as jnp
from jax import lax
from jax.experimental import pallas as pl
from jax.experimental.pallas import tpu as pltpu
from jax.sharding import Mesh
from jax.sharding import PartitionSpec as P

DK_HEAD = 256
DV_HEAD = 512
RANK = 16
BLOCK = 128
SP_TP = ("sp_0", "sp_1", "tp")
SP = ("sp_0", "sp_1")
NZ, NX, NY = 8, 4, 4
WIDTH = 4096
HALF = 2048
ANY = pl.BlockSpec(memory_space=pl.ANY)
VM = pl.BlockSpec(memory_space=pltpu.VMEM)
BF, F32 = jnp.bfloat16, jnp.float32


EPS = 1e-06
TAU = 16.0


def matmul(left, right):
    return jnp.dot(left, right, preferred_element_type=jnp.float32)


def rms_scale(vectors, gain):
    return vectors * lax.rsqrt(jnp.mean(vectors * vectors, axis=-1, keepdims=True) + EPS) * gain


def shape_of(*dims, dtype=BF):
    return jax.ShapeDtypeStruct(dims, dtype)


def send(src, dst, send_sem, recv_sem, **where):
    copy = pltpu.make_async_remote_copy(
        src_ref=src,
        dst_ref=dst,
        send_sem=send_sem,
        recv_sem=recv_sem,
        device_id=where,
        device_id_type=pl.DeviceIdType.MESH,
    )
    copy.start()
    return copy


def greet(partners):
    barrier = pltpu.get_barrier_semaphore()
    for where in partners:
        pl.semaphore_signal(
            barrier, inc=1, device_id=where, device_id_type=pl.DeviceIdType.MESH
        )
    return lambda: pl.semaphore_wait(barrier, len(partners))


def position():
    return tuple(lax.axis_index(a) for a in ("sp_0", "sp_1", "tp", "dp"))


def log_sigmoid(v):
    return jnp.minimum(v, 0.0) - jnp.log1p(jnp.exp(-jnp.abs(v)))


def log_decays(lowrank, decay_up, decay_bias):
    return [
        log_sigmoid(
            matmul(lowrank[:, way * RANK : (way + 1) * RANK], decay_up[way])
            + decay_bias[way : way + 1]
        )
        / TAU
        for way in range(2)
    ]


def triangle(n, lower):
    r = lax.broadcasted_iota(jnp.int32, (n, n), 0)
    c = lax.broadcasted_iota(jnp.int32, (n, n), 1)
    return r >= c if lower else r <= c


def running_sum(decay, lower):
    ones = jnp.where(triangle(decay.shape[0], lower), 1.0, 0.0).astype(BF)
    high = decay.astype(BF)
    rest = decay - high.astype(F32)
    middle = rest.astype(BF)
    low = (rest - middle.astype(F32)).astype(BF)
    return matmul(ones, high) + matmul(ones, middle) + matmul(ones, low)


def across(left, right):
    return lax.dot_general(left, right, (((1,), (1,)), ((), ())), preferred_element_type=F32)


def outer(left, right):
    return lax.dot_general(left, right, (((0,), (0,)), ((), ())), preferred_element_type=F32)


def scores_of(q, k, fwd, bwd, store):
    lower, upper = triangle(BLOCK, True), triangle(BLOCK, False)
    bf = lambda a: a.astype(BF)
    for b in range(2):
        sl = slice(b * BLOCK, (b + 1) * BLOCK)
        osl = slice((1 - b) * BLOCK, (2 - b) * BLOCK)
        f, g = fwd[sl], bwd[sl]
        cf, cg = f[BLOCK // 2 : BLOCK // 2 + 1], g[BLOCK // 2 - 1 : BLOCK // 2]
        sf = across(bf(q[sl] * jnp.exp(f - cf)), bf(k[sl] * jnp.exp(cf - f)))
        sb = across(bf(q[sl] * jnp.exp(g - cg)), bf(k[sl] * jnp.exp(cg - g)))
        store[sl, sl] = bf(jnp.where(lower, sf, 0.0) + jnp.where(upper, sb, 0.0))
        if b == 0:
            mine, other, edge = g, bwd[osl], bwd[BLOCK : BLOCK + 1]
        else:
            mine, other, edge = f, fwd[osl], fwd[BLOCK - 1 : BLOCK]
        store[sl, osl] = bf(across(bf(q[sl] * jnp.exp(mine - edge)), bf(k[osl] * jnp.exp(edge - other))))


def arrived_at(ref, sem):
    pltpu.make_async_copy(ref, ref, sem).wait()


def mixer_kernel(
    lat, context, cond, cond_ctx, gain_pre, gain_post, head_gain, w_shift, w_scale, w_gate,
    wq, wk, wv, wg, wo, w_down, decay_up, decay_bias,
    result,
    w_mod, partial, partials, tile, tiles, column_sum, mods, vectors, norms, lat_all, rows, w_all,
    proj, low, w_out,
    pack, packs, states, got_states, relays, relays_e, decays, got_decays, scores, local, entering,
    group, groups, ctx_group, ctx_groups, group_decays, all_decays,
    back, entry, before, leaving, entries, heads, part_a, part_b, near, sum_a, sum_b, relay_a, relay_c,
    s_load, m_sem, l_send, l_recv, w_sem, c_sem, x_sem, z_sem, e_sem, y_sem,
):
    z, x, y, c = position()
    x_peers = [lax.rem(x + d, NX) for d in (1, 3, 2)]
    z_peers = [lax.rem(z + d, NZ) for d in (4, 3, 5, 2, 6, 1, 7)]
    xy_peers = [
        dict(sp_1=lax.rem(x + k // NY, NX), tp=lax.rem(y + k % NY, NY)) for k in range(1, NX * NY)
    ]
    above, below, facing = (lax.rem(y + k, NY) for k in (1, 3, 2))
    up, down = dict(tp=above), dict(tp=below)
    east, west = lax.rem(x + 1, NX), lax.rem(x + 3, NX)
    opposite = lax.rem(x + 2, NX)
    other = dict(dp=1 - c)
    columns = [pl.ds(pl.multiple_of(k * HALF, HALF), HALF) for k in (c, 1 - c)]
    entered = greet([dict(sp_0=p) for p in z_peers] + xy_peers + [other])
    spans = (slice(0, 256), slice(256, 512), slice(512, 1024), slice(1024, 1536))
    sources = list(zip((wq, wk, wv, wg), spans))
    for k, w in enumerate((w_shift, w_scale, w_gate)):
        pltpu.make_async_copy(w, w_mod.at[k], s_load.at[0]).start()
    own_rows = pltpu.make_async_copy(lat, lat_all.at[y], s_load.at[1])
    own_rows.start()
    for w, span in sources:
        pltpu.make_async_copy(w, w_all.at[0, :, span], s_load.at[2]).start()
    own_out = pltpu.make_async_copy(wo, w_out.at[0], s_load.at[3])
    own_out.start()
    line = lax.broadcasted_iota(jnp.int32, (16, 128), 0)
    act = jax.nn.silu(cond[...].astype(F32)).astype(BF).astype(F32)
    act_ctx = jax.nn.silu(cond_ctx[...].astype(F32)).astype(BF).astype(F32)
    arrived_at(w_mod, s_load.at[0])
    total = None
    for k in range(3):
        left = jnp.where(line == k, act, jnp.where(line == k + 3, act_ctx, 0.0)).astype(BF)
        part = matmul(left, w_mod[k])
        total = part if total is None else total + part
    for k in range(NZ):
        partial[k] = total[:8, k * 128 : (k + 1) * 128]
    own_rows.wait()
    entered()
    for p in z_peers:
        send(partial.at[p], partials.at[z], m_sem.at[0], m_sem.at[1], sp_0=p)
    partials[z] = partial[z]
    top, bottom = pl.ds(0, 32), pl.ds(32, 32)
    up_1 = send(lat_all.at[y, top], lat_all.at[y, top], l_send.at[0], l_recv.at[0], **up)
    down_1 = send(lat_all.at[y, bottom], lat_all.at[y, bottom], l_send.at[0], l_recv.at[1], **down)
    for w, span in sources:
        send(w, w_all.at[1, :, span], w_sem.at[0], w_sem.at[1], **other)
    out_weight = send(wo, w_out.at[1], w_sem.at[2], w_sem.at[3], **other)

    def norm_of(source, target, length):
        def step(k, carry):
            v = source[pl.ds(pl.multiple_of(k * 16, 16), 16)].astype(F32)
            square = jnp.sum(v * v, axis=1, keepdims=True)
            norms[pl.ds(pl.multiple_of(target + k * 16, 16), 16)] = jnp.broadcast_to(
                lax.rsqrt(square / WIDTH + EPS), (16, 128)
            )
            return carry

        lax.fori_loop(0, length // 16, step, 0)

    norm_of(context, 0, 32)
    norm_of(lat_all.at[y], 32, 64)
    arrived_at(partials.at[pl.ds(0, NZ - 1)], m_sem.at[1])
    summed = partials[0]
    for k in range(1, NZ):
        summed = summed + partials[k]
    tile[...] = summed
    tiles[y * NX + x] = summed
    for w in xy_peers:
        send(tile, tiles.at[y * NX + x], m_sem.at[2], m_sem.at[3], **w)
    up_2 = send(lat_all.at[y, bottom], lat_all.at[y, bottom], l_send.at[0], l_recv.at[2], **up)
    down_2 = send(lat_all.at[y, top], lat_all.at[y, top], l_send.at[0], l_recv.at[3], **down)
    arrived_at(tiles.at[pl.ds(0, NX * NY - 1)], m_sem.at[3])
    for k in range(NY):
        block = tiles[k * NX] + tiles[k * NX + 1] + tiles[k * NX + 2] + tiles[k * NX + 3]
        column_sum[k] = block
        mods[z, k] = block
    for p in z_peers:
        send(column_sum, mods.at[z], m_sem.at[4], m_sem.at[5], sp_0=p)
    up_1.wait_recv()
    passed = lat_all.at[below, top]
    relay_up = send(passed, passed, l_send.at[0], l_recv.at[4], **up)
    down_1.wait_recv()
    passed = lat_all.at[above, bottom]
    relay_down = send(passed, passed, l_send.at[0], l_recv.at[5], **down)
    up_2.wait_recv()
    norm_of(lat_all.at[below], 96, 64)
    down_2.wait_recv()
    norm_of(lat_all.at[above], 160, 64)
    arrived_at(mods.at[pl.ds(0, NZ - 1)], m_sem.at[5])
    for k in range(NY):
        for j in range(NZ):
            at = (k * NZ + j) * 128
            vectors[:, at : at + 128] = mods[j, k]

    def modulate(source, target, scale_row, shift_row, length):
        def step(k, carry):
            at = pl.ds(pl.multiple_of(k * 16, 16), 16)
            to = pl.ds(pl.multiple_of(target + k * 16, 16), 16)
            norm = norms[to, 0:1]
            for h in range(2):
                weight = gain_pre[columns[h]].reshape(1, HALF).astype(F32) * (
                    1.0 + vectors[scale_row : scale_row + 1, columns[h]]
                )
                shift = vectors[shift_row : shift_row + 1, columns[h]]
                rows[h, to] = (source[at, columns[h]].astype(F32) * norm * weight + shift).astype(BF)
            return carry

        lax.fori_loop(0, length // 16, step, 0)

    def project_rows(at, length, places):
        def step(k, carry):
            span = pl.ds(pl.multiple_of(k * 256, 256), 256)
            out = matmul(rows[0, at : at + length], w_all[0, :, span])
            out = (out + matmul(rows[1, at : at + length], w_all[1, :, span])).astype(BF)
            for offset, place, count in places:
                to = pl.ds(pl.multiple_of(place, 32), count)
                proj[to, span] = out[offset : offset + count]
            return carry

        lax.fori_loop(0, 6, step, 0)
        out = across(rows[0, at : at + length], w_down[:, columns[0]])
        out = (out + across(rows[1, at : at + length], w_down[:, columns[1]])).astype(BF)
        for offset, place, count in places:
            low[pl.ds(pl.multiple_of(place, 32), count)] = out[offset : offset + count]

    modulate(context, 0, 4, 3, 32)
    modulate(lat_all.at[y], 32, 1, 0, 64)
    modulate(lat_all.at[below], 96, 1, 0, 64)
    arrived_at(w_all.at[0], s_load.at[2])
    arrived_at(w_all.at[1], w_sem.at[1])
    project_rows(0, 160, ((0, 256, 32), (32, y * 64, 64), (96, below * 64, 64)))
    for j in range(NX):
        pack[j] = jnp.zeros((32, 512), BF)
        pack[j, :, :DK_HEAD] = proj[256:288, 256:512]
        pack[j, :, DK_HEAD : DK_HEAD + 128] = proj[256:288, 512 + j * 128 : 640 + j * 128]
        pack[j, :, DK_HEAD + 128 : DK_HEAD + 128 + 2 * RANK] = low[256:288]
    for p in x_peers:
        send(pack.at[p], packs.at[x], c_sem.at[0], c_sem.at[1], sp_1=p)
    packs[x] = pack[x]
    modulate(lat_all.at[above], 160, 1, 0, 64)
    relay_up.wait_recv()
    relay_down.wait_recv()
    norm_of(lat_all.at[facing], 224, 64)
    modulate(lat_all.at[facing], 224, 1, 0, 64)
    project_rows(160, 128, ((0, above * 64, 64), (64, facing * 64, 64)))
    decay_f, decay_b = log_decays(low[:256], decay_up[...], decay_bias[...])
    fwd, bwd = running_sum(decay_f, True), running_sum(decay_b, False)
    decays[0:1] = fwd[-1:]
    decays[1:2] = bwd[:1]
    decays[2:8] = jnp.zeros((6, DK_HEAD), F32)
    for p in x_peers:
        send(decays, got_decays.at[x], c_sem.at[2], c_sem.at[3], sp_1=p)
    got_decays[x] = decays[...]
    k = proj[:256, 256:512].astype(F32)
    v = proj[:256, 512:1024]
    first, second = pl.ds(0, 64), pl.ds(64, 64)

    def swap(source, target, relay, way, sems):
        far = source.at[way, opposite]
        there = target.at[way, x]
        sent, got = sems.at[way, 0], sems.at[way, 1]
        passed = sems.at[way, 2]
        send(far.at[first], relay.at[way, 0], sent, passed, sp_1=east)
        send(far.at[second], relay.at[way, 1], sent, passed, sp_1=west)
        send(source.at[way, east], there, sent, got, sp_1=east)
        send(source.at[way, west], there, sent, got, sp_1=west)

    def pass_on(target, relay, way, sems):
        arrived_at(relay.at[way], sems.at[way, 2])
        sent, got = sems.at[way, 0], sems.at[way, 1]
        send(relay.at[way, 0], target.at[way, west, first], sent, got, sp_1=east)
        send(relay.at[way, 1], target.at[way, east, second], sent, got, sp_1=west)

    def swapped(target, way, sems):
        arrived_at(target.at[way, pl.ds(0, NX - 1)], sems.at[way, 1])

    def local_state(way, scaled):
        state = outer(v, (k * scaled).astype(BF)).astype(BF)
        for j in range(NX):
            states[way, j] = state[j * 128 : (j + 1) * 128]
        swap(states, got_states, relays, way, x_sem)
        got_states[way, x] = states[way, x]

    local_state(0, jnp.exp(fwd[-1:] - fwd))
    local_state(1, jnp.exp(bwd[:1] - bwd))
    arrived_at(packs.at[pl.ds(0, NX - 1)], c_sem.at[1])
    ctx = packs[...].reshape(NX * 32, 512)
    ctx_k = ctx[:, :DK_HEAD].astype(F32)
    ctx_v = ctx[:, DK_HEAD : DK_HEAD + 128]
    ctx_lr = ctx[:, DK_HEAD + 128 : DK_HEAD + 128 + 2 * RANK]
    cdf, cdb = log_decays(ctx_lr, decay_up[...], decay_bias[...])
    cf, cb = running_sum(cdf, True), running_sum(cdb, False)
    for way, scaled in enumerate((jnp.exp(cf[-1:] - cf), jnp.exp(cb[:1] - cb))):
        state = outer(ctx_v, (ctx_k * scaled).astype(BF)).astype(BF)
        for j in range(NZ):
            ctx_group[j, way] = state[j * 16 : (j + 1) * 16]
    for p in z_peers:
        send(ctx_group.at[p], ctx_groups.at[z], z_sem.at[0], z_sem.at[1], sp_0=p)
    ctx_groups[z] = ctx_group[z]
    pass_on(got_states, relays, 0, x_sem)
    arrived_at(got_decays.at[pl.ds(0, NX - 1)], c_sem.at[3])
    group_decays[0:2] = sum(got_decays[j, 0:2] for j in range(NX))
    group_decays[2:3] = cf[-1:]
    group_decays[3:4] = cb[:1]
    group_decays[4:8] = jnp.zeros((4, DK_HEAD), F32)
    for p in z_peers:
        send(group_decays, all_decays.at[z], z_sem.at[2], z_sem.at[3], sp_0=p)
    all_decays[z] = group_decays[...]
    pass_on(got_states, relays, 1, x_sem)
    q = proj[:256, :256].astype(F32) * DK_HEAD ** (-0.5)
    scores_of(q, k, fwd, bwd, scores)
    ways = (tuple(range(NX)), tuple(reversed(range(NX))))
    orders = (tuple(range(NZ)), tuple(reversed(range(NZ))))
    for way in range(2):
        swapped(got_states, way, x_sem)
        state = None
        for j in ways[way]:
            piece = got_states[way, j].astype(F32)
            state = piece if state is None else state * jnp.exp(got_decays[j, way : way + 1]) + piece
        state = state.astype(BF)
        for j in range(NZ):
            group[way, j] = state[j * 16 : (j + 1) * 16]
        for p in z_peers:
            send(group.at[way, p], groups.at[way, z], z_sem.at[4 + way], z_sem.at[6 + way], sp_0=p)
        groups[way, z] = group[way, z]
    for way in range(2):
        state = jnp.zeros((128, DK_HEAD), F32)
        for j in ways[way]:
            before[way, j] = state
            state = state * jnp.exp(got_decays[j, way : way + 1]) + got_states[way, j].astype(F32)
    local[...] = matmul(scores[...], v)
    entering[0] = (q * jnp.exp(fwd)).astype(BF)
    entering[1] = (q * jnp.exp(bwd)).astype(BF)
    arrived_at(ctx_groups.at[pl.ds(0, NZ - 1)], z_sem.at[1])
    arrived_at(all_decays.at[pl.ds(0, NZ - 1)], z_sem.at[3])
    starts = []
    for way in range(2):
        state = jnp.zeros((16, DK_HEAD), F32)
        for j in orders[way]:
            state = state * jnp.exp(all_decays[j, 2 + way : 3 + way]) + ctx_groups[j, way].astype(F32)
        starts.append(state)
    for way in range(2):
        arrived_at(groups.at[way, pl.ds(0, NZ - 1)], z_sem.at[6 + way])
        state = starts[way]
        for j in orders[way]:
            back[way, j] = state.astype(BF)
            state = state * jnp.exp(all_decays[j, way : way + 1]) + groups[way, j].astype(F32)
        for p in z_peers:
            send(back.at[way, p], entry.at[way, z], z_sem.at[8 + way], z_sem.at[10 + way], sp_0=p)
        entry[way, z] = back[way, z]
    gate = jax.nn.silu(proj[:256, 1024:1536].astype(F32)) * head_gain[...].reshape(1, DV_HEAD).astype(F32)
    for way in range(2):
        arrived_at(entry.at[way, pl.ds(0, NZ - 1)], z_sem.at[10 + way])
        start = entry[way].reshape(128, DK_HEAD).astype(F32)
        passed = jnp.zeros((1, DK_HEAD), F32)
        for j in ways[way]:
            leaving[way, j] = (start * jnp.exp(passed) + before[way, j]).astype(BF)
            passed = passed + got_decays[j, way : way + 1]
        swap(leaving, entries, relays_e, way, e_sem)
        entries[way, x] = leaving[way, x]
    pass_on(entries, relays_e, 0, e_sem)
    pass_on(entries, relays_e, 1, e_sem)
    own_out.wait()
    out_weight.wait_recv()
    swapped(entries, 0, e_sem)
    out = [
        local[:, j * 128 : (j + 1) * 128] + across(entering[0], entries[0, j]) for j in range(NX)
    ]
    swapped(entries, 1, e_sem)
    out = [o + across(entering[1], entries[1, j]) for j, o in enumerate(out)]
    square = sum(jnp.sum(o * o, axis=1, keepdims=True) for o in out)
    scale = lax.rsqrt(square / DV_HEAD + EPS)
    for j in range(NX):
        heads[:, j * 128 : (j + 1) * 128] = (out[j] * scale * gate[:, j * 128 : (j + 1) * 128]).astype(BF)
    count = 64

    def project(owner, part, half):
        at = heads[pl.ds(pl.multiple_of(owner * count, count), count)]
        part[owner] = matmul(at, w_out[half]).astype(BF)

    project(facing, part_a, 0)
    first_a = send(part_a.at[facing], relay_a, y_sem.at[0], y_sem.at[1], **down)
    project(facing, part_b, 1)
    first_b = send(part_b.at[facing], relay_c, y_sem.at[0], y_sem.at[2], **up)
    project(below, part_b, 1)
    send(part_b.at[below], near.at[1], y_sem.at[0], y_sem.at[3], **down)
    project(above, part_a, 0)
    send(part_a.at[above], near.at[0], y_sem.at[0], y_sem.at[3], **up)
    project(below, part_a, 0)
    project(above, part_b, 1)
    first_a.wait_recv()
    sum_a[...] = (relay_a[...].astype(F32) + part_a[below].astype(F32)).astype(BF)
    send(sum_a, near.at[2], y_sem.at[0], y_sem.at[3], **down)
    first_b.wait_recv()
    sum_b[...] = (relay_c[...].astype(F32) + part_b[above].astype(F32)).astype(BF)
    send(sum_b, near.at[3], y_sem.at[0], y_sem.at[3], **up)
    project(y, part_a, 0)
    project(y, part_b, 1)
    arrived_at(partials.at[pl.ds(0, NZ - 1)], m_sem.at[0])
    arrived_at(tiles.at[pl.ds(0, NX * NY - 1)], m_sem.at[2])
    arrived_at(mods.at[pl.ds(0, NZ - 1)], m_sem.at[4])
    arrived_at(lat_all.at[pl.ds(0, 3)], l_send.at[0])
    arrived_at(w_all.at[1], w_sem.at[0])
    out_weight.wait_send()
    arrived_at(packs.at[pl.ds(0, NX - 1)], c_sem.at[0])
    arrived_at(got_decays.at[pl.ds(0, NX - 1)], c_sem.at[2])
    arrived_at(ctx_groups.at[pl.ds(0, NZ - 1)], z_sem.at[0])
    arrived_at(all_decays.at[pl.ds(0, NZ - 1)], z_sem.at[2])
    for way in range(2):
        arrived_at(states.at[way], x_sem.at[way, 0])
        arrived_at(leaving.at[way], e_sem.at[way, 0])
        arrived_at(groups.at[way, pl.ds(0, NZ - 1)], z_sem.at[4 + way])
        arrived_at(entry.at[way, pl.ds(0, NZ - 1)], z_sem.at[8 + way])
    arrived_at(near, y_sem.at[3])

    def finish(k, carry):
        at = pl.ds(pl.multiple_of(k * 16, 16), 16)
        a = part_a[y, at].astype(F32) + near[0, at].astype(F32) + near[2, at].astype(F32)
        b = part_b[y, at].astype(F32) + near[1, at].astype(F32) + near[3, at].astype(F32)
        square = jnp.sum(a * a, axis=1, keepdims=True) + jnp.sum(b * b, axis=1, keepdims=True)
        scale = lax.rsqrt(square / WIDTH + EPS)
        for span, half in zip(columns, (a, b)):
            weight = vectors[2:3, span] * gain_post[span].reshape(1, HALF).astype(F32)
            result[at, span] = (
                lat_all[y, at, span].astype(F32) + half * scale * weight
            ).astype(BF)
        return carry

    lax.fori_loop(0, count // 16, finish, 0)
    arrived_at(lat_all.at[pl.ds(0, 3)], y_sem.at[0])


def mixer(*args):
    dma = pltpu.SemaphoreType.DMA
    vm = pltpu.VMEM
    half = vm((64, HALF), BF)
    in_specs = [VM] * len(args)
    for k in (0, 7, 8, 9, 10, 11, 12, 13, 14):
        in_specs[k] = ANY
    slices = vm((2, NX, 128, DK_HEAD), BF)
    thin = vm((2, NZ, 16, DK_HEAD), BF)
    return pl.pallas_call(
        mixer_kernel,
        out_shape=shape_of(64, WIDTH),
        in_specs=in_specs,
        out_specs=VM,
        scratch_shapes=[
            vm((3, 128, 1024), BF), vm((NZ, 8, 128), F32), vm((NZ, 8, 128), F32),
            vm((8, 128), F32), vm((NY * NX, 8, 128), F32), vm((NY, 8, 128), F32),
            vm((NZ, NY, 8, 128), F32), vm((8, WIDTH), F32), vm((288, 128), F32),
            vm((NY, 64, WIDTH), BF), vm((2, 288, HALF), BF), vm((2, HALF, 1536), BF),
            vm((288, 1536), BF), vm((288, 2 * RANK), BF), vm((2, DV_HEAD, HALF), BF),
            vm((NX, 32, 512), BF), vm((NX, 32, 512), BF),
            slices, slices, vm((2, 2, 64, DK_HEAD), BF), vm((2, 2, 64, DK_HEAD), BF),
            vm((8, DK_HEAD), F32), vm((NX, 8, DK_HEAD), F32),
            vm((256, 256), BF), vm((256, DV_HEAD), F32), vm((2, 256, DK_HEAD), BF),
            thin, thin, vm((NZ, 2, 16, DK_HEAD), BF), vm((NZ, 2, 16, DK_HEAD), BF),
            vm((8, DK_HEAD), F32), vm((NZ, 8, DK_HEAD), F32),
            thin, thin, vm((2, NX, 128, DK_HEAD), F32), slices, slices,
            vm((256, DV_HEAD), BF),
            vm((NY, 64, HALF), BF), vm((NY, 64, HALF), BF), vm((4, 64, HALF), BF),
            half, half, half, half,
            dma((4,)), dma((6,)), dma((1,)), dma((6,)), dma((4,)), dma((4,)),
            dma((2, 3)), dma((12,)), dma((2, 3)), dma((4,)),
        ],
        compiler_params=pltpu.CompilerParams(
            collective_id=0, has_side_effects=True, vmem_limit_bytes=60 * 2**20
        ),
        name="mixer",
    )(*args)


def body(
    latents, cond, cond_ctx, context, w_shift, w_scale, w_gate, gain_pre, gain_post,
    w_query, w_key, w_value, w_outgate, w_down, decay_up, decay_bias, head_gain, w_out,
):
    result = mixer(
        latents[0], context[0], cond, cond_ctx[None], gain_pre, gain_post, head_gain,
        w_shift, w_scale, w_gate, w_query, w_key, w_value, w_outgate, w_out,
        w_down.T, decay_up, decay_bias,
    )
    return result[None]


def solution(mesh):
    finer = Mesh(
        mesh.devices.reshape(8, 4, mesh.shape["tp"], mesh.shape["dp"]), ("sp_0", "sp_1", "tp", "dp")
    )
    in_specs = (
        P("dp", SP_TP, None),
        P("dp", SP),
        P(SP),
        P("dp", SP, None),
        P(SP, "tp"),
        P(SP, "tp"),
        P(SP, "tp"),
        P(),
        P(),
        P("dp", "tp"),
        P("dp", "tp"),
        P("dp", "tp"),
        P("dp", "tp"),
        P(),
        P(None, None, "tp"),
        P(None, "tp"),
        P("tp"),
        P("tp", "dp"),
    )
    out_specs = P("dp", SP_TP, None)
    return jax.shard_map(body, mesh=finer, in_specs=in_specs, out_specs=out_specs, check_vma=False)
```

time: 87.9 us -> 80.1 us (0.911)
  local copies, waits for them, and re-layouts: 5.75 us -> 1.87 us
  Pallas kernels: 81.9 us -> 78.1 us
    broadcast_in_dim x3 -> x0, local copies, waits for them, and re-layouts: 3.88 us -> none  [the longest x1 1.31 us: body(): gain_pre[None]]
    pallas_call x1, Pallas kernels: 81.9 us -> 78.1 us  [mixer(): pl.pallas_call(mixer_kernel, out_shape=shape_of(64, WIDTH), in_specs=in_s...]
where the time goes in v4:
time: 80.1 us; the launch traced here: 80 us
  Pallas kernels  78.1 us (98%)
  local copies, waits for them, and re-layouts  1.87 us (2%)
    pallas_call x1, Pallas kernels, mixer(): pl.pallas_call(mixer_kernel, out_shape=shape_of(64, WIDTH), in_specs=in_s...  78.1 us
    unnamed x1, local copies, waits for them, and re-layouts  1.87 us

profile of v4, /device:TPU:2, one launch (start us, length us, event | category | flops | bytes accessed | tf_op | source)
XLA Modules:
  0.0 80.0 jit_solution(3318883018013161061)
XLA Ops:
  0.0 78.1 %mixer.1 = bf16[64,4096]{1,0:T(8,128)(2,1)} custom-call(bf16[64,4096]{1,0:T(8,128)(2,1)} %bitcast.6, bf16[32,4096]{1,0:T(8,128)(2,1)} %bitcast.7, bf16[1,128]{1,0:T(2,128)(2,1)} %cond.1, bf16[1,128]{1,0:T(2,128)(2,1)} %bitcast.9, bf16[4096]{0:T(1024)(128)(2,1)} %gain_pre.1, bf16[4096]{0:T(1024)(128)(2,1)} %gain_post.1, bf16[512]{0:T(512)(128)(2,1)} %head_gain.1, ...), custom_call_target="tpu_custom_call" | custom-call | tf_op jit(solution)/shard_map/mixer/pallas_call | solution.py:475
  78.1 1.9 %copy.20 = bf16[1,64,4096]{2,1,0:T(8,128)(2,1)} copy(bf16[1,64,4096]{2,1,0:T(8,128)(2,1)} %bitcast.5) | data formatting | bytes 1048576

commit v5 on v4

--- a/solution.py
+++ b/solution.py
@@ -83,13 +83,17 @@
     return r >= c if lower else r <= c
 
 
-def running_sum(decay, lower):
-    ones = jnp.where(triangle(decay.shape[0], lower), 1.0, 0.0).astype(BF)
-    high = decay.astype(BF)
-    rest = decay - high.astype(F32)
-    middle = rest.astype(BF)
-    low = (rest - middle.astype(F32)).astype(BF)
-    return matmul(ones, high) + matmul(ones, middle) + matmul(ones, low)
+def running_sums(decay_f, decay_b):
+    n = decay_f.shape[0]
+    parts = []
+    for decay in (decay_f, decay_b):
+        high = decay.astype(BF)
+        parts += [high, (decay - high.astype(F32)).astype(BF)]
+    fwd = matmul(jnp.where(triangle(n, True), 1.0, 0.0).astype(BF), parts[0])
+    fwd = fwd + matmul(jnp.where(triangle(n, True), 1.0, 0.0).astype(BF), parts[1])
+    bwd = matmul(jnp.where(triangle(n, False), 1.0, 0.0).astype(BF), parts[2])
+    bwd = bwd + matmul(jnp.where(triangle(n, False), 1.0, 0.0).astype(BF), parts[3])
+    return fwd, bwd
 
 
 def across(left, right):
@@ -123,16 +127,20 @@
 
 
 def mixer_kernel(
-    lat, context, cond, cond_ctx, gain_pre, gain_post, head_gain, w_shift, w_scale, w_gate,
-    wq, wk, wv, wg, wo, w_down, decay_up, decay_bias,
+    lat, *inputs_and_rest
+):
+    (
+    context_in, cond_in, cond_ctx_in, gain_pre_in, gain_post_in, head_gain_in, w_shift, w_scale, w_gate,
+    wq, wk, wv, wg, wo, w_down_in, decay_up_in, decay_bias_in,
     result,
-    w_mod, partial, partials, tile, tiles, column_sum, mods, vectors, norms, lat_all, rows, w_all,
+    context, cond, cond_ctx, gain_pre, gain_post, head_gain, w_down, decay_up, decay_bias,
+    factor, offset, w_mod, partial, partials, tile, tiles, column_sum, mods, vectors, norms, lat_all, rows, w_all,
     proj, low, w_out,
     pack, packs, states, got_states, relays, relays_e, decays, got_decays, scores, local, entering,
     group, groups, ctx_group, ctx_groups, group_decays, all_decays,
     back, entry, before, leaving, entries, heads, part_a, part_b, near, sum_a, sum_b, relay_a, relay_c,
-    s_load, m_sem, l_send, l_recv, w_sem, c_sem, x_sem, z_sem, e_sem, y_sem,
-):
+    s_load, s_small, m_sem, l_send, l_recv, w_sem, c_sem, x_sem, z_sem, e_sem, y_sem,
+    ) = inputs_and_rest
     z, x, y, c = position()
     x_peers = [lax.rem(x + d, NX) for d in (1, 3, 2)]
     z_peers = [lax.rem(z + d, NZ) for d in (4, 3, 5, 2, 6, 1, 7)]
@@ -146,16 +154,37 @@
     other = dict(dp=1 - c)
     columns = [pl.ds(pl.multiple_of(k * HALF, HALF), HALF) for k in (c, 1 - c)]
     entered = greet([dict(sp_0=p) for p in z_peers] + xy_peers + [other])
-    spans = (slice(0, 256), slice(256, 512), slice(512, 1024), slice(1024, 1536))
-    sources = list(zip((wq, wk, wv, wg), spans))
+    spans = (slice(0, 256), slice(256, 768), slice(768, 1024), slice(1024, 1536))
+    sources = list(zip((wk, wv, wq, wg), spans))
+    own_rows = pltpu.make_async_copy(lat, lat_all.at[y], s_load.at[1])
+    own_rows.start()
+    small = [
+        pltpu.make_async_copy(src, dst, s_small.at[k])
+        for k, (src, dst) in enumerate(
+            [
+                (cond_in, cond), (cond_ctx_in, cond_ctx), (context_in, context),
+                (gain_pre_in, gain_pre), (gain_post_in, gain_post), (head_gain_in, head_gain),
+                (w_down_in, w_down), (decay_up_in, decay_up), (decay_bias_in, decay_bias),
+            ]
+        )
+    ]
+    for load in small[:2]:
+        load.start()
     for k, w in enumerate((w_shift, w_scale, w_gate)):
         pltpu.make_async_copy(w, w_mod.at[k], s_load.at[0]).start()
-    own_rows = pltpu.make_async_copy(lat, lat_all.at[y], s_load.at[1])
-    own_rows.start()
+    for load in small[2:]:
+        load.start()
     for w, span in sources:
         pltpu.make_async_copy(w, w_all.at[0, :, span], s_load.at[2]).start()
     own_out = pltpu.make_async_copy(wo, w_out.at[0], s_load.at[3])
     own_out.start()
+    own_rows.wait()
+    entered()
+    top, bottom = pl.ds(0, 32), pl.ds(32, 32)
+    up_1 = send(lat_all.at[y, top], lat_all.at[y, top], l_send.at[0], l_recv.at[0], **up)
+    down_1 = send(lat_all.at[y, bottom], lat_all.at[y, bottom], l_send.at[0], l_recv.at[1], **down)
+    small[0].wait()
+    small[1].wait()
     line = lax.broadcasted_iota(jnp.int32, (16, 128), 0)
     act = jax.nn.silu(cond[...].astype(F32)).astype(BF).astype(F32)
     act_ctx = jax.nn.silu(cond_ctx[...].astype(F32)).astype(BF).astype(F32)
@@ -167,14 +196,9 @@
         total = part if total is None else total + part
     for k in range(NZ):
         partial[k] = total[:8, k * 128 : (k + 1) * 128]
-    own_rows.wait()
-    entered()
     for p in z_peers:
         send(partial.at[p], partials.at[z], m_sem.at[0], m_sem.at[1], sp_0=p)
     partials[z] = partial[z]
-    top, bottom = pl.ds(0, 32), pl.ds(32, 32)
-    up_1 = send(lat_all.at[y, top], lat_all.at[y, top], l_send.at[0], l_recv.at[0], **up)
-    down_1 = send(lat_all.at[y, bottom], lat_all.at[y, bottom], l_send.at[0], l_recv.at[1], **down)
     for w, span in sources:
         send(w, w_all.at[1, :, span], w_sem.at[0], w_sem.at[1], **other)
     out_weight = send(wo, w_out.at[1], w_sem.at[2], w_sem.at[3], **other)
@@ -190,6 +214,17 @@
 
         lax.fori_loop(0, length // 16, step, 0)
 
+    for load in small[2:]:
+        load.wait()
+    ones = jnp.ones((1, WIDTH), F32)
+    zeros = jnp.zeros((1, WIDTH), F32)
+    pre = gain_pre[...].reshape(1, WIDTH).astype(F32)
+    post = gain_post[...].reshape(1, WIDTH).astype(F32)
+    for k, (by, plus) in enumerate(
+        ((ones, zeros), (pre, pre), (post, zeros), (ones, zeros), (pre, pre))
+    ):
+        factor[k : k + 1] = by
+        offset[k : k + 1] = plus
     norm_of(context, 0, 32)
     norm_of(lat_all.at[y], 32, 64)
     arrived_at(partials.at[pl.ds(0, NZ - 1)], m_sem.at[1])
@@ -215,77 +250,83 @@
     down_1.wait_recv()
     passed = lat_all.at[above, bottom]
     relay_down = send(passed, passed, l_send.at[0], l_recv.at[5], **down)
-    up_2.wait_recv()
-    norm_of(lat_all.at[below], 96, 64)
-    down_2.wait_recv()
-    norm_of(lat_all.at[above], 160, 64)
     arrived_at(mods.at[pl.ds(0, NZ - 1)], m_sem.at[5])
     for k in range(NY):
         for j in range(NZ):
             at = (k * NZ + j) * 128
-            vectors[:, at : at + 128] = mods[j, k]
-
-    def modulate(source, target, scale_row, shift_row, length):
+            span = slice(at, at + 128)
+            vectors[:, span] = mods[j, k] * factor[:, span] + offset[:, span]
+
+    def modulate(source, target, scale_row, shift_row, length, known):
         def step(k, carry):
             at = pl.ds(pl.multiple_of(k * 16, 16), 16)
             to = pl.ds(pl.multiple_of(target + k * 16, 16), 16)
-            norm = norms[to, 0:1]
+            halves = [source[at, columns[h]].astype(F32) for h in range(2)]
+            if known:
+                norm = norms[to, 0:1]
+            else:
+                square = sum(jnp.sum(v * v, axis=1, keepdims=True) for v in halves)
+                norm = lax.rsqrt(square / WIDTH + EPS)
             for h in range(2):
-                weight = gain_pre[columns[h]].reshape(1, HALF).astype(F32) * (
-                    1.0 + vectors[scale_row : scale_row + 1, columns[h]]
-                )
+                weight = vectors[scale_row : scale_row + 1, columns[h]]
                 shift = vectors[shift_row : shift_row + 1, columns[h]]
-                rows[h, to] = (source[at, columns[h]].astype(F32) * norm * weight + shift).astype(BF)
+                rows[h, to] = (halves[h] * norm * weight + shift).astype(BF)
             return carry
 
         lax.fori_loop(0, length // 16, step, 0)
 
-    def project_rows(at, length, places):
+    def project_rows(at, length, places, chunks):
         def step(k, carry):
             span = pl.ds(pl.multiple_of(k * 256, 256), 256)
             out = matmul(rows[0, at : at + length], w_all[0, :, span])
             out = (out + matmul(rows[1, at : at + length], w_all[1, :, span])).astype(BF)
             for offset, place, count in places:
                 to = pl.ds(pl.multiple_of(place, 32), count)
-                proj[to, span] = out[offset : offset + count]
+                proj[to, span] = out[offset - at : offset - at + count]
             return carry
 
-        lax.fori_loop(0, 6, step, 0)
+        lax.fori_loop(chunks.start, chunks.stop, step, 0)
+
+    def project_down(at, length, places):
         out = across(rows[0, at : at + length], w_down[:, columns[0]])
         out = (out + across(rows[1, at : at + length], w_down[:, columns[1]])).astype(BF)
         for offset, place, count in places:
-            low[pl.ds(pl.multiple_of(place, 32), count)] = out[offset : offset + count]
-
-    modulate(context, 0, 4, 3, 32)
-    modulate(lat_all.at[y], 32, 1, 0, 64)
-    modulate(lat_all.at[below], 96, 1, 0, 64)
+            low[pl.ds(pl.multiple_of(place, 32), count)] = out[offset - at : offset - at + count]
+
+    modulate(context, 0, 4, 3, 32, True)
+    modulate(lat_all.at[y], 32, 1, 0, 64, True)
+    up_2.wait_recv()
+    modulate(lat_all.at[below], 96, 1, 0, 64, False)
+    down_2.wait_recv()
+    modulate(lat_all.at[above], 160, 1, 0, 64, False)
     arrived_at(w_all.at[0], s_load.at[2])
     arrived_at(w_all.at[1], w_sem.at[1])
-    project_rows(0, 160, ((0, 256, 32), (32, y * 64, 64), (96, below * 64, 64)))
+    places = ((32, y * 64, 64), (96, below * 64, 64), (160, above * 64, 64), (224, facing * 64, 64))
+    project_rows(0, 224, ((0, 256, 32), *places[:3]), range(0, 3))
+    project_down(0, 224, ((0, 256, 32), *places[:3]))
     for j in range(NX):
         pack[j] = jnp.zeros((32, 512), BF)
-        pack[j, :, :DK_HEAD] = proj[256:288, 256:512]
-        pack[j, :, DK_HEAD : DK_HEAD + 128] = proj[256:288, 512 + j * 128 : 640 + j * 128]
+        pack[j, :, :DK_HEAD] = proj[256:288, 0:256]
+        pack[j, :, DK_HEAD : DK_HEAD + 128] = proj[256:288, 256 + j * 128 : 384 + j * 128]
         pack[j, :, DK_HEAD + 128 : DK_HEAD + 128 + 2 * RANK] = low[256:288]
     for p in x_peers:
         send(pack.at[p], packs.at[x], c_sem.at[0], c_sem.at[1], sp_1=p)
     packs[x] = pack[x]
-    modulate(lat_all.at[above], 160, 1, 0, 64)
     relay_up.wait_recv()
     relay_down.wait_recv()
-    norm_of(lat_all.at[facing], 224, 64)
-    modulate(lat_all.at[facing], 224, 1, 0, 64)
-    project_rows(160, 128, ((0, above * 64, 64), (64, facing * 64, 64)))
+    modulate(lat_all.at[facing], 224, 1, 0, 64, False)
+    project_rows(224, 64, places[3:], range(0, 3))
+    project_down(224, 64, places[3:])
     decay_f, decay_b = log_decays(low[:256], decay_up[...], decay_bias[...])
-    fwd, bwd = running_sum(decay_f, True), running_sum(decay_b, False)
+    fwd, bwd = running_sums(decay_f, decay_b)
     decays[0:1] = fwd[-1:]
     decays[1:2] = bwd[:1]
     decays[2:8] = jnp.zeros((6, DK_HEAD), F32)
     for p in x_peers:
         send(decays, got_decays.at[x], c_sem.at[2], c_sem.at[3], sp_1=p)
     got_decays[x] = decays[...]
-    k = proj[:256, 256:512].astype(F32)
-    v = proj[:256, 512:1024]
+    k = proj[:256, :256].astype(F32)
+    v = proj[:256, 256:768]
     first, second = pl.ds(0, 64), pl.ds(64, 64)
 
     def swap(source, target, relay, way, sems):
@@ -322,7 +363,7 @@
     ctx_v = ctx[:, DK_HEAD : DK_HEAD + 128]
     ctx_lr = ctx[:, DK_HEAD + 128 : DK_HEAD + 128 + 2 * RANK]
     cdf, cdb = log_decays(ctx_lr, decay_up[...], decay_bias[...])
-    cf, cb = running_sum(cdf, True), running_sum(cdb, False)
+    cf, cb = running_sums(cdf, cdb)
     for way, scaled in enumerate((jnp.exp(cf[-1:] - cf), jnp.exp(cb[:1] - cb))):
         state = outer(ctx_v, (ctx_k * scaled).astype(BF)).astype(BF)
         for j in range(NZ):
@@ -330,6 +371,7 @@
     for p in z_peers:
         send(ctx_group.at[p], ctx_groups.at[z], z_sem.at[0], z_sem.at[1], sp_0=p)
     ctx_groups[z] = ctx_group[z]
+    project_rows(32, 256, places, range(3, 4))
     pass_on(got_states, relays, 0, x_sem)
     arrived_at(got_decays.at[pl.ds(0, NX - 1)], c_sem.at[3])
     group_decays[0:2] = sum(got_decays[j, 0:2] for j in range(NX))
@@ -340,7 +382,7 @@
         send(group_decays, all_decays.at[z], z_sem.at[2], z_sem.at[3], sp_0=p)
     all_decays[z] = group_decays[...]
     pass_on(got_states, relays, 1, x_sem)
-    q = proj[:256, :256].astype(F32) * DK_HEAD ** (-0.5)
+    q = proj[:256, 768:1024].astype(F32) * DK_HEAD ** (-0.5)
     scores_of(q, k, fwd, bwd, scores)
     ways = (tuple(range(NX)), tuple(reversed(range(NX))))
     orders = (tuple(range(NZ)), tuple(reversed(range(NZ))))
@@ -356,6 +398,7 @@
         for p in z_peers:
             send(group.at[way, p], groups.at[way, z], z_sem.at[4 + way], z_sem.at[6 + way], sp_0=p)
         groups[way, z] = group[way, z]
+    project_rows(32, 256, places, range(4, 6))
     for way in range(2):
         state = jnp.zeros((128, DK_HEAD), F32)
         for j in ways[way]:
@@ -453,9 +496,8 @@
         square = jnp.sum(a * a, axis=1, keepdims=True) + jnp.sum(b * b, axis=1, keepdims=True)
         scale = lax.rsqrt(square / WIDTH + EPS)
         for span, half in zip(columns, (a, b)):
-            weight = vectors[2:3, span] * gain_post[span].reshape(1, HALF).astype(F32)
             result[at, span] = (
-                lat_all[y, at, span].astype(F32) + half * scale * weight
+                lat_all[y, at, span].astype(F32) + half * scale * vectors[2:3, span]
             ).astype(BF)
         return carry
 
@@ -467,9 +509,7 @@
     dma = pltpu.SemaphoreType.DMA
     vm = pltpu.VMEM
     half = vm((64, HALF), BF)
-    in_specs = [VM] * len(args)
-    for k in (0, 7, 8, 9, 10, 11, 12, 13, 14):
-        in_specs[k] = ANY
+    in_specs = [ANY] * len(args)
     slices = vm((2, NX, 128, DK_HEAD), BF)
     thin = vm((2, NZ, 16, DK_HEAD), BF)
     return pl.pallas_call(
@@ -478,7 +518,10 @@
         in_specs=in_specs,
         out_specs=VM,
         scratch_shapes=[
-            vm((3, 128, 1024), BF), vm((NZ, 8, 128), F32), vm((NZ, 8, 128), F32),
+            vm((32, WIDTH), BF), vm((1, 128), BF), vm((1, 128), BF),
+            vm((WIDTH,), BF), vm((WIDTH,), BF), vm((DV_HEAD,), BF),
+            vm((2 * RANK, WIDTH), BF), vm((2, RANK, DK_HEAD), BF), vm((2, DK_HEAD), F32),
+            vm((8, WIDTH), F32), vm((8, WIDTH), F32), vm((3, 128, 1024), BF), vm((NZ, 8, 128), F32), vm((NZ, 8, 128), F32),
             vm((8, 128), F32), vm((NY * NX, 8, 128), F32), vm((NY, 8, 128), F32),
             vm((NZ, NY, 8, 128), F32), vm((8, WIDTH), F32), vm((288, 128), F32),
             vm((NY, 64, WIDTH), BF), vm((2, 288, HALF), BF), vm((2, HALF, 1536), BF),
@@ -493,7 +536,7 @@
             vm((256, DV_HEAD), BF),
             vm((NY, 64, HALF), BF), vm((NY, 64, HALF), BF), vm((4, 64, HALF), BF),
             half, half, half, half,
-            dma((4,)), dma((6,)), dma((1,)), dma((6,)), dma((4,)), dma((4,)),
+            dma((4,)), dma((9,)), dma((6,)), dma((1,)), dma((6,)), dma((4,)), dma((4,)),
             dma((2, 3)), dma((12,)), dma((2, 3)), dma((4,)),
         ],
         compiler_params=pltpu.CompilerParams(

time: 80.1 us -> 77 us (0.961)
  Pallas kernels: 78.1 us -> 75 us
    pallas_call x1, Pallas kernels: 78.1 us -> 75 us  [mixer(): pl.pallas_call(mixer_kernel, out_shape=shape_of(64, WIDTH), in_specs=in_s...]
where the time goes in v5:
time: 77 us; the launch traced here: 76.9 us
  Pallas kernels  75 us (97%)
  local copies, waits for them, and re-layouts  1.87 us (2%)
    pallas_call x1, Pallas kernels, mixer(): pl.pallas_call(mixer_kernel, out_shape=shape_of(64, WIDTH), in_specs=in_s...  75 us
    unnamed x1, local copies, waits for them, and re-layouts  1.87 us

profile of v5, /device:TPU:2, one launch (start us, length us, event | category | flops | bytes accessed | tf_op | source)
XLA Modules:
  0.0 76.9 jit_solution(6426150771712286520)
XLA Ops:
  0.0 75.0 %mixer.1 = bf16[64,4096]{1,0:T(8,128)(2,1)} custom-call(bf16[64,4096]{1,0:T(8,128)(2,1)} %bitcast.6, bf16[32,4096]{1,0:T(8,128)(2,1)} %bitcast.7, bf16[1,128]{1,0:T(2,128)(2,1)} %inputs_and_rest_1_.1, bf16[1,128]{1,0:T(2,128)(2,1)} %bitcast.9, bf16[4096]{0:T(1024)(128)(2,1)} %inputs_and_rest_3_.1, bf16[4096]{0:T(1024)(128)(2,1)} %inputs_and_rest_4_.1, ...), custom_call_target="tpu_custom_call" | custom-call | tf_op jit(solution)/shard_map/mixer/pallas_call | solution.py:515
  75.0 1.9 %copy.20 = bf16[1,64,4096]{2,1,0:T(8,128)(2,1)} copy(bf16[1,64,4096]{2,1,0:T(8,128)(2,1)} %bitcast.5) | data formatting | bytes 1048576

commit v6 on v5

--- a/solution.py
+++ b/solution.py
@@ -15,6 +15,8 @@
 NZ, NX, NY = 8, 4, 4
 WIDTH = 4096
 HALF = 2048
+WHOLE = 768
+REST = HALF - WHOLE
 ANY = pl.BlockSpec(memory_space=pl.ANY)
 VM = pl.BlockSpec(memory_space=pltpu.VMEM)
 BF, F32 = jnp.bfloat16, jnp.float32
@@ -139,7 +141,8 @@
     pack, packs, states, got_states, relays, relays_e, decays, got_decays, scores, local, entering,
     group, groups, ctx_group, ctx_groups, group_decays, all_decays,
     back, entry, before, leaving, entries, heads, part_a, part_b, near, sum_a, sum_b, relay_a, relay_c,
-    s_load, s_small, m_sem, l_send, l_recv, w_sem, c_sem, x_sem, z_sem, e_sem, y_sem,
+    w_far, everyone, relay_h, whole, crossing, crossed,
+    s_load, s_small, m_sem, l_send, l_recv, w_sem, c_sem, x_sem, z_sem, e_sem, y_sem, f_sem, h_sem,
     ) = inputs_and_rest
     z, x, y, c = position()
     x_peers = [lax.rem(x + d, NX) for d in (1, 3, 2)]
@@ -201,7 +204,8 @@
     partials[z] = partial[z]
     for w, span in sources:
         send(w, w_all.at[1, :, span], w_sem.at[0], w_sem.at[1], **other)
-    out_weight = send(wo, w_out.at[1], w_sem.at[2], w_sem.at[3], **other)
+    tail = pl.ds(WHOLE, REST)
+    out_weight = send(wo.at[:, tail], w_out.at[1, :, tail], w_sem.at[2], w_sem.at[3], **other)
 
     def norm_of(source, target, length):
         def step(k, carry):
@@ -250,6 +254,12 @@
     down_1.wait_recv()
     passed = lat_all.at[above, bottom]
     relay_down = send(passed, passed, l_send.at[0], l_recv.at[5], **down)
+    own_out.wait()
+    whole_at, high, low_half = pl.ds(0, WHOLE), pl.ds(0, 256), pl.ds(256, 256)
+    far_up = send(w_out.at[0, high, whole_at], w_far.at[2, high], f_sem.at[0], f_sem.at[1], **up)
+    far_down = send(w_out.at[0, low_half, whole_at], w_far.at[0, low_half], f_sem.at[0], f_sem.at[2], **down)
+    send(w_out.at[0, low_half, whole_at], w_far.at[2, low_half], f_sem.at[0], f_sem.at[3], **up)
+    send(w_out.at[0, high, whole_at], w_far.at[0, high], f_sem.at[0], f_sem.at[4], **down)
     arrived_at(mods.at[pl.ds(0, NZ - 1)], m_sem.at[5])
     for k in range(NY):
         for j in range(NZ):
@@ -399,6 +409,10 @@
             send(group.at[way, p], groups.at[way, z], z_sem.at[4 + way], z_sem.at[6 + way], sp_0=p)
         groups[way, z] = group[way, z]
     project_rows(32, 256, places, range(4, 6))
+    far_up.wait_recv()
+    send(w_far.at[2, high], w_far.at[1, high], f_sem.at[0], f_sem.at[5], **up)
+    far_down.wait_recv()
+    send(w_far.at[0, low_half], w_far.at[1, low_half], f_sem.at[0], f_sem.at[6], **down)
     for way in range(2):
         state = jnp.zeros((128, DK_HEAD), F32)
         for j in ways[way]:
@@ -436,7 +450,6 @@
         entries[way, x] = leaving[way, x]
     pass_on(entries, relays_e, 0, e_sem)
     pass_on(entries, relays_e, 1, e_sem)
-    own_out.wait()
     out_weight.wait_recv()
     swapped(entries, 0, e_sem)
     out = [
@@ -450,14 +463,27 @@
         heads[:, j * 128 : (j + 1) * 128] = (out[j] * scale * gate[:, j * 128 : (j + 1) * 128]).astype(BF)
     count = 64
 
+    def rows_of(owner, offset=0, length=64):
+        return pl.ds(pl.multiple_of(owner * count + offset, length), length)
+
+    mine, half_1, half_2 = pl.ds(0, count), pl.ds(0, 32), pl.ds(32, 32)
+    pass_up = send(heads.at[rows_of(facing, 0, 32)], relay_h.at[0], h_sem.at[0], h_sem.at[1], **up)
+    pass_down = send(heads.at[rows_of(facing, 32, 32)], relay_h.at[1], h_sem.at[0], h_sem.at[2], **down)
+    send(heads.at[rows_of(above)], everyone.at[3, mine], h_sem.at[0], h_sem.at[3], **up)
+    send(heads.at[rows_of(below)], everyone.at[1, mine], h_sem.at[0], h_sem.at[4], **down)
+    everyone[0, :count] = heads[rows_of(y)]
+
     def project(owner, part, half):
-        at = heads[pl.ds(pl.multiple_of(owner * count, count), count)]
-        part[owner] = matmul(at, w_out[half]).astype(BF)
+        part[owner] = matmul(heads[rows_of(owner)], w_out[half, :, WHOLE:]).astype(BF)
 
     project(facing, part_a, 0)
-    first_a = send(part_a.at[facing], relay_a, y_sem.at[0], y_sem.at[1], **down)
+    first_a = send(part_a.at[facing], relay_a, y_sem.at[4], y_sem.at[1], **down)
     project(facing, part_b, 1)
-    first_b = send(part_b.at[facing], relay_c, y_sem.at[0], y_sem.at[2], **up)
+    first_b = send(part_b.at[facing], relay_c, y_sem.at[4], y_sem.at[2], **up)
+    pass_up.wait_recv()
+    send(relay_h.at[0], everyone.at[2, half_1], h_sem.at[0], h_sem.at[5], **up)
+    pass_down.wait_recv()
+    send(relay_h.at[1], everyone.at[2, half_2], h_sem.at[0], h_sem.at[6], **down)
     project(below, part_b, 1)
     send(part_b.at[below], near.at[1], y_sem.at[0], y_sem.at[3], **down)
     project(above, part_a, 0)
@@ -470,8 +496,25 @@
     first_b.wait_recv()
     sum_b[...] = (relay_c[...].astype(F32) + part_b[above].astype(F32)).astype(BF)
     send(sum_b, near.at[3], y_sem.at[0], y_sem.at[3], **up)
+    arrived_at(everyone.at[3, mine], h_sem.at[3])
+    arrived_at(everyone.at[1, mine], h_sem.at[4])
+    arrived_at(everyone.at[2, half_1], h_sem.at[5])
+    arrived_at(everyone.at[2, half_2], h_sem.at[6])
+    theirs = pl.ds(count, count)
+    over = send(everyone.at[:, mine], everyone.at[:, theirs], h_sem.at[7], h_sem.at[8], **other)
     project(y, part_a, 0)
     project(y, part_b, 1)
+    arrived_at(w_far.at[2, high], f_sem.at[3])
+    arrived_at(w_far.at[0, high], f_sem.at[4])
+    arrived_at(w_far.at[1, high], f_sem.at[5])
+    arrived_at(w_far.at[1, high], f_sem.at[6])
+    over.wait()
+    sums = matmul(everyone[0], w_out[0, :, :WHOLE])
+    for d in range(1, NY):
+        sums = sums + matmul(everyone[d], w_far[d - 1])
+    whole[...] = sums[:count]
+    crossing[...] = sums[count:]
+    cross = send(crossing, crossed, h_sem.at[9], h_sem.at[10], **other)
     arrived_at(partials.at[pl.ds(0, NZ - 1)], m_sem.at[0])
     arrived_at(tiles.at[pl.ds(0, NX * NY - 1)], m_sem.at[2])
     arrived_at(mods.at[pl.ds(0, NZ - 1)], m_sem.at[4])
@@ -487,28 +530,34 @@
         arrived_at(leaving.at[way], e_sem.at[way, 0])
         arrived_at(groups.at[way, pl.ds(0, NZ - 1)], z_sem.at[4 + way])
         arrived_at(entry.at[way, pl.ds(0, NZ - 1)], z_sem.at[8 + way])
+    arrived_at(heads.at[pl.ds(0, 256)], h_sem.at[0])
+    arrived_at(w_far, f_sem.at[0])
+    cross.wait()
     arrived_at(near, y_sem.at[3])
 
     def finish(k, carry):
         at = pl.ds(pl.multiple_of(k * 16, 16), 16)
         a = part_a[y, at].astype(F32) + near[0, at].astype(F32) + near[2, at].astype(F32)
         b = part_b[y, at].astype(F32) + near[1, at].astype(F32) + near[3, at].astype(F32)
-        square = jnp.sum(a * a, axis=1, keepdims=True) + jnp.sum(b * b, axis=1, keepdims=True)
+        pieces = ((whole[at], c, 0), (a, c, WHOLE), (crossed[at], 1 - c, 0), (b, 1 - c, WHOLE))
+        square = sum(jnp.sum(v * v, axis=1, keepdims=True) for v, _, _ in pieces)
         scale = lax.rsqrt(square / WIDTH + EPS)
-        for span, half in zip(columns, (a, b)):
+        for v, half, start in pieces:
+            span = pl.ds(pl.multiple_of(half * HALF + start, 128), v.shape[1])
             result[at, span] = (
-                lat_all[y, at, span].astype(F32) + half * scale * vectors[2:3, span]
+                lat_all[y, at, span].astype(F32) + v * scale * vectors[2:3, span]
             ).astype(BF)
         return carry
 
     lax.fori_loop(0, count // 16, finish, 0)
-    arrived_at(lat_all.at[pl.ds(0, 3)], y_sem.at[0])
+    arrived_at(near, y_sem.at[0])
+    arrived_at(near.at[pl.ds(0, 2)], y_sem.at[4])
 
 
 def mixer(*args):
     dma = pltpu.SemaphoreType.DMA
     vm = pltpu.VMEM
-    half = vm((64, HALF), BF)
+    half = vm((64, REST), BF)
     in_specs = [ANY] * len(args)
     slices = vm((2, NX, 128, DK_HEAD), BF)
     thin = vm((2, NZ, 16, DK_HEAD), BF)
@@ -534,10 +583,12 @@
             vm((8, DK_HEAD), F32), vm((NZ, 8, DK_HEAD), F32),
             thin, thin, vm((2, NX, 128, DK_HEAD), F32), slices, slices,
             vm((256, DV_HEAD), BF),
-            vm((NY, 64, HALF), BF), vm((NY, 64, HALF), BF), vm((4, 64, HALF), BF),
+            vm((NY, 64, REST), BF), vm((NY, 64, REST), BF), vm((4, 64, REST), BF),
             half, half, half, half,
+            vm((3, DV_HEAD, WHOLE), BF), vm((NY, 128, DV_HEAD), BF), vm((2, 32, DV_HEAD), BF),
+            vm((64, WHOLE), F32), vm((64, WHOLE), F32), vm((64, WHOLE), F32),
             dma((4,)), dma((9,)), dma((6,)), dma((1,)), dma((6,)), dma((4,)), dma((4,)),
-            dma((2, 3)), dma((12,)), dma((2, 3)), dma((4,)),
+            dma((2, 3)), dma((12,)), dma((2, 3)), dma((5,)), dma((7,)), dma((11,)),
         ],
         compiler_params=pltpu.CompilerParams(
             collective_id=0, has_side_effects=True, vmem_limit_bytes=60 * 2**20

time: 77 us -> 74.2 us (0.964); the launches traced: 76.9 us -> 73.2 us
  Pallas kernels: 75 us -> 71.4 us
    pallas_call x1, Pallas kernels: 75 us -> 71.4 us  [mixer(): pl.pallas_call(mixer_kernel, out_shape=shape_of(64, WIDTH), in_specs=in_s...]
where the time goes in v6:
time: 74.2 us; the launch traced here: 73.2 us
  Pallas kernels  71.4 us (96%)
  local copies, waits for them, and re-layouts  1.87 us (3%)
    pallas_call x1, Pallas kernels, mixer(): pl.pallas_call(mixer_kernel, out_shape=shape_of(64, WIDTH), in_specs=in_s...  71.4 us
    unnamed x1, local copies, waits for them, and re-layouts  1.87 us

profile of v6, /device:TPU:2, one launch (start us, length us, event | category | flops | bytes accessed | tf_op | source)
XLA Modules:
  0.0 73.2 jit_solution(7983217498154200890)
XLA Ops:
  0.0 71.4 %mixer.1 = bf16[64,4096]{1,0:T(8,128)(2,1)} custom-call(bf16[64,4096]{1,0:T(8,128)(2,1)} %bitcast.6, bf16[32,4096]{1,0:T(8,128)(2,1)} %bitcast.7, bf16[1,128]{1,0:T(2,128)(2,1)} %inputs_and_rest_1_.1, bf16[1,128]{1,0:T(2,128)(2,1)} %bitcast.9, bf16[4096]{0:T(1024)(128)(2,1)} %inputs_and_rest_3_.1, bf16[4096]{0:T(1024)(128)(2,1)} %inputs_and_rest_4_.1, ...), custom_call_target="tpu_custom_call" | custom-call | tf_op jit(solution)/shard_map/mixer/pallas_call | solution.py:564
  71.4 1.9 %copy.20 = bf16[1,64,4096]{2,1,0:T(8,128)(2,1)} copy(bf16[1,64,4096]{2,1,0:T(8,128)(2,1)} %bitcast.5) | data formatting | bytes 1048576

commit v7 on v6

--- a/solution.py
+++ b/solution.py
@@ -15,7 +15,7 @@
 NZ, NX, NY = 8, 4, 4
 WIDTH = 4096
 HALF = 2048
-WHOLE = 768
+WHOLE = 640
 REST = HALF - WHOLE
 ANY = pl.BlockSpec(memory_space=pl.ANY)
 VM = pl.BlockSpec(memory_space=pltpu.VMEM)
@@ -138,10 +138,10 @@
     context, cond, cond_ctx, gain_pre, gain_post, head_gain, w_down, decay_up, decay_bias,
     factor, offset, w_mod, partial, partials, tile, tiles, column_sum, mods, vectors, norms, lat_all, rows, w_all,
     proj, low, w_out,
-    pack, packs, states, got_states, relays, relays_e, decays, got_decays, scores, local, entering,
+    pack, packs, states, got_states, decays, got_decays, scores, local, entering,
     group, groups, ctx_group, ctx_groups, group_decays, all_decays,
     back, entry, before, leaving, entries, heads, part_a, part_b, near, sum_a, sum_b, relay_a, relay_c,
-    w_far, everyone, relay_h, whole, crossing, crossed,
+    w_far, everyone, whole, crossing, crossed,
     s_load, s_small, m_sem, l_send, l_recv, w_sem, c_sem, x_sem, z_sem, e_sem, y_sem, f_sem, h_sem,
     ) = inputs_and_rest
     z, x, y, c = position()
@@ -337,23 +337,10 @@
     got_decays[x] = decays[...]
     k = proj[:256, :256].astype(F32)
     v = proj[:256, 256:768]
-    first, second = pl.ds(0, 64), pl.ds(64, 64)
-
-    def swap(source, target, relay, way, sems):
-        far = source.at[way, opposite]
-        there = target.at[way, x]
-        sent, got = sems.at[way, 0], sems.at[way, 1]
-        passed = sems.at[way, 2]
-        send(far.at[first], relay.at[way, 0], sent, passed, sp_1=east)
-        send(far.at[second], relay.at[way, 1], sent, passed, sp_1=west)
-        send(source.at[way, east], there, sent, got, sp_1=east)
-        send(source.at[way, west], there, sent, got, sp_1=west)
-
-    def pass_on(target, relay, way, sems):
-        arrived_at(relay.at[way], sems.at[way, 2])
-        sent, got = sems.at[way, 0], sems.at[way, 1]
-        send(relay.at[way, 0], target.at[way, west, first], sent, got, sp_1=east)
-        send(relay.at[way, 1], target.at[way, east, second], sent, got, sp_1=west)
+
+    def swap(source, target, way, sems):
+        for p in (opposite, east, west):
+            send(source.at[way, p], target.at[way, x], sems.at[way, 0], sems.at[way, 1], sp_1=p)
 
     def swapped(target, way, sems):
         arrived_at(target.at[way, pl.ds(0, NX - 1)], sems.at[way, 1])
@@ -362,7 +349,7 @@
         state = outer(v, (k * scaled).astype(BF)).astype(BF)
         for j in range(NX):
             states[way, j] = state[j * 128 : (j + 1) * 128]
-        swap(states, got_states, relays, way, x_sem)
+        swap(states, got_states, way, x_sem)
         got_states[way, x] = states[way, x]
 
     local_state(0, jnp.exp(fwd[-1:] - fwd))
@@ -382,7 +369,6 @@
         send(ctx_group.at[p], ctx_groups.at[z], z_sem.at[0], z_sem.at[1], sp_0=p)
     ctx_groups[z] = ctx_group[z]
     project_rows(32, 256, places, range(3, 4))
-    pass_on(got_states, relays, 0, x_sem)
     arrived_at(got_decays.at[pl.ds(0, NX - 1)], c_sem.at[3])
     group_decays[0:2] = sum(got_decays[j, 0:2] for j in range(NX))
     group_decays[2:3] = cf[-1:]
@@ -391,7 +377,6 @@
     for p in z_peers:
         send(group_decays, all_decays.at[z], z_sem.at[2], z_sem.at[3], sp_0=p)
     all_decays[z] = group_decays[...]
-    pass_on(got_states, relays, 1, x_sem)
     q = proj[:256, 768:1024].astype(F32) * DK_HEAD ** (-0.5)
     scores_of(q, k, fwd, bwd, scores)
     ways = (tuple(range(NX)), tuple(reversed(range(NX))))
@@ -446,10 +431,8 @@
         for j in ways[way]:
             leaving[way, j] = (start * jnp.exp(passed) + before[way, j]).astype(BF)
             passed = passed + got_decays[j, way : way + 1]
-        swap(leaving, entries, relays_e, way, e_sem)
+        swap(leaving, entries, way, e_sem)
         entries[way, x] = leaving[way, x]
-    pass_on(entries, relays_e, 0, e_sem)
-    pass_on(entries, relays_e, 1, e_sem)
     out_weight.wait_recv()
     swapped(entries, 0, e_sem)
     out = [
@@ -463,14 +446,13 @@
         heads[:, j * 128 : (j + 1) * 128] = (out[j] * scale * gate[:, j * 128 : (j + 1) * 128]).astype(BF)
     count = 64
 
-    def rows_of(owner, offset=0, length=64):
-        return pl.ds(pl.multiple_of(owner * count + offset, length), length)
-
-    mine, half_1, half_2 = pl.ds(0, count), pl.ds(0, 32), pl.ds(32, 32)
-    pass_up = send(heads.at[rows_of(facing, 0, 32)], relay_h.at[0], h_sem.at[0], h_sem.at[1], **up)
-    pass_down = send(heads.at[rows_of(facing, 32, 32)], relay_h.at[1], h_sem.at[0], h_sem.at[2], **down)
-    send(heads.at[rows_of(above)], everyone.at[3, mine], h_sem.at[0], h_sem.at[3], **up)
-    send(heads.at[rows_of(below)], everyone.at[1, mine], h_sem.at[0], h_sem.at[4], **down)
+    def rows_of(owner):
+        return pl.ds(pl.multiple_of(owner * count, count), count)
+
+    mine = pl.ds(0, count)
+    send(heads.at[rows_of(facing)], everyone.at[2, mine], h_sem.at[0], h_sem.at[1], tp=facing)
+    send(heads.at[rows_of(above)], everyone.at[3, mine], h_sem.at[0], h_sem.at[1], **up)
+    send(heads.at[rows_of(below)], everyone.at[1, mine], h_sem.at[0], h_sem.at[1], **down)
     everyone[0, :count] = heads[rows_of(y)]
 
     def project(owner, part, half):
@@ -480,30 +462,23 @@
     first_a = send(part_a.at[facing], relay_a, y_sem.at[4], y_sem.at[1], **down)
     project(facing, part_b, 1)
     first_b = send(part_b.at[facing], relay_c, y_sem.at[4], y_sem.at[2], **up)
-    pass_up.wait_recv()
-    send(relay_h.at[0], everyone.at[2, half_1], h_sem.at[0], h_sem.at[5], **up)
-    pass_down.wait_recv()
-    send(relay_h.at[1], everyone.at[2, half_2], h_sem.at[0], h_sem.at[6], **down)
     project(below, part_b, 1)
     send(part_b.at[below], near.at[1], y_sem.at[0], y_sem.at[3], **down)
     project(above, part_a, 0)
     send(part_a.at[above], near.at[0], y_sem.at[0], y_sem.at[3], **up)
     project(below, part_a, 0)
     project(above, part_b, 1)
+    arrived_at(everyone.at[pl.ds(1, 3), mine], h_sem.at[1])
+    theirs = pl.ds(count, count)
+    over = send(everyone.at[:, mine], everyone.at[:, theirs], h_sem.at[2], h_sem.at[3], **other)
+    project(y, part_a, 0)
+    project(y, part_b, 1)
     first_a.wait_recv()
     sum_a[...] = (relay_a[...].astype(F32) + part_a[below].astype(F32)).astype(BF)
     send(sum_a, near.at[2], y_sem.at[0], y_sem.at[3], **down)
     first_b.wait_recv()
     sum_b[...] = (relay_c[...].astype(F32) + part_b[above].astype(F32)).astype(BF)
     send(sum_b, near.at[3], y_sem.at[0], y_sem.at[3], **up)
-    arrived_at(everyone.at[3, mine], h_sem.at[3])
-    arrived_at(everyone.at[1, mine], h_sem.at[4])
-    arrived_at(everyone.at[2, half_1], h_sem.at[5])
-    arrived_at(everyone.at[2, half_2], h_sem.at[6])
-    theirs = pl.ds(count, count)
-    over = send(everyone.at[:, mine], everyone.at[:, theirs], h_sem.at[7], h_sem.at[8], **other)
-    project(y, part_a, 0)
-    project(y, part_b, 1)
     arrived_at(w_far.at[2, high], f_sem.at[3])
     arrived_at(w_far.at[0, high], f_sem.at[4])
     arrived_at(w_far.at[1, high], f_sem.at[5])
@@ -514,7 +489,7 @@
         sums = sums + matmul(everyone[d], w_far[d - 1])
     whole[...] = sums[:count]
     crossing[...] = sums[count:]
-    cross = send(crossing, crossed, h_sem.at[9], h_sem.at[10], **other)
+    cross = send(crossing, crossed, h_sem.at[4], h_sem.at[5], **other)
     arrived_at(partials.at[pl.ds(0, NZ - 1)], m_sem.at[0])
     arrived_at(tiles.at[pl.ds(0, NX * NY - 1)], m_sem.at[2])
     arrived_at(mods.at[pl.ds(0, NZ - 1)], m_sem.at[4])
@@ -526,11 +501,11 @@
     arrived_at(ctx_groups.at[pl.ds(0, NZ - 1)], z_sem.at[0])
     arrived_at(all_decays.at[pl.ds(0, NZ - 1)], z_sem.at[2])
     for way in range(2):
-        arrived_at(states.at[way], x_sem.at[way, 0])
-        arrived_at(leaving.at[way], e_sem.at[way, 0])
+        arrived_at(states.at[way, pl.ds(0, NX - 1)], x_sem.at[way, 0])
+        arrived_at(leaving.at[way, pl.ds(0, NX - 1)], e_sem.at[way, 0])
         arrived_at(groups.at[way, pl.ds(0, NZ - 1)], z_sem.at[4 + way])
         arrived_at(entry.at[way, pl.ds(0, NZ - 1)], z_sem.at[8 + way])
-    arrived_at(heads.at[pl.ds(0, 256)], h_sem.at[0])
+    arrived_at(heads.at[pl.ds(0, 192)], h_sem.at[0])
     arrived_at(w_far, f_sem.at[0])
     cross.wait()
     arrived_at(near, y_sem.at[3])
@@ -576,7 +551,7 @@
             vm((NY, 64, WIDTH), BF), vm((2, 288, HALF), BF), vm((2, HALF, 1536), BF),
             vm((288, 1536), BF), vm((288, 2 * RANK), BF), vm((2, DV_HEAD, HALF), BF),
             vm((NX, 32, 512), BF), vm((NX, 32, 512), BF),
-            slices, slices, vm((2, 2, 64, DK_HEAD), BF), vm((2, 2, 64, DK_HEAD), BF),
+            slices, slices,
             vm((8, DK_HEAD), F32), vm((NX, 8, DK_HEAD), F32),
             vm((256, 256), BF), vm((256, DV_HEAD), F32), vm((2, 256, DK_HEAD), BF),
             thin, thin, vm((NZ, 2, 16, DK_HEAD), BF), vm((NZ, 2, 16, DK_HEAD), BF),
@@ -585,10 +560,10 @@
             vm((256, DV_HEAD), BF),
             vm((NY, 64, REST), BF), vm((NY, 64, REST), BF), vm((4, 64, REST), BF),
             half, half, half, half,
-            vm((3, DV_HEAD, WHOLE), BF), vm((NY, 128, DV_HEAD), BF), vm((2, 32, DV_HEAD), BF),
+            vm((3, DV_HEAD, WHOLE), BF), vm((NY, 128, DV_HEAD), BF),
             vm((64, WHOLE), F32), vm((64, WHOLE), F32), vm((64, WHOLE), F32),
             dma((4,)), dma((9,)), dma((6,)), dma((1,)), dma((6,)), dma((4,)), dma((4,)),
-            dma((2, 3)), dma((12,)), dma((2, 3)), dma((5,)), dma((7,)), dma((11,)),
+            dma((2, 2)), dma((12,)), dma((2, 2)), dma((5,)), dma((7,)), dma((6,)),
         ],
         compiler_params=pltpu.CompilerParams(
             collective_id=0, has_side_effects=True, vmem_limit_bytes=60 * 2**20

time: 74.2 us -> 70.7 us (0.953); the launches traced: 73.2 us -> 70.6 us
  Pallas kernels: 71.4 us -> 68.7 us
    pallas_call x1, Pallas kernels: 71.4 us -> 68.7 us  [mixer(): pl.pallas_call(mixer_kernel, out_shape=shape_of(64, WIDTH), in_specs=in_s...]
where the time goes in v7:
time: 70.7 us; the launch traced here: 70.6 us
  Pallas kernels  68.7 us (97%)
  local copies, waits for them, and re-layouts  1.87 us (3%)
    pallas_call x1, Pallas kernels, mixer(): pl.pallas_call(mixer_kernel, out_shape=shape_of(64, WIDTH), in_specs=in_s...  68.7 us
    unnamed x1, local copies, waits for them, and re-layouts  1.87 us

profile of v7, /device:TPU:2, one launch (start us, length us, event | category | flops | bytes accessed | tf_op | source)
XLA Modules:
  0.0 70.6 jit_solution(2121590661375747882)
XLA Ops:
  0.0 68.7 %mixer.1 = bf16[64,4096]{1,0:T(8,128)(2,1)} custom-call(bf16[64,4096]{1,0:T(8,128)(2,1)} %bitcast.6, bf16[32,4096]{1,0:T(8,128)(2,1)} %bitcast.7, bf16[1,128]{1,0:T(2,128)(2,1)} %inputs_and_rest_1_.1, bf16[1,128]{1,0:T(2,128)(2,1)} %bitcast.9, bf16[4096]{0:T(1024)(128)(2,1)} %inputs_and_rest_3_.1, bf16[4096]{0:T(1024)(128)(2,1)} %inputs_and_rest_4_.1, ...), custom_call_target="tpu_custom_call" | custom-call | tf_op jit(solution)/shard_map/mixer/pallas_call | solution.py:539
  68.7 1.9 %copy.20 = bf16[1,64,4096]{2,1,0:T(8,128)(2,1)} copy(bf16[1,64,4096]{2,1,0:T(8,128)(2,1)} %bitcast.5) | data formatting | bytes 1048576
